TPU v7x, 768 devices: a whole 4x8x12 slice. The times are simulated.
768 devices in a mesh: ep: 24 (over z, core), tp: 32 (over y, x).
Axes of the slice: x: 4, y: 8, z: 12, core: 2. Of those that a mesh axis runs over, the one named last changes fastest.
Arguments:
- tokens: bfloat16 [6144, 2048], P('ep'), may hold values from -6 to 6
- norm_gain: float32 [2048], replicated, may hold values from 0.1 to 1.9
- expert_ids: int32 [6144, 2], P('ep'), may hold values from 0 to 23, all different within a row; in each aligned block of 256 rows (0 to 255, 256 to 511, ...) at most 32 rows name the same one
- routing_weight: float32 [6144, 2], P('ep'), may hold values from 0.1 to 1
- expert_gate: bfloat16 [24, 2048, 5632], P('ep', None, 'tp'), may hold values from -0.125 to 0.125
- expert_up: bfloat16 [24, 2048, 5632], P('ep', None, 'tp'), may hold values from -0.125 to 0.125
- expert_down: bfloat16 [24, 5632, 2048], P('ep', 'tp'), may hold values from -0.078125 to 0.078125
- dense_gate_w: bfloat16 [2048, 1024], P(None, 'tp'), may hold values from -0.125 to 0.125
- dense_up_w: bfloat16 [2048, 1024], P(None, 'tp'), may hold values from -0.125 to 0.125
- dense_down_w: bfloat16 [1024, 2048], P('tp'), may hold values from -0.1875 to 0.1875
- dense_gate: float32 [2048], P('tp'), may hold values from -3 to 3
Outputs:
- layer_out: bfloat16 [6144, 2048], P('ep', 'tp')
Inputs may be any that keep to these rules, and one draw needn't show every extreme that they name: `expert_ids`: within the 256 rows of one device along ep, each row names two different experts and no expert is named by more than 32 rows; some expert is named by exactly 32 rows.
All inputs are finite; a program needn't handle non-finite values.
Results may differ from a plain program's by a relative error of at most 0.017.
Values may be sent and summed in bfloat16 or wider, within the bound.
No kernel may reach another device: no remote copies, remote signals or barrier semaphores. Data moves between devices by JAX's collectives and lax.ppermute only.
A program may use at most 64 MiB of HBM per device.

v0:
```python
import jax
import jax.numpy as jnp
from jax import lax
from jax.sharding import Mesh
from jax.sharding import PartitionSpec as P

TP = ("yh", "yl", "xh", "xl")
FAR, NEAR = 8, 4

EPSILON = 1e-06


def exchange(blocks, axes):
    return lax.all_to_all(blocks, axes, split_axis=0, concat_axis=0, tiled=True)


def send(value, target):
    pairs = []
    for y in range(FAR):
        for x in range(NEAR):
            there_y, there_x = target(y, x)
            pairs.append((y * NEAR + x, there_y % FAR * NEAR + there_x % NEAR))
    return lax.ppermute(value, TP, pairs)


def pair(y, x):
    return y, x ^ 1


def across(x):
    return x + (1 if x % 2 else -1)


def up_one(y, x):
    return y + 1, across(x)


def down_one(y, x):
    return y - 1, across(x)


def up_two(y, x):
    return y + 2, x


def down_two(y, x):
    return y - 2, x


def dot(left, right, left_dim, right_dim):
    return lax.dot_general(
        left, right, (((left_dim,), (right_dim,)), ((), ())), preferred_element_type=jnp.float32
    )


def slots_of(ids, experts):
    tokens = ids.shape[1]
    named = ids[:, None, :] == jnp.arange(experts, dtype=jnp.int32)[None, :, None]
    count = (named[0] | named[1]).astype(jnp.bfloat16)
    before = lax.broadcasted_iota(jnp.int32, (tokens, tokens), 0) < lax.broadcasted_iota(
        jnp.int32, (tokens, tokens), 1
    )
    earlier = dot(count, before.astype(jnp.bfloat16), 1, 0).astype(jnp.int32)
    return jnp.sum(jnp.where(named, earlier[None], 0), axis=1)


def silu_times(gate_act, up_act):
    return (jax.nn.silu(gate_act) * up_act).astype(jnp.bfloat16)


def total_of(terms):
    return sum(term.astype(jnp.float32) for term in terms).astype(jnp.bfloat16)


def by_class(weight):
    run = weight.shape[1] // FAR
    order = [(m + 4 * high) * run for m in range(4) for high in range(2)]
    return jnp.concatenate([weight[:, first : first + run] for first in order], axis=1)


def local(
    tokens,
    norm_gain,
    expert_ids,
    routing_weight,
    expert_gate,
    expert_up,
    expert_down,
    dense_gate_w,
    dense_up_w,
    dense_down_w,
    dense_gate,
):
    experts = lax.axis_size("ep")
    group_tokens, model_width = tokens.shape
    capacity = 3 * group_tokens // experts
    few = capacity // 2
    rows_mine = experts * few
    part = model_width // (FAR * NEAR)
    wide = model_width // 4
    hidden_part = expert_gate.shape[2]
    x_at = lax.axis_index("xh") * 2 + lax.axis_index("xl")
    mine = lax.axis_index("yl")
    color = (x_at + mine) % 2
    far_at = lax.axis_index("yh") * 2 + lax.axis_index("xh")

    own_w = [expert_gate[0].T, expert_up[0].T, by_class(expert_down[0])]
    swapped = send(jnp.concatenate(own_w, axis=0), pair)
    other_w = [swapped[i * hidden_part : (i + 1) * hidden_part] for i in range(3)]

    def of_class(weight, step, dim):
        return lax.dynamic_slice_in_dim(weight, (mine + step) % 4 * wide, wide, dim)

    values = tokens.astype(jnp.float32)
    factor = lax.rsqrt(jnp.mean(values * values, axis=-1, keepdims=True) + EPSILON)
    normed = (values * factor * norm_gain[None, :]).astype(jnp.bfloat16)
    ids = expert_ids.T
    shifted = slots_of(ids, experts) - color * few
    places = jnp.where((shifted >= 0) & (shifted < few), ids * few + shifted, -1)
    slot_no = lax.broadcasted_iota(jnp.int32, (rows_mine, group_tokens), 0)
    chosen = [(places[c][None, :] == slot_no).astype(jnp.bfloat16) for c in range(2)]
    outgoing = dot(chosen[0] + chosen[1], of_class(normed, 0, 1), 1, 0).astype(jnp.bfloat16)
    landed = exchange(outgoing.reshape(experts, few, wide), "ep").reshape(rows_mine, wide)

    dense_hidden = silu_times(dot(normed, dense_gate_w, 1, 0), dot(normed, dense_up_w, 1, 0))
    dense_down = by_class(dense_down_w)
    dense_part = [
        dot(of_class(dense_down, step, 1), dense_hidden, 0, 1).astype(jnp.bfloat16)
        for step in range(4)
    ]
    dense_sum = total_of(
        [
            dense_part[0],
            send(dense_part[1], up_one),
            send(dense_part[2], up_two),
            send(dense_part[3], down_one),
        ]
    )
    dense_pieces = exchange(dense_sum.reshape(8, part, group_tokens), ("yh", "xh", "xl"))
    dense_out = dense_pieces.astype(jnp.float32).sum(axis=0)

    block = rows_mine // 2
    arrived = [
        landed,
        send(landed, up_one),
        jnp.concatenate([send(landed[:block], up_two), send(landed[block:], down_two)], axis=0),
        send(landed, down_one),
    ]

    def hidden_of(weights):
        gate_act = sum(dot(r, of_class(weights[0], -k, 1), 1, 1) for k, r in enumerate(arrived))
        up_act = sum(dot(r, of_class(weights[1], -k, 1), 1, 1) for k, r in enumerate(arrived))
        return silu_times(gate_act, up_act)

    own_hidden, other_hidden = hidden_of(own_w), hidden_of(other_w)
    partial = [
        (
            dot(own_hidden, of_class(own_w[2], step, 1), 1, 0)
            + dot(other_hidden, of_class(other_w[2], step, 1), 1, 0)
        ).astype(jnp.bfloat16)
        for step in range(4)
    ]
    back_two = [send(partial[2][:block], up_two), send(partial[2][block:], down_two)]
    near_sum = total_of(
        [
            partial[0],
            jnp.concatenate(back_two, axis=0),
            send(partial[1], up_one),
            send(partial[3], down_one),
        ]
    )

    def far_piece(step):
        return lax.dynamic_slice_in_dim(near_sum, (far_at ^ step) * 2 * part, 2 * part, 1)

    expert_out = total_of(
        [
            far_piece(0),
            send(far_piece(1), lambda y, x: (y, x + 2)),
            send(far_piece(2), lambda y, x: (y + 4, x)),
            send(far_piece(3), lambda y, x: (y + 4, x + 2)),
        ]
    )
    returned = exchange(expert_out.reshape(experts, few, 2 * part), "ep")
    returned = returned.reshape(rows_mine, 2 * part)
    weight = routing_weight.T
    routed = sum(weight[c][None, :] * dot(returned, chosen[c], 0, 0) for c in range(2))
    keep = lax.dynamic_slice_in_dim(routed, x_at % 2 * part, part, 0)
    give = lax.dynamic_slice_in_dim(routed, (1 - x_at % 2) * part, part, 0)
    routed = keep + send(give.astype(jnp.bfloat16), pair).astype(jnp.float32)
    gate_factor = jax.nn.sigmoid(dense_gate)[:, None]
    return (routed + gate_factor * dense_out).astype(jnp.bfloat16).T


def solution(mesh):
    sizes = (mesh.shape["ep"], FAR // 4, 4, NEAR // 2, 2)
    finer = Mesh(mesh.devices.reshape(sizes), ("ep", *TP))
    in_specs = (
        P("ep", None),
        P(),
        P("ep", None),
        P("ep", None),
        P("ep", None, TP),
        P("ep", None, TP),
        P("ep", TP, None),
        P(None, TP),
        P(None, TP),
        P(TP, None),
        P(TP),
    )
    out_specs = P("ep", TP)
    return jax.shard_map(local, mesh=finer, in_specs=in_specs, out_specs=out_specs, check_vma=False)
```

profile of v0, /device:TPU:1, one launch (start us, length us, event | category | flops | bytes accessed | tf_op | source)
XLA Modules:
  0.0 182.0 jit_solution(5698721390667801591)
XLA Ops:
  6.5 16.7 %all-to-all-start = ((bf16[24,16,512]{2,1,0:T(8,128)(2,1)}), bf16[24,16,512]{2,1,0:T(8,128)(2,1)S(1)}, u32[]{:S(2)}, u32[]{:S(2)}) async-start(bf16[24,16,512]{2,1,0:T(8,128)(2,1)} %bitcast.6), calls=%async_computation | async-start | bytes 786432 | tf_op jit(solution)/shard_map/all_to_all | solution.py:14
  30.5 2.8 %pad_maximum_fusion = bf16[528,2048]{1,0:T(8,128)(2,1)} fusion(bf16[176,2048]{1,0:T(8,128)(2,1)S(1)} %slice_dynamic-update-slice_fusion, bf16[176,2048]{1,0:T(8,128)(2,1)} %bitcast.93, bf16[176,2048]{1,0:T(8,128)(2,1)S(1)} %bitcast.92), kind=kLoop, calls=%fused_computation.2 | loop fusion | flops 6488064 | bytes 4325376 | tf_op jit(solution)/shard_map/concatenate | solution.py:108
  33.2 3.1 %collective-permute-start.4 = (bf16[528,2048]{1,0:T(8,128)(2,1)}, bf16[528,2048]{1,0:T(8,128)(2,1)}, u32[]{:S(2)}, u32[]{:S(2)}) collective-permute-start(bf16[528,2048]{1,0:T(8,128)(2,1)} %pad_maximum_fusion), channel_id=1, source_target_pairs={{0,1},{1,0},{2,3},{3,2},{4,5},{5,4},{6,7},{7,6},{8,9},{9,8},{10,11... | collective-permute-start | bytes 6488072 | tf_op jit(solution)/shard_map/ppermute | solution.py:23
  37.6 4.7 %collective-permute-start.13 = (bf16[512,256]{1,0:T(8,128)(2,1)S(1)}, bf16[512,256]{1,0:T(8,128)(2,1)}, u32[]{:S(2)}, u32[]{:S(2)}) collective-permute-start(bf16[512,256]{1,0:T(8,128)(2,1)S(1)} %convolution_convert_fusion.3), channel_id=1, source_target_pairs={{0,7},{1,6},{2,5},{3,4},{4,11},{5,10},{6,9},{7,8},{8,15},{9,14},{1... | collective-permute-start | bytes 786440 | tf_op jit(solution)/shard_map/ppermute | solution.py:23
  43.7 5.0 %collective-permute-start.3 = (bf16[384,512]{1,0:T(8,128)(2,1)S(1)}, bf16[384,512]{1,0:T(8,128)(2,1)S(1)}, u32[]{:S(2)}, u32[]{:S(2)}) collective-permute-start(bf16[384,512]{1,0:T(8,128)(2,1)S(1)} %bitcast.86), channel_id=1, source_target_pairs={{0,31},{1,30},{2,29},{3,28},{4,3},{5,2},{6,1},{7,0},{8,7},{9,6},{1... | collective-permute-start | bytes 1179656 | tf_op jit(solution)/shard_map/ppermute | solution.py:23
  51.1 5.5 %collective-permute-start.2 = (bf16[192,512]{1,0:T(8,128)(2,1)S(1)}, bf16[192,512]{1,0:T(8,128)(2,1)S(1)}, u32[]{:S(2)}, u32[]{:S(2)}) collective-permute-start(bf16[192,512]{1,0:T(8,128)(2,1)S(1)} %bitcast.104), channel_id=1, source_target_pairs={{0,24},{1,25},{2,26},{3,27},{4,28},{5,29},{6,30},{7,31},{8,0},{9,1... | collective-permute-start | bytes 589832 | tf_op jit(solution)/shard_map/ppermute | solution.py:23
  56.9 4.6 %collective-permute-done.1 = bf16[192,512]{1,0:T(8,128)(2,1)S(1)} collective-permute-done((bf16[192,512]{1,0:T(8,128)(2,1)S(1)}, bf16[192,512]{1,0:T(8,128)(2,1)S(1)}, u32[]{:S(2)}, u32[]{:S(2)}) %collective-permute-start.1) | collective-permute-done | bytes 196640 | tf_op jit(solution)/shard_map/ppermute | solution.py:23
  63.4 3.4 %collective-permute-done.2 = bf16[192,512]{1,0:T(8,128)(2,1)S(1)} collective-permute-done((bf16[192,512]{1,0:T(8,128)(2,1)S(1)}, bf16[192,512]{1,0:T(8,128)(2,1)S(1)}, u32[]{:S(2)}, u32[]{:S(2)}) %collective-permute-start.2) | collective-permute-done | bytes 196640 | tf_op jit(solution)/shard_map/ppermute | solution.py:23
  67.4 7.4 %collective-permute-done = bf16[384,512]{1,0:T(8,128)(2,1)S(1)} collective-permute-done((bf16[384,512]{1,0:T(8,128)(2,1)S(1)}, bf16[384,512]{1,0:T(8,128)(2,1)S(1)}, u32[]{:S(2)}, u32[]{:S(2)}) %collective-permute-start) | collective-permute-done | bytes 393248 | tf_op jit(solution)/shard_map/ppermute | solution.py:23
  77.0 6.9 %collective-permute-done.4 = bf16[528,2048]{1,0:T(8,128)(2,1)} collective-permute-done((bf16[528,2048]{1,0:T(8,128)(2,1)}, bf16[528,2048]{1,0:T(8,128)(2,1)}, u32[]{:S(2)}, u32[]{:S(2)}) %collective-permute-start.4) | collective-permute-done | bytes 2162720 | tf_op jit(solution)/shard_map/ppermute | solution.py:23
  88.7 5.4 %collective-permute-start.7 = (bf16[384,512]{1,0:T(8,128)(2,1)S(1)}, bf16[384,512]{1,0:T(8,128)(2,1)S(1)}, u32[]{:S(2)}, u32[]{:S(2)}) collective-permute-start(bf16[384,512]{1,0:T(8,128)(2,1)S(1)} %fusion.5), channel_id=1, source_target_pairs={{0,7},{1,6},{2,5},{3,4},{4,11},{5,10},{6,9},{7,8},{8,15},{9,14},{1... | collective-permute-start | bytes 1179656 | tf_op jit(solution)/shard_map/ppermute | solution.py:23
  94.4 3.8 %collective-permute-start.8 = (bf16[384,512]{1,0:T(8,128)(2,1)S(1)}, bf16[384,512]{1,0:T(8,128)(2,1)S(1)}, u32[]{:S(2)}, u32[]{:S(2)}) collective-permute-start(bf16[384,512]{1,0:T(8,128)(2,1)S(1)} %fusion.6), channel_id=1, source_target_pairs={{0,31},{1,30},{2,29},{3,28},{4,3},{5,2},{6,1},{7,0},{8,7},{9,6},{1... | collective-permute-start | bytes 1179656 | tf_op jit(solution)/shard_map/ppermute | solution.py:23
  98.3 2.4 %collective-permute-start.5 = (bf16[192,512]{1,0:T(8,128)(2,1)S(1)}, bf16[192,512]{1,0:T(8,128)(2,1)S(1)}, u32[]{:S(2)}, u32[]{:S(2)}) collective-permute-start(bf16[192,512]{1,0:T(8,128)(2,1)S(1)} %get-tuple-element.11), channel_id=1, source_target_pairs={{0,8},{1,9},{2,10},{3,11},{4,12},{5,13},{6,14},{7,15},{8,16},{9,17... | collective-permute-start | bytes 589832 | tf_op jit(solution)/shard_map/ppermute | solution.py:23
  100.7 5.0 %collective-permute-start.6 = (bf16[192,512]{1,0:T(8,128)(2,1)S(1)}, bf16[192,512]{1,0:T(8,128)(2,1)S(1)}, u32[]{:S(2)}, u32[]{:S(2)}) collective-permute-start(bf16[192,512]{1,0:T(8,128)(2,1)S(1)} %get-tuple-element.12), channel_id=1, source_target_pairs={{0,24},{1,25},{2,26},{3,27},{4,28},{5,29},{6,30},{7,31},{8,0},{9,1... | collective-permute-start | bytes 589832 | tf_op jit(solution)/shard_map/ppermute | solution.py:23
  106.0 9.3 %collective-permute-done.5 = bf16[192,512]{1,0:T(8,128)(2,1)S(1)} collective-permute-done((bf16[192,512]{1,0:T(8,128)(2,1)S(1)}, bf16[192,512]{1,0:T(8,128)(2,1)S(1)}, u32[]{:S(2)}, u32[]{:S(2)}) %collective-permute-start.5) | collective-permute-done | bytes 196640 | tf_op jit(solution)/shard_map/ppermute | solution.py:23
  118.0 5.8 %collective-permute-start.10 = (bf16[384,128]{1,0:T(8,128)(2,1)S(1)}, bf16[384,128]{1,0:T(8,128)(2,1)S(1)}, u32[]{:S(2)}, u32[]{:S(2)}) collective-permute-start(bf16[384,128]{1,0:T(8,128)(2,1)S(1)} %get-tuple-element.10), channel_id=1, source_target_pairs={{0,16},{1,17},{2,18},{3,19},{4,20},{5,21},{6,22},{7,23},{8,24},{9,... | collective-permute-start | bytes 294920 | tf_op jit(solution)/shard_map/ppermute | solution.py:23
  123.8 3.5 %collective-permute-start.11 = (bf16[384,128]{1,0:T(8,128)(2,1)S(1)}, bf16[384,128]{1,0:T(8,128)(2,1)S(1)}, u32[]{:S(2)}, u32[]{:S(2)}) collective-permute-start(bf16[384,128]{1,0:T(8,128)(2,1)S(1)} %get-tuple-element.9), channel_id=1, source_target_pairs={{0,18},{1,19},{2,16},{3,17},{4,22},{5,23},{6,20},{7,21},{8,26},{9,... | collective-permute-start | bytes 294920 | tf_op jit(solution)/shard_map/ppermute | solution.py:23
  127.3 4.5 %collective-permute-start.9 = (bf16[384,128]{1,0:T(8,128)(2,1)S(1)}, bf16[384,128]{1,0:T(8,128)(2,1)S(1)}, u32[]{:S(2)}, u32[]{:S(2)}) collective-permute-start(bf16[384,128]{1,0:T(8,128)(2,1)S(1)} %get-tuple-element.8), channel_id=1, source_target_pairs={{0,2},{1,3},{2,0},{3,1},{4,6},{5,7},{6,4},{7,5},{8,10},{9,11},{10,... | collective-permute-start | bytes 294920 | tf_op jit(solution)/shard_map/ppermute | solution.py:23
  131.8 7.9 %collective-permute-start.15 = (bf16[512,256]{1,0:T(8,128)(2,1)S(1)}, bf16[512,256]{1,0:T(8,128)(2,1)S(1)}, u32[]{:S(2)}, u32[]{:S(2)}) collective-permute-start(bf16[512,256]{1,0:T(8,128)(2,1)S(1)} %convolution_convert_fusion.1), channel_id=1, source_target_pairs={{0,31},{1,30},{2,29},{3,28},{4,3},{5,2},{6,1},{7,0},{8,7},{9,6},{1... | collective-permute-start | bytes 786440 | tf_op jit(solution)/shard_map/ppermute | solution.py:23
  140.4 12.6 %all-to-all-start.1 = ((bf16[24,16,128]{2,1,0:T(8,128)(2,1)}), bf16[24,16,128]{2,1,0:T(8,128)(2,1)S(1)}, u32[]{:S(2)}, u32[]{:S(2)}) async-start(bf16[24,16,128]{2,1,0:T(8,128)(2,1)} %bitcast.23), calls=%async_computation.1 | async-start | bytes 196608 | tf_op jit(solution)/shard_map/all_to_all | solution.py:14
  155.0 9.0 %all-to-all-done.1 = bf16[24,16,128]{2,1,0:T(8,128)(2,1)S(1)} async-done(((bf16[24,16,128]{2,1,0:T(8,128)(2,1)}), bf16[24,16,128]{2,1,0:T(8,128)(2,1)S(1)}, u32[]{:S(2)}, u32[]{:S(2)}) %all-to-all-start.1) | async-done | bytes 98336 | tf_op jit(solution)/shard_map/all_to_all | solution.py:14
  164.0 7.1 %all-to-all-start.2 = ((bf16[8,64,256]{2,1,0:T(8,128)(2,1)}), bf16[8,64,256]{2,1,0:T(8,128)(2,1)S(1)}, u32[]{:S(2)}, u32[]{:S(2)}) async-start(bf16[8,64,256]{2,1,0:T(8,128)(2,1)} %bitcast.26), calls=%async_computation.2 | async-start | bytes 524288 | tf_op jit(solution)/shard_map/all_to_all | solution.py:14
  171.6 3.4 %collective-permute-start.12 = (bf16[64,256]{1,0:T(8,128)(2,1)S(1)}, bf16[64,256]{1,0:T(8,128)(2,1)S(1)}, u32[]{:S(2)}, u32[]{:S(2)}) collective-permute-start(bf16[64,256]{1,0:T(8,128)(2,1)S(1)} %dynamic-slice_convert_fusion), channel_id=1, source_target_pairs={{0,1},{1,0},{2,3},{3,2},{4,5},{5,4},{6,7},{7,6},{8,9},{9,8},{10,11... | collective-permute-start | bytes 98312 | tf_op jit(solution)/shard_map/ppermute | solution.py:23
  175.0 6.2 %all-to-all-done.2 = bf16[8,64,256]{2,1,0:T(8,128)(2,1)S(1)} async-done(((bf16[8,64,256]{2,1,0:T(8,128)(2,1)}), bf16[8,64,256]{2,1,0:T(8,128)(2,1)S(1)}, u32[]{:S(2)}, u32[]{:S(2)}) %all-to-all-start.2) | async-done | bytes 262176 | tf_op jit(solution)/shard_map/all_to_all | solution.py:14
  (108 shorter events, 35.1 us)
Async XLA Ops:
  0.0 36.4 %copy-start = (bf16[2048,32]{0,1:T(8,128)(2,1)S(1)}, bf16[2048,32]{0,1:T(8,128)(2,1)}, u32[]{:S(2)}) copy-start(bf16[2048,32]{0,1:T(8,128)(2,1)} %param.18) | copy-start | bytes 393220
  6.5 37.2 %all-to-all-start = ((bf16[24,16,512]{2,1,0:T(8,128)(2,1)}), bf16[24,16,512]{2,1,0:T(8,128)(2,1)S(1)}, u32[]{:S(2)}, u32[]{:S(2)}) async-start(bf16[24,16,512]{2,1,0:T(8,128)(2,1)} %bitcast.6), calls=%async_computation | async-start | bytes 786432 | tf_op jit(solution)/shard_map/all_to_all | solution.py:14
  33.2 50.6 %collective-permute-start.4 = (bf16[528,2048]{1,0:T(8,128)(2,1)}, bf16[528,2048]{1,0:T(8,128)(2,1)}, u32[]{:S(2)}, u32[]{:S(2)}) collective-permute-start(bf16[528,2048]{1,0:T(8,128)(2,1)} %pad_maximum_fusion), channel_id=1, source_target_pairs={{0,1},{1,0},{2,3},{3,2},{4,5},{5,4},{6,7},{7,6},{8,9},{9,8},{10,11... | collective-permute-start | bytes 6488072 | tf_op jit(solution)/shard_map/ppermute | solution.py:23
  37.6 115.4 %collective-permute-start.13 = (bf16[512,256]{1,0:T(8,128)(2,1)S(1)}, bf16[512,256]{1,0:T(8,128)(2,1)}, u32[]{:S(2)}, u32[]{:S(2)}) collective-permute-start(bf16[512,256]{1,0:T(8,128)(2,1)S(1)} %convolution_convert_fusion.3), channel_id=1, source_target_pairs={{0,7},{1,6},{2,5},{3,4},{4,11},{5,10},{6,9},{7,8},{8,15},{9,14},{1... | collective-permute-start | bytes 786440 | tf_op jit(solution)/shard_map/ppermute | solution.py:23
  43.7 23.1 %collective-permute-start.3 = (bf16[384,512]{1,0:T(8,128)(2,1)S(1)}, bf16[384,512]{1,0:T(8,128)(2,1)S(1)}, u32[]{:S(2)}, u32[]{:S(2)}) collective-permute-start(bf16[384,512]{1,0:T(8,128)(2,1)S(1)} %bitcast.86), channel_id=1, source_target_pairs={{0,31},{1,30},{2,29},{3,28},{4,3},{5,2},{6,1},{7,0},{8,7},{9,6},{1... | collective-permute-start | bytes 1179656 | tf_op jit(solution)/shard_map/ppermute | solution.py:23
  49.1 12.3 %collective-permute-start.1 = (bf16[192,512]{1,0:T(8,128)(2,1)S(1)}, bf16[192,512]{1,0:T(8,128)(2,1)S(1)}, u32[]{:S(2)}, u32[]{:S(2)}) collective-permute-start(bf16[192,512]{1,0:T(8,128)(2,1)S(1)} %bitcast.105), channel_id=1, source_target_pairs={{0,8},{1,9},{2,10},{3,11},{4,12},{5,13},{6,14},{7,15},{8,16},{9,17... | collective-permute-start | bytes 589832 | tf_op jit(solution)/shard_map/ppermute | solution.py:23
  51.1 15.7 %collective-permute-start.2 = (bf16[192,512]{1,0:T(8,128)(2,1)S(1)}, bf16[192,512]{1,0:T(8,128)(2,1)S(1)}, u32[]{:S(2)}, u32[]{:S(2)}) collective-permute-start(bf16[192,512]{1,0:T(8,128)(2,1)S(1)} %bitcast.104), channel_id=1, source_target_pairs={{0,24},{1,25},{2,26},{3,27},{4,28},{5,29},{6,30},{7,31},{8,0},{9,1... | collective-permute-start | bytes 589832 | tf_op jit(solution)/shard_map/ppermute | solution.py:23
  61.4 13.4 %collective-permute-start = (bf16[384,512]{1,0:T(8,128)(2,1)S(1)}, bf16[384,512]{1,0:T(8,128)(2,1)S(1)}, u32[]{:S(2)}, u32[]{:S(2)}) collective-permute-start(bf16[384,512]{1,0:T(8,128)(2,1)S(1)} %bitcast.89), channel_id=1, source_target_pairs={{0,7},{1,6},{2,5},{3,4},{4,11},{5,10},{6,9},{7,8},{8,15},{9,14},{1... | collective-permute-start | bytes 1179656 | tf_op jit(solution)/shard_map/ppermute | solution.py:23
  88.7 28.8 %collective-permute-start.7 = (bf16[384,512]{1,0:T(8,128)(2,1)S(1)}, bf16[384,512]{1,0:T(8,128)(2,1)S(1)}, u32[]{:S(2)}, u32[]{:S(2)}) collective-permute-start(bf16[384,512]{1,0:T(8,128)(2,1)S(1)} %fusion.5), channel_id=1, source_target_pairs={{0,7},{1,6},{2,5},{3,4},{4,11},{5,10},{6,9},{7,8},{8,15},{9,14},{1... | collective-permute-start | bytes 1179656 | tf_op jit(solution)/shard_map/ppermute | solution.py:23
  94.4 23.1 %collective-permute-start.8 = (bf16[384,512]{1,0:T(8,128)(2,1)S(1)}, bf16[384,512]{1,0:T(8,128)(2,1)S(1)}, u32[]{:S(2)}, u32[]{:S(2)}) collective-permute-start(bf16[384,512]{1,0:T(8,128)(2,1)S(1)} %fusion.6), channel_id=1, source_target_pairs={{0,31},{1,30},{2,29},{3,28},{4,3},{5,2},{6,1},{7,0},{8,7},{9,6},{1... | collective-permute-start | bytes 1179656 | tf_op jit(solution)/shard_map/ppermute | solution.py:23
  98.3 17.0 %collective-permute-start.5 = (bf16[192,512]{1,0:T(8,128)(2,1)S(1)}, bf16[192,512]{1,0:T(8,128)(2,1)S(1)}, u32[]{:S(2)}, u32[]{:S(2)}) collective-permute-start(bf16[192,512]{1,0:T(8,128)(2,1)S(1)} %get-tuple-element.11), channel_id=1, source_target_pairs={{0,8},{1,9},{2,10},{3,11},{4,12},{5,13},{6,14},{7,15},{8,16},{9,17... | collective-permute-start | bytes 589832 | tf_op jit(solution)/shard_map/ppermute | solution.py:23
  100.7 31.1 %copy-start.10 = (f32[256,2]{0,1:T(2,128)S(1)}, f32[256,2]{0,1:T(2,128)}, u32[]{:S(2)}) copy-start(f32[256,2]{0,1:T(2,128)} %param.14) | copy-start | bytes 6148
  100.7 16.8 %collective-permute-start.6 = (bf16[192,512]{1,0:T(8,128)(2,1)S(1)}, bf16[192,512]{1,0:T(8,128)(2,1)S(1)}, u32[]{:S(2)}, u32[]{:S(2)}) collective-permute-start(bf16[192,512]{1,0:T(8,128)(2,1)S(1)} %get-tuple-element.12), channel_id=1, source_target_pairs={{0,24},{1,25},{2,26},{3,27},{4,28},{5,29},{6,30},{7,31},{8,0},{9,1... | collective-permute-start | bytes 589832 | tf_op jit(solution)/shard_map/ppermute | solution.py:23
  106.0 47.0 %copy-start.11 = (f32[64]{0:T(128)S(1)}, f32[64]{0:T(128)}, u32[]{:S(2)}) copy-start(f32[64]{0:T(128)} %param.21) | copy-start | bytes 772
  106.0 65.1 %copy-start.9 = (s32[1,256]{1,0:T(1,128)S(1)}, s32[1,256]{1,0:T(1,128)}, u32[]{:S(2)}) copy-start(s32[1,256]{1,0:T(1,128)} %copy-done.8) | copy-start | bytes 3076
  115.3 37.8 %collective-permute-start.14 = (bf16[512,256]{1,0:T(8,128)(2,1)S(1)}, bf16[512,256]{1,0:T(8,128)(2,1)S(1)}, u32[]{:S(2)}, u32[]{:S(2)}) collective-permute-start(bf16[512,256]{1,0:T(8,128)(2,1)S(1)} %copy-done.3), channel_id=1, source_target_pairs={{0,8},{1,9},{2,10},{3,11},{4,12},{5,13},{6,14},{7,15},{8,16},{9,17... | collective-permute-start | bytes 786440 | tf_op jit(solution)/shard_map/ppermute | solution.py:23
  117.9 53.5 %copy-start.7 = (s32[1,256]{1,0:T(1,128)S(1)}, s32[1,256]{1,0:T(1,128)}, u32[]{:S(2)}) copy-start(s32[1,256]{1,0:T(1,128)} %copy-done.6) | copy-start | bytes 3076
  118.0 13.8 %collective-permute-start.10 = (bf16[384,128]{1,0:T(8,128)(2,1)S(1)}, bf16[384,128]{1,0:T(8,128)(2,1)S(1)}, u32[]{:S(2)}, u32[]{:S(2)}) collective-permute-start(bf16[384,128]{1,0:T(8,128)(2,1)S(1)} %get-tuple-element.10), channel_id=1, source_target_pairs={{0,16},{1,17},{2,18},{3,19},{4,20},{5,21},{6,22},{7,23},{8,24},{9,... | collective-permute-start | bytes 294920 | tf_op jit(solution)/shard_map/ppermute | solution.py:23
  123.8 15.9 %collective-permute-start.11 = (bf16[384,128]{1,0:T(8,128)(2,1)S(1)}, bf16[384,128]{1,0:T(8,128)(2,1)S(1)}, u32[]{:S(2)}, u32[]{:S(2)}) collective-permute-start(bf16[384,128]{1,0:T(8,128)(2,1)S(1)} %get-tuple-element.9), channel_id=1, source_target_pairs={{0,18},{1,19},{2,16},{3,17},{4,22},{5,23},{6,20},{7,21},{8,26},{9,... | collective-permute-start | bytes 294920 | tf_op jit(solution)/shard_map/ppermute | solution.py:23
  127.3 12.4 %collective-permute-start.9 = (bf16[384,128]{1,0:T(8,128)(2,1)S(1)}, bf16[384,128]{1,0:T(8,128)(2,1)S(1)}, u32[]{:S(2)}, u32[]{:S(2)}) collective-permute-start(bf16[384,128]{1,0:T(8,128)(2,1)S(1)} %get-tuple-element.8), channel_id=1, source_target_pairs={{0,2},{1,3},{2,0},{3,1},{4,6},{5,7},{6,4},{7,5},{8,10},{9,11},{10,... | collective-permute-start | bytes 294920 | tf_op jit(solution)/shard_map/ppermute | solution.py:23
  131.8 21.3 %collective-permute-start.15 = (bf16[512,256]{1,0:T(8,128)(2,1)S(1)}, bf16[512,256]{1,0:T(8,128)(2,1)S(1)}, u32[]{:S(2)}, u32[]{:S(2)}) collective-permute-start(bf16[512,256]{1,0:T(8,128)(2,1)S(1)} %convolution_convert_fusion.1), channel_id=1, source_target_pairs={{0,31},{1,30},{2,29},{3,28},{4,3},{5,2},{6,1},{7,0},{8,7},{9,6},{1... | collective-permute-start | bytes 786440 | tf_op jit(solution)/shard_map/ppermute | solution.py:23
  140.4 23.6 %all-to-all-start.1 = ((bf16[24,16,128]{2,1,0:T(8,128)(2,1)}), bf16[24,16,128]{2,1,0:T(8,128)(2,1)S(1)}, u32[]{:S(2)}, u32[]{:S(2)}) async-start(bf16[24,16,128]{2,1,0:T(8,128)(2,1)} %bitcast.23), calls=%async_computation.1 | async-start | bytes 196608 | tf_op jit(solution)/shard_map/all_to_all | solution.py:14
  164.0 17.2 %all-to-all-start.2 = ((bf16[8,64,256]{2,1,0:T(8,128)(2,1)}), bf16[8,64,256]{2,1,0:T(8,128)(2,1)S(1)}, u32[]{:S(2)}, u32[]{:S(2)}) async-start(bf16[8,64,256]{2,1,0:T(8,128)(2,1)} %bitcast.26), calls=%async_computation.2 | async-start | bytes 524288 | tf_op jit(solution)/shard_map/all_to_all | solution.py:14
  171.6 9.6 %collective-permute-start.12 = (bf16[64,256]{1,0:T(8,128)(2,1)S(1)}, bf16[64,256]{1,0:T(8,128)(2,1)S(1)}, u32[]{:S(2)}, u32[]{:S(2)}) collective-permute-start(bf16[64,256]{1,0:T(8,128)(2,1)S(1)} %dynamic-slice_convert_fusion), channel_id=1, source_target_pairs={{0,1},{1,0},{2,3},{3,2},{4,5},{5,4},{6,7},{7,6},{8,9},{9,8},{10,11... | collective-permute-start | bytes 98312 | tf_op jit(solution)/shard_map/ppermute | solution.py:23
  (7 other events, 94.0 us)
where the time goes:
time: 185 us; the launch traced here: 182 us
  starting transfers between devices  102 us (55%)
  waiting for transfers between devices  46.8 us (25%)
  matrix products  13.1 us (7%)
  other arithmetic  9.46 us (5%)
  local copies, waits for them, and re-layouts  9.28 us (5%)
    ppermute x16, starting transfers between devices, send(): return lax.ppermute(value, TP, pairs)  66 us
    all_to_all x3, starting transfers between devices, exchange(): return lax.all_to_all(blocks, axes, split_axis=0, concat_axis=0, tiled=True)  36.4 us
    ppermute x16, waiting for transfers between devices, send(): return lax.ppermute(value, TP, pairs)  31.6 us
    all_to_all x3, waiting for transfers between devices, exchange(): return lax.all_to_all(blocks, axes, split_axis=0, concat_axis=0, tiled=True)  15.2 us
    dot_general x34, matrix products, dot(): lax.dot_general(left, right, (((left_dim,), (right_dim,)), ((), ())), pre...  13.1 us
    unnamed x39, local copies, waits for them, and re-layouts  6.43 us
  transfers between devices with their start and end apart: 19, of which 7 were waited for; matrix products, arithmetic and copies ran while one was open for 14% of the time, Pallas kernels for 0%

commit v1 on v0

v1 whole, which is shorter than its diff:
```python
import jax
import jax.numpy as jnp
from jax import lax
from jax.sharding import Mesh
from jax.sharding import PartitionSpec as P

TP = ("ya", "yb", "yc", "xh", "xl")
FAR, NEAR = 8, 4

EPSILON = 1e-06


def exchange(blocks, axes):
    return lax.all_to_all(blocks, axes, split_axis=0, concat_axis=0, tiled=True)


def send(value, target):
    pairs = []
    for y in range(FAR):
        for x in range(NEAR):
            there_y, there_x = target(y, x)
            pairs.append((y * NEAR + x, there_y % FAR * NEAR + there_x % NEAR))
    return lax.ppermute(value, TP, pairs)


def along_y(steps):
    return lambda y, x: (y + steps, x)


def dot(left, right, left_dim, right_dim):
    return lax.dot_general(
        left, right, (((left_dim,), (right_dim,)), ((), ())), preferred_element_type=jnp.float32
    )


def slots_of(ids, experts):
    tokens = ids.shape[1]
    named = ids[:, None, :] == jnp.arange(experts, dtype=jnp.int32)[None, :, None]
    count = (named[0] | named[1]).astype(jnp.bfloat16)
    before = lax.broadcasted_iota(jnp.int32, (tokens, tokens), 0) < lax.broadcasted_iota(
        jnp.int32, (tokens, tokens), 1
    )
    earlier = dot(count, before.astype(jnp.bfloat16), 1, 0).astype(jnp.int32)
    return jnp.sum(jnp.where(named, earlier[None], 0), axis=1)


def silu_times(gate_act, up_act):
    return (jax.nn.silu(gate_act) * up_act).astype(jnp.bfloat16)


def total_of(terms):
    return sum(term.astype(jnp.float32) for term in terms).astype(jnp.bfloat16)


def columns(weight, starts, size):
    return jnp.concatenate(
        [lax.dynamic_slice_in_dim(weight, start, size, 1) for start in starts], axis=1
    )


def local(
    tokens,
    norm_gain,
    expert_ids,
    routing_weight,
    expert_gate,
    expert_up,
    expert_down,
    dense_gate_w,
    dense_up_w,
    dense_down_w,
    dense_gate,
):
    experts = lax.axis_size("ep")
    group_tokens, model_width = tokens.shape
    capacity = 3 * group_tokens // experts
    few = capacity // 2
    rows_mine = experts * few
    part = model_width // (FAR * NEAR)
    wide = model_width // 4
    row_width = model_width // FAR
    hidden_part = expert_gate.shape[2]
    odd_y, odd_x = lax.axis_index("yc"), lax.axis_index("xl")
    mod_y = lax.axis_index("yb") * 2 + odd_y

    own_w = [expert_gate[0].T, expert_up[0].T, expert_down[0]]
    swapped = send(jnp.concatenate(own_w, axis=0), lambda y, x: (y, x ^ 1))
    other_w = [swapped[i * hidden_part : (i + 1) * hidden_part] for i in range(3)]

    values = tokens.astype(jnp.float32)
    factor = lax.rsqrt(jnp.mean(values * values, axis=-1, keepdims=True) + EPSILON)
    normed = (values * factor * norm_gain[None, :]).astype(jnp.bfloat16)
    ids = expert_ids.T
    shifted = slots_of(ids, experts) - odd_x * few
    places = jnp.where((shifted >= 0) & (shifted < few), ids * few + shifted, -1)
    slot_no = lax.broadcasted_iota(jnp.int32, (rows_mine, group_tokens), 0)
    chosen = [(places[c][None, :] == slot_no).astype(jnp.bfloat16) for c in range(2)]

    def side(weight, other):
        return lax.dynamic_slice_in_dim(weight, (odd_y ^ other) * 2 * wide, 2 * wide, 1)

    outgoing = dot(chosen[0] + chosen[1], side(normed, 0), 1, 0).astype(jnp.bfloat16)
    landed = exchange(outgoing.reshape(experts, few, 2 * wide), "ep")
    landed = landed.reshape(rows_mine, 2 * wide)

    dense_hidden = silu_times(dot(normed, dense_gate_w, 1, 0), dot(normed, dense_up_w, 1, 0))

    def dense_part(step):
        first = (mod_y + step) % 4 * row_width
        down = columns(dense_down_w, [first, first + 4 * row_width], row_width)
        return dot(down, dense_hidden, 0, 1).astype(jnp.bfloat16)

    dense_terms = [
        send(dense_part(1), along_y(1)),
        send(dense_part(2), along_y(2)),
        send(dense_part(3), along_y(-1)),
    ]
    dense_sum = total_of([dense_part(0), *dense_terms])
    dense_pieces = exchange(dense_sum.reshape(8, part, group_tokens), ("ya", "xh", "xl"))
    dense_out = dense_pieces.astype(jnp.float32).sum(axis=0)

    block = rows_mine // 2
    arrived = [send(landed[:block], along_y(1)), send(landed[block:], along_y(-1))]

    def hidden_of(weights):
        halves = []
        for i in range(2):
            rows = [landed[i * block : (i + 1) * block], arrived[i]]
            gate_act = sum(dot(r, side(weights[0], k), 1, 1) for k, r in enumerate(rows))
            up_act = sum(dot(r, side(weights[1], k), 1, 1) for k, r in enumerate(rows))
            halves.append(silu_times(gate_act, up_act))
        return jnp.concatenate(halves, axis=0)

    own_hidden = hidden_of(own_w)
    other_hidden = hidden_of(other_w)
    partial = dot(own_w[2], own_hidden, 0, 1) + dot(other_w[2], other_hidden, 0, 1)
    partial = partial.astype(jnp.bfloat16).reshape(4, 2, 2, 2 * part, rows_mine)
    partial = partial.transpose(1, 2, 0, 3, 4).reshape(4, wide, rows_mine)
    near_terms = exchange(partial, ("yc", "xh"))
    near_sum = total_of([near_terms[k] for k in range(4)])
    returned = exchange(near_sum.T.reshape(experts, few, wide), "ep")
    returned = returned.reshape(rows_mine, wide)
    weight = routing_weight.T
    routed = sum(weight[c][None, :] * dot(returned, chosen[c], 0, 0) for c in range(2))
    pieces = exchange(
        routed.astype(jnp.bfloat16).reshape(8, part, group_tokens), ("ya", "yb", "xl")
    )
    routed = pieces.astype(jnp.float32).sum(axis=0)
    gate_factor = jax.nn.sigmoid(dense_gate)[:, None]
    return (routed + gate_factor * dense_out).astype(jnp.bfloat16).T


def solution(mesh):
    finer = Mesh(mesh.devices.reshape(mesh.shape["ep"], 2, 2, 2, 2, 2), ("ep", *TP))
    in_specs = (
        P("ep", None),
        P(),
        P("ep", None),
        P("ep", None),
        P("ep", None, TP),
        P("ep", None, TP),
        P("ep", TP, None),
        P(None, TP),
        P(None, TP),
        P(TP, None),
        P(TP),
    )
    out_specs = P("ep", TP)
    return jax.shard_map(local, mesh=finer, in_specs=in_specs, out_specs=out_specs, check_vma=False)
```

time: 185 us -> 186 us (level)
  the two profiles are of different devices: /device:TPU:1 before, /device:TPU:10 now
where the time goes in v1:
time: 186 us; the launch traced here: 185 us
  waiting for transfers between devices  86.5 us (47%)
  starting transfers between devices  69.4 us (37%)
  matrix products  13.5 us (7%)
  local copies, waits for them, and re-layouts  10.1 us (5%)
  other arithmetic  4.84 us (3%)
    ppermute x6, waiting for transfers between devices, send(): return lax.ppermute(value, TP, pairs)  49.9 us
    all_to_all x5, starting transfers between devices, exchange(): return lax.all_to_all(blocks, axes, split_axis=0, concat_axis=0, tiled=True)  48.3 us
    all_to_all x5, waiting for transfers between devices, exchange(): return lax.all_to_all(blocks, axes, split_axis=0, concat_axis=0, tiled=True)  36.6 us
    ppermute x6, starting transfers between devices, send(): return lax.ppermute(value, TP, pairs)  21.2 us
    dot_general x28, matrix products, dot(): lax.dot_general(left, right, (((left_dim,), (right_dim,)), ((), ())), pre...  13.5 us
    reshape x2, local copies, waits for them, and re-layouts, local(): partial = partial.astype(jnp.bfloat16).reshape(4, 2, 2, 2 * part, rows_mine)  6.46 us
  transfers between devices with their start and end apart: 11, of which 8 were waited for; matrix products, arithmetic and copies ran while one was open for 5% of the time, Pallas kernels for 0%

profile of v1, /device:TPU:10, one launch (start us, length us, event | category | flops | bytes accessed | tf_op | source)
XLA Modules:
  0.0 184.9 jit_solution(13256086113456708212)
XLA Ops:
  0.0 3.2 %pad_maximum_fusion = bf16[528,2048]{1,0:T(8,128)(2,1)} fusion(bf16[176,2048]{1,0:T(8,128)(2,1)} %bitcast.99, bf16[176,2048]{1,0:T(8,128)(2,1)} %bitcast.98, bf16[176,2048]{1,0:T(8,128)(2,1)} %bitcast.87), kind=kLoop, calls=%fused_computation.4 | loop fusion | flops 6488064 | bytes 4325376 | tf_op jit(solution)/shard_map/concatenate | solution.py:87
  3.2 2.4 %collective-permute-start.2 = (bf16[528,2048]{1,0:T(8,128)(2,1)}, bf16[528,2048]{1,0:T(8,128)(2,1)}, u32[]{:S(2)}, u32[]{:S(2)}) collective-permute-start(bf16[528,2048]{1,0:T(8,128)(2,1)} %pad_maximum_fusion), channel_id=1, source_target_pairs={{0,1},{1,0},{2,3},{3,2},{4,5},{5,4},{6,7},{7,6},{8,9},{9,8},{10,11... | collective-permute-start | bytes 6488072 | tf_op jit(solution)/shard_map/ppermute | solution.py:23
  7.8 15.4 %all-to-all-start = ((bf16[24,16,1024]{2,1,0:T(8,128)(2,1)}), bf16[24,16,1024]{2,1,0:T(8,128)(2,1)S(1)}, u32[]{:S(2)}, u32[]{:S(2)}) async-start(bf16[24,16,1024]{2,1,0:T(8,128)(2,1)} %bitcast.6), calls=%async_computation | async-start | bytes 1572864 | tf_op jit(solution)/shard_map/all_to_all | solution.py:14
  23.2 31.0 %collective-permute-done.2 = bf16[528,2048]{1,0:T(8,128)(2,1)} collective-permute-done((bf16[528,2048]{1,0:T(8,128)(2,1)}, bf16[528,2048]{1,0:T(8,128)(2,1)}, u32[]{:S(2)}, u32[]{:S(2)}) %collective-permute-start.2) | collective-permute-done | bytes 2162720 | tf_op jit(solution)/shard_map/ppermute | solution.py:23
  54.2 2.3 %fusion.109 = (bf16[176,2048]{1,0:T(8,128)(2,1)}, bf16[176,2048]{1,0:T(8,128)(2,1)S(1)}) fusion(bf16[528,2048]{1,0:T(8,128)(2,1)} %collective-permute-done.2), kind=kLoop, calls=%fused_computation.145 | loop fusion | bytes 2883584 | tf_op jit(solution)/shard_map/slice | solution.py:88
  56.6 3.6 %collective-permute-start = (bf16[192,1024]{1,0:T(8,128)(2,1)S(1)}, bf16[192,1024]{1,0:T(8,128)(2,1)S(1)}, u32[]{:S(2)}, u32[]{:S(2)}) collective-permute-start(bf16[192,1024]{1,0:T(8,128)(2,1)S(1)} %bitcast.93), channel_id=1, source_target_pairs={{0,4},{1,5},{2,6},{3,7},{4,8},{5,9},{6,10},{7,11},{8,12},{9,13},{1... | collective-permute-start | bytes 1179656 | tf_op jit(solution)/shard_map/ppermute | solution.py:23
  60.8 2.4 %collective-permute-start.1 = (bf16[192,1024]{1,0:T(8,128)(2,1)S(1)}, bf16[192,1024]{1,0:T(8,128)(2,1)S(1)}, u32[]{:S(2)}, u32[]{:S(2)}) collective-permute-start(bf16[192,1024]{1,0:T(8,128)(2,1)S(1)} %bitcast.88), channel_id=1, source_target_pairs={{0,28},{1,29},{2,30},{3,31},{4,0},{5,1},{6,2},{7,3},{8,4},{9,5},{1... | collective-permute-start | bytes 1179656 | tf_op jit(solution)/shard_map/ppermute | solution.py:23
  63.8 4.9 %collective-permute-done = bf16[192,1024]{1,0:T(8,128)(2,1)S(1)} collective-permute-done((bf16[192,1024]{1,0:T(8,128)(2,1)S(1)}, bf16[192,1024]{1,0:T(8,128)(2,1)S(1)}, u32[]{:S(2)}, u32[]{:S(2)}) %collective-permute-start) | collective-permute-done | bytes 393248 | tf_op jit(solution)/shard_map/ppermute | solution.py:23
  69.2 3.2 %collective-permute-done.1 = bf16[192,1024]{1,0:T(8,128)(2,1)S(1)} collective-permute-done((bf16[192,1024]{1,0:T(8,128)(2,1)S(1)}, bf16[192,1024]{1,0:T(8,128)(2,1)S(1)}, u32[]{:S(2)}, u32[]{:S(2)}) %collective-permute-start.1) | collective-permute-done | bytes 393248 | tf_op jit(solution)/shard_map/ppermute | solution.py:23
  76.3 3.0 %fusion = bf16[2048,384]{0,1:T(8,128)(2,1)} fusion(f32[384,2048]{1,0:T(8,128)S(1)} %fusion.56, bf16[528,2048]{1,0:T(8,128)(2,1)} %collective-permute-done.2, bf16[192,176]{0,1:T(8,128)(2,1)S(1)} %multiply_convert_fusion, bf16[192,176]{0,1:T(8,128)(2,1)S(1)} %multiply_convert_fusion.1), kind=kOutput, calls=%fused_computation.1 | convolution fusion | flops 278667264 | bytes 5574656 | tf_op jit(solution)/shard_map/dot_general | solution.py:31
  79.2 2.8 %reshape.62 = bf16[4,2,2,128,384]{3,2,1,0,4:T(2,128)(2,1)S(1)} reshape(bf16[2048,384]{0,1:T(8,128)(2,1)} %fusion) | data formatting | bytes 3145728 | tf_op jit(solution)/shard_map/reshape | solution.py:137
  82.1 3.6 %copy.17 = bf16[4,2,2,128,384]{4,3,0,2,1:T(8,128)(2,1)} copy(bf16[4,2,2,128,384]{3,2,1,0,4:T(2,128)(2,1)S(1)} %reshape.62) | data formatting | bytes 3145728 | tf_op jit(solution)/shard_map/reshape | solution.py:137
  85.7 5.0 %all-to-all-start.1 = ((bf16[4,512,384]{2,1,0:T(8,128)(2,1)}), bf16[4,512,384]{2,1,0:T(8,128)(2,1)S(1)}, u32[]{:S(2)}, u32[]{:S(2)}) async-start(bf16[4,512,384]{2,1,0:T(8,128)(2,1)} %bitcast.20), calls=%async_computation.1 | async-start | bytes 3145728 | tf_op jit(solution)/shard_map/all_to_all | solution.py:14
  91.6 17.2 %all-to-all-done.1 = bf16[4,512,384]{2,1,0:T(8,128)(2,1)S(1)} async-done(((bf16[4,512,384]{2,1,0:T(8,128)(2,1)}), bf16[4,512,384]{2,1,0:T(8,128)(2,1)S(1)}, u32[]{:S(2)}, u32[]{:S(2)}) %all-to-all-start.1) | async-done | bytes 1572896 | tf_op jit(solution)/shard_map/all_to_all | solution.py:14
  110.0 15.4 %all-to-all-start.2 = ((bf16[24,16,512]{2,1,0:T(8,128)(2,1)}), bf16[24,16,512]{2,1,0:T(8,128)(2,1)S(1)}, u32[]{:S(2)}, u32[]{:S(2)}) async-start(bf16[24,16,512]{2,1,0:T(8,128)(2,1)} %bitcast.23), calls=%async_computation.2 | async-start | bytes 786432 | tf_op jit(solution)/shard_map/all_to_all | solution.py:14
  125.7 6.0 %collective-permute-start.3 = (bf16[512,256]{1,0:T(8,128)(2,1)S(1)}, bf16[512,256]{1,0:T(8,128)(2,1)S(1)}, u32[]{:S(2)}, u32[]{:S(2)}) collective-permute-start(bf16[512,256]{1,0:T(8,128)(2,1)S(1)} %convolution_convert_fusion.3), channel_id=1, source_target_pairs={{0,4},{1,5},{2,6},{3,7},{4,8},{5,9},{6,10},{7,11},{8,12},{9,13},{1... | collective-permute-start | bytes 786440 | tf_op jit(solution)/shard_map/ppermute | solution.py:23
  131.9 2.8 %collective-permute-start.4 = (bf16[512,256]{1,0:T(8,128)(2,1)S(1)}, bf16[512,256]{1,0:T(8,128)(2,1)S(1)}, u32[]{:S(2)}, u32[]{:S(2)}) collective-permute-start(bf16[512,256]{1,0:T(8,128)(2,1)S(1)} %convolution_convert_fusion.2), channel_id=1, source_target_pairs={{0,8},{1,9},{2,10},{3,11},{4,12},{5,13},{6,14},{7,15},{8,16},{9,17... | collective-permute-start | bytes 786440 | tf_op jit(solution)/shard_map/ppermute | solution.py:23
  135.0 3.9 %collective-permute-start.5 = (bf16[512,256]{1,0:T(8,128)(2,1)S(1)}, bf16[512,256]{1,0:T(8,128)(2,1)S(1)}, u32[]{:S(2)}, u32[]{:S(2)}) collective-permute-start(bf16[512,256]{1,0:T(8,128)(2,1)S(1)} %convolution_convert_fusion.1), channel_id=1, source_target_pairs={{0,28},{1,29},{2,30},{3,31},{4,0},{5,1},{6,2},{7,3},{8,4},{9,5},{1... | collective-permute-start | bytes 786440 | tf_op jit(solution)/shard_map/ppermute | solution.py:23
  139.0 2.6 %collective-permute-done.3 = bf16[512,256]{1,0:T(8,128)(2,1)S(1)} collective-permute-done((bf16[512,256]{1,0:T(8,128)(2,1)S(1)}, bf16[512,256]{1,0:T(8,128)(2,1)S(1)}, u32[]{:S(2)}, u32[]{:S(2)}) %collective-permute-start.3) | collective-permute-done | bytes 262176 | tf_op jit(solution)/shard_map/ppermute | solution.py:23
  141.5 8.2 %collective-permute-done.4 = bf16[512,256]{1,0:T(8,128)(2,1)S(1)} collective-permute-done((bf16[512,256]{1,0:T(8,128)(2,1)S(1)}, bf16[512,256]{1,0:T(8,128)(2,1)S(1)}, u32[]{:S(2)}, u32[]{:S(2)}) %collective-permute-start.4) | collective-permute-done | bytes 262176 | tf_op jit(solution)/shard_map/ppermute | solution.py:23
  150.8 7.1 %all-to-all-start.4 = ((bf16[8,64,256]{2,1,0:T(8,128)(2,1)}), bf16[8,64,256]{2,1,0:T(8,128)(2,1)S(1)}, u32[]{:S(2)}, u32[]{:S(2)}) async-start(bf16[8,64,256]{2,1,0:T(8,128)(2,1)} %bitcast.27), calls=%async_computation.4 | async-start | bytes 524288 | tf_op jit(solution)/shard_map/all_to_all | solution.py:14
  159.3 9.7 %all-to-all-done.4 = bf16[8,64,256]{2,1,0:T(8,128)(2,1)S(1)} async-done(((bf16[8,64,256]{2,1,0:T(8,128)(2,1)}), bf16[8,64,256]{2,1,0:T(8,128)(2,1)S(1)}, u32[]{:S(2)}, u32[]{:S(2)}) %all-to-all-start.4) | async-done | bytes 262176 | tf_op jit(solution)/shard_map/all_to_all | solution.py:14
  169.0 5.4 %all-to-all-start.3 = ((bf16[8,64,256]{2,1,0:T(8,128)(2,1)}), bf16[8,64,256]{2,1,0:T(8,128)(2,1)S(1)}, u32[]{:S(2)}, u32[]{:S(2)}) async-start(bf16[8,64,256]{2,1,0:T(8,128)(2,1)} %bitcast.26), calls=%async_computation.3 | async-start | bytes 524288 | tf_op jit(solution)/shard_map/all_to_all | solution.py:14
  174.4 9.7 %all-to-all-done.3 = bf16[8,64,256]{2,1,0:T(8,128)(2,1)S(1)} async-done(((bf16[8,64,256]{2,1,0:T(8,128)(2,1)}), bf16[8,64,256]{2,1,0:T(8,128)(2,1)S(1)}, u32[]{:S(2)}, u32[]{:S(2)}) %all-to-all-start.3) | async-done | bytes 262176 | tf_op jit(solution)/shard_map/all_to_all | solution.py:14
  (70 shorter events, 13.5 us)
Async XLA Ops:
  0.0 90.7 %copy-start = (bf16[2048,32]{0,1:T(8,128)(2,1)S(1)}, bf16[2048,32]{0,1:T(8,128)(2,1)}, u32[]{:S(2)}) copy-start(bf16[2048,32]{0,1:T(8,128)(2,1)} %param.18) | copy-start | bytes 393220
  0.0 5.7 %copy-start.2 = (bf16[256,2048]{1,0:T(8,128)(2,1)S(1)}, bf16[256,2048]{1,0:T(8,128)(2,1)}, u32[]{:S(2)}) copy-start(bf16[256,2048]{1,0:T(8,128)(2,1)} %param.11) | copy-start | bytes 3145732
  0.0 6.0 %copy-start.8 = (s32[256,2]{0,1:T(2,128)S(1)}, s32[256,2]{0,1:T(2,128)}, u32[]{:S(2)}) copy-start(s32[256,2]{0,1:T(2,128)} %param.13) | copy-start | bytes 6148
  0.0 6.2 %copy-start.9 = (f32[2048]{0:T(1024)S(1)}, f32[2048]{0:T(1024)}, u32[]{:S(2)}) copy-start(f32[2048]{0:T(1024)} %param.12) | copy-start | bytes 24580
  3.2 51.0 %collective-permute-start.2 = (bf16[528,2048]{1,0:T(8,128)(2,1)}, bf16[528,2048]{1,0:T(8,128)(2,1)}, u32[]{:S(2)}, u32[]{:S(2)}) collective-permute-start(bf16[528,2048]{1,0:T(8,128)(2,1)} %pad_maximum_fusion), channel_id=1, source_target_pairs={{0,1},{1,0},{2,3},{3,2},{4,5},{5,4},{6,7},{7,6},{8,9},{9,8},{10,11... | collective-permute-start | bytes 6488072 | tf_op jit(solution)/shard_map/ppermute | solution.py:23
  7.8 48.7 %all-to-all-start = ((bf16[24,16,1024]{2,1,0:T(8,128)(2,1)}), bf16[24,16,1024]{2,1,0:T(8,128)(2,1)S(1)}, u32[]{:S(2)}, u32[]{:S(2)}) async-start(bf16[24,16,1024]{2,1,0:T(8,128)(2,1)} %bitcast.6), calls=%async_computation | async-start | bytes 1572864 | tf_op jit(solution)/shard_map/all_to_all | solution.py:14
  23.2 37.0 %copy-start.1 = (bf16[1,2048,176]{1,2,0:T(8,128)(2,1)S(1)}, bf16[1,2048,176]{1,2,0:T(8,128)(2,1)}, u32[]{:S(2)}) copy-start(bf16[1,2048,176]{1,2,0:T(8,128)(2,1)} %param.15) | copy-start | bytes 2162692
  56.5 4.0 %copy-start.3 = (bf16[1,2048,176]{1,2,0:T(8,128)(2,1)S(1)}, bf16[1,2048,176]{1,2,0:T(8,128)(2,1)}, u32[]{:S(2)}) copy-start(bf16[1,2048,176]{1,2,0:T(8,128)(2,1)} %param.16) | copy-start | bytes 2162692
  56.6 12.0 %collective-permute-start = (bf16[192,1024]{1,0:T(8,128)(2,1)S(1)}, bf16[192,1024]{1,0:T(8,128)(2,1)S(1)}, u32[]{:S(2)}, u32[]{:S(2)}) collective-permute-start(bf16[192,1024]{1,0:T(8,128)(2,1)S(1)} %bitcast.93), channel_id=1, source_target_pairs={{0,4},{1,5},{2,6},{3,7},{4,8},{5,9},{6,10},{7,11},{8,12},{9,13},{1... | collective-permute-start | bytes 1179656 | tf_op jit(solution)/shard_map/ppermute | solution.py:23
  60.8 11.6 %collective-permute-start.1 = (bf16[192,1024]{1,0:T(8,128)(2,1)S(1)}, bf16[192,1024]{1,0:T(8,128)(2,1)S(1)}, u32[]{:S(2)}, u32[]{:S(2)}) collective-permute-start(bf16[192,1024]{1,0:T(8,128)(2,1)S(1)} %bitcast.88), channel_id=1, source_target_pairs={{0,28},{1,29},{2,30},{3,31},{4,0},{5,1},{6,2},{7,3},{8,4},{9,5},{1... | collective-permute-start | bytes 1179656 | tf_op jit(solution)/shard_map/ppermute | solution.py:23
  63.8 9.2 %copy-start.4 = (bf16[176,2048]{1,0:T(8,128)(2,1)S(1)}, bf16[176,2048]{1,0:T(8,128)(2,1)}, u32[]{:S(2)}) copy-start(bf16[176,2048]{1,0:T(8,128)(2,1)} %get-tuple-element.5) | copy-start | bytes 2162692
  74.5 1.1 copy-start.5
  85.7 5.0 %copy-start.7 = (bf16[32,2048]{1,0:T(8,128)(2,1)S(1)}, bf16[32,2048]{1,0:T(8,128)(2,1)}, u32[]{:S(2)}) copy-start(bf16[32,2048]{1,0:T(8,128)(2,1)} %param.20) | copy-start | bytes 393220
  85.7 5.5 %copy-start.6 = (bf16[2048,32]{0,1:T(8,128)(2,1)S(1)}, bf16[2048,32]{0,1:T(8,128)(2,1)}, u32[]{:S(2)}) copy-start(bf16[2048,32]{0,1:T(8,128)(2,1)} %param.19) | copy-start | bytes 393220
  85.7 23.1 %all-to-all-start.1 = ((bf16[4,512,384]{2,1,0:T(8,128)(2,1)}), bf16[4,512,384]{2,1,0:T(8,128)(2,1)S(1)}, u32[]{:S(2)}, u32[]{:S(2)}) async-start(bf16[4,512,384]{2,1,0:T(8,128)(2,1)} %bitcast.20), calls=%async_computation.1 | async-start | bytes 3145728 | tf_op jit(solution)/shard_map/all_to_all | solution.py:14
  91.6 47.4 %copy-start.10 = (f32[256,2]{0,1:T(2,128)S(1)}, f32[256,2]{0,1:T(2,128)}, u32[]{:S(2)}) copy-start(f32[256,2]{0,1:T(2,128)} %param.14) | copy-start | bytes 6148
  110.0 40.8 %all-to-all-start.2 = ((bf16[24,16,512]{2,1,0:T(8,128)(2,1)}), bf16[24,16,512]{2,1,0:T(8,128)(2,1)S(1)}, u32[]{:S(2)}, u32[]{:S(2)}) async-start(bf16[24,16,512]{2,1,0:T(8,128)(2,1)} %bitcast.23), calls=%async_computation.2 | async-start | bytes 786432 | tf_op jit(solution)/shard_map/all_to_all | solution.py:14
  125.7 15.9 %collective-permute-start.3 = (bf16[512,256]{1,0:T(8,128)(2,1)S(1)}, bf16[512,256]{1,0:T(8,128)(2,1)S(1)}, u32[]{:S(2)}, u32[]{:S(2)}) collective-permute-start(bf16[512,256]{1,0:T(8,128)(2,1)S(1)} %convolution_convert_fusion.3), channel_id=1, source_target_pairs={{0,4},{1,5},{2,6},{3,7},{4,8},{5,9},{6,10},{7,11},{8,12},{9,13},{1... | collective-permute-start | bytes 786440 | tf_op jit(solution)/shard_map/ppermute | solution.py:23
  131.9 17.8 %collective-permute-start.4 = (bf16[512,256]{1,0:T(8,128)(2,1)S(1)}, bf16[512,256]{1,0:T(8,128)(2,1)S(1)}, u32[]{:S(2)}, u32[]{:S(2)}) collective-permute-start(bf16[512,256]{1,0:T(8,128)(2,1)S(1)} %convolution_convert_fusion.2), channel_id=1, source_target_pairs={{0,8},{1,9},{2,10},{3,11},{4,12},{5,13},{6,14},{7,15},{8,16},{9,17... | collective-permute-start | bytes 786440 | tf_op jit(solution)/shard_map/ppermute | solution.py:23
  135.0 39.3 %copy-start.11 = (f32[64]{0:T(128)S(1)}, f32[64]{0:T(128)}, u32[]{:S(2)}) copy-start(f32[64]{0:T(128)} %param.21) | copy-start | bytes 772
  135.0 14.7 %collective-permute-start.5 = (bf16[512,256]{1,0:T(8,128)(2,1)S(1)}, bf16[512,256]{1,0:T(8,128)(2,1)S(1)}, u32[]{:S(2)}, u32[]{:S(2)}) collective-permute-start(bf16[512,256]{1,0:T(8,128)(2,1)S(1)} %convolution_convert_fusion.1), channel_id=1, source_target_pairs={{0,28},{1,29},{2,30},{3,31},{4,0},{5,1},{6,2},{7,3},{8,4},{9,5},{1... | collective-permute-start | bytes 786440 | tf_op jit(solution)/shard_map/ppermute | solution.py:23
  150.8 18.2 %all-to-all-start.4 = ((bf16[8,64,256]{2,1,0:T(8,128)(2,1)}), bf16[8,64,256]{2,1,0:T(8,128)(2,1)S(1)}, u32[]{:S(2)}, u32[]{:S(2)}) async-start(bf16[8,64,256]{2,1,0:T(8,128)(2,1)} %bitcast.27), calls=%async_computation.4 | async-start | bytes 524288 | tf_op jit(solution)/shard_map/all_to_all | solution.py:14
  169.0 15.2 %all-to-all-start.3 = ((bf16[8,64,256]{2,1,0:T(8,128)(2,1)}), bf16[8,64,256]{2,1,0:T(8,128)(2,1)S(1)}, u32[]{:S(2)}, u32[]{:S(2)}) async-start(bf16[8,64,256]{2,1,0:T(8,128)(2,1)} %bitcast.26), calls=%async_computation.3 | async-start | bytes 524288 | tf_op jit(solution)/shard_map/all_to_all | solution.py:14

commit v2 on v1

--- a/solution.py
+++ b/solution.py
@@ -83,9 +83,8 @@
     odd_y, odd_x = lax.axis_index("yc"), lax.axis_index("xl")
     mod_y = lax.axis_index("yb") * 2 + odd_y
 
-    own_w = [expert_gate[0].T, expert_up[0].T, expert_down[0]]
-    swapped = send(jnp.concatenate(own_w, axis=0), lambda y, x: (y, x ^ 1))
-    other_w = [swapped[i * hidden_part : (i + 1) * hidden_part] for i in range(3)]
+    own_w = jnp.concatenate([expert_gate[0].T, expert_up[0].T, expert_down[0]], axis=0)
+    other_w = send(own_w, lambda y, x: (y, x ^ 1))
 
     values = tokens.astype(jnp.float32)
     factor = lax.rsqrt(jnp.mean(values * values, axis=-1, keepdims=True) + EPSILON)
@@ -116,24 +115,35 @@
         send(dense_part(3), along_y(-1)),
     ]
     dense_sum = total_of([dense_part(0), *dense_terms])
-    dense_pieces = exchange(dense_sum.reshape(8, part, group_tokens), ("ya", "xh", "xl"))
-    dense_out = dense_pieces.astype(jnp.float32).sum(axis=0)
+    dense_sum = dense_sum.reshape(2, NEAR, part, group_tokens)
 
-    block = rows_mine // 2
-    arrived = [send(landed[:block], along_y(1)), send(landed[block:], along_y(-1))]
+    def for_x(step):
+        there = (lax.axis_index("xh") * 2 + odd_x + step) % NEAR
+        return lax.dynamic_index_in_dim(dense_sum, there, 1, keepdims=False)
+
+    dense_x = total_of(
+        [for_x(0)] + [send(for_x(k), lambda y, x, k=k: (y, x + k)) for k in range(1, NEAR)]
+    )
+    high = lax.axis_index("ya")
+    dense_mine = lax.dynamic_index_in_dim(dense_x, high, 0, keepdims=False)
+    dense_theirs = lax.dynamic_index_in_dim(dense_x, 1 - high, 0, keepdims=False)
+    dense_theirs = send(dense_theirs, along_y(4))
+    dense_out = dense_mine.astype(jnp.float32) + dense_theirs.astype(jnp.float32)
+
+    arrived = [send(landed[:, :wide], along_y(1)), send(landed[:, wide:], along_y(-1))]
 
     def hidden_of(weights):
-        halves = []
+        gate_up = weights[: 2 * hidden_part]
+        act = dot(side(gate_up, 0), landed, 1, 1)
+        beside = side(gate_up, 1)
         for i in range(2):
-            rows = [landed[i * block : (i + 1) * block], arrived[i]]
-            gate_act = sum(dot(r, side(weights[0], k), 1, 1) for k, r in enumerate(rows))
-            up_act = sum(dot(r, side(weights[1], k), 1, 1) for k, r in enumerate(rows))
-            halves.append(silu_times(gate_act, up_act))
-        return jnp.concatenate(halves, axis=0)
+            act = act + dot(beside[:, i * wide : (i + 1) * wide], arrived[i], 1, 1)
+        return silu_times(act[:hidden_part], act[hidden_part:])
 
     own_hidden = hidden_of(own_w)
     other_hidden = hidden_of(other_w)
-    partial = dot(own_w[2], own_hidden, 0, 1) + dot(other_w[2], other_hidden, 0, 1)
+    partial = dot(own_w[2 * hidden_part :], own_hidden, 0, 0)
+    partial = partial + dot(other_w[2 * hidden_part :], other_hidden, 0, 0)
     partial = partial.astype(jnp.bfloat16).reshape(4, 2, 2, 2 * part, rows_mine)
     partial = partial.transpose(1, 2, 0, 3, 4).reshape(4, wide, rows_mine)
     near_terms = exchange(partial, ("yc", "xh"))

time: 186 us -> 192 us (1.032)
  the two profiles are of different devices: /device:TPU:10 before, /device:TPU:40 now
where the time goes in v2:
time: 192 us; the launch traced here: 191 us
  waiting for transfers between devices  90 us (47%)
  starting transfers between devices  68.6 us (36%)
  matrix products  12.9 us (7%)
  local copies, waits for them, and re-layouts  9.97 us (5%)
  other arithmetic  8.95 us (5%)
    all_to_all x4, waiting for transfers between devices, exchange(): return lax.all_to_all(blocks, axes, split_axis=0, concat_axis=0, tiled=True)  48 us
    ppermute x10, waiting for transfers between devices, send(): return lax.ppermute(value, TP, pairs)  42 us
    all_to_all x4, starting transfers between devices, exchange(): return lax.all_to_all(blocks, axes, split_axis=0, concat_axis=0, tiled=True)  37.9 us
    ppermute x10, starting transfers between devices, send(): return lax.ppermute(value, TP, pairs)  30.7 us
    dot_general x18, matrix products, dot(): lax.dot_general(left, right, (((left_dim,), (right_dim,)), ((), ())), pre...  12.9 us
    reshape x2, local copies, waits for them, and re-layouts, local(): partial = partial.astype(jnp.bfloat16).reshape(4, 2, 2, 2 * part, rows_mine)  6.5 us
  transfers between devices with their start and end apart: 14, of which 8 were waited for; matrix products, arithmetic and copies ran while one was open for 5% of the time, Pallas kernels for 0%

profile of v2, /device:TPU:40, one launch (start us, length us, event | category | flops | bytes accessed | tf_op | source)
XLA Modules:
  0.0 190.9 jit_solution(5980266961477079253)
XLA Ops:
  6.8 15.4 %all-to-all-start = ((bf16[24,16,1024]{2,1,0:T(8,128)(2,1)}), bf16[24,16,1024]{2,1,0:T(8,128)(2,1)S(1)}, u32[]{:S(2)}, u32[]{:S(2)}) async-start(bf16[24,16,1024]{2,1,0:T(8,128)(2,1)} %bitcast.10), calls=%async_computation | async-start | bytes 1572864 | tf_op jit(solution)/shard_map/all_to_all | solution.py:14
  22.2 2.6 %pad_maximum_fusion = bf16[528,2048]{1,0:T(8,128)(2,1)} fusion(bf16[176,2048]{1,0:T(8,128)(2,1)} %bitcast.81, bf16[176,2048]{1,0:T(8,128)(2,1)S(1)} %bitcast.78, bf16[176,2048]{1,0:T(8,128)(2,1)S(1)} %bitcast.75), kind=kLoop, calls=%fused_computation.4 | loop fusion | flops 6488064 | bytes 4325376 | tf_op jit(solution)/shard_map/concatenate | solution.py:86
  24.8 3.4 %collective-permute-start.2 = (bf16[528,2048]{1,0:T(8,128)(2,1)}, bf16[528,2048]{1,0:T(8,128)(2,1)}, u32[]{:S(2)}, u32[]{:S(2)}) collective-permute-start(bf16[528,2048]{1,0:T(8,128)(2,1)} %pad_maximum_fusion), channel_id=1, source_target_pairs={{0,1},{1,0},{2,3},{3,2},{4,5},{5,4},{6,7},{7,6},{8,9},{9,8},{10,11... | collective-permute-start | bytes 6488072 | tf_op jit(solution)/shard_map/ppermute | solution.py:23
  28.2 27.0 %all-to-all-done = bf16[24,16,1024]{2,1,0:T(8,128)(2,1)S(1)} async-done(((bf16[24,16,1024]{2,1,0:T(8,128)(2,1)}), bf16[24,16,1024]{2,1,0:T(8,128)(2,1)S(1)}, u32[]{:S(2)}, u32[]{:S(2)}) %all-to-all-start) | async-done | bytes 786464 | tf_op jit(solution)/shard_map/all_to_all | solution.py:14
  56.1 2.6 %collective-permute-start = (bf16[384,512]{1,0:T(8,128)(2,1)}, bf16[384,512]{1,0:T(8,128)(2,1)}, u32[]{:S(2)}, u32[]{:S(2)}) collective-permute-start(bf16[384,512]{1,0:T(8,128)(2,1)} %get-tuple-element.6), channel_id=1, source_target_pairs={{0,4},{1,5},{2,6},{3,7},{4,8},{5,9},{6,10},{7,11},{8,12},{9,13},{1... | collective-permute-start | bytes 1179656 | tf_op jit(solution)/shard_map/ppermute | solution.py:23
  58.8 17.4 %collective-permute-done.2 = bf16[528,2048]{1,0:T(8,128)(2,1)} collective-permute-done((bf16[528,2048]{1,0:T(8,128)(2,1)}, bf16[528,2048]{1,0:T(8,128)(2,1)}, u32[]{:S(2)}, u32[]{:S(2)}) %collective-permute-start.2) | collective-permute-done | bytes 2162720 | tf_op jit(solution)/shard_map/ppermute | solution.py:23
  77.7 3.3 %collective-permute-start.1 = (bf16[384,512]{1,0:T(8,128)(2,1)S(1)}, bf16[384,512]{1,0:T(8,128)(2,1)S(1)}, u32[]{:S(2)}, u32[]{:S(2)}) collective-permute-start(bf16[384,512]{1,0:T(8,128)(2,1)S(1)} %copy-done.4), channel_id=1, source_target_pairs={{0,28},{1,29},{2,30},{3,31},{4,0},{5,1},{6,2},{7,3},{8,4},{9,5},{1... | collective-permute-start | bytes 1179656 | tf_op jit(solution)/shard_map/ppermute | solution.py:23
  83.0 7.1 %collective-permute-done.1 = bf16[384,512]{1,0:T(8,128)(2,1)S(1)} collective-permute-done((bf16[384,512]{1,0:T(8,128)(2,1)S(1)}, bf16[384,512]{1,0:T(8,128)(2,1)S(1)}, u32[]{:S(2)}, u32[]{:S(2)}) %collective-permute-start.1) | collective-permute-done | bytes 393248 | tf_op jit(solution)/shard_map/ppermute | solution.py:23
  93.4 2.9 %fusion = bf16[2048,384]{0,1:T(8,128)(2,1)} fusion(f32[384,2048]{1,0:T(8,128)S(1)} %fusion.34, bf16[528,2048]{1,0:T(8,128)(2,1)} %collective-permute-done.2, f32[352,384]{1,0:T(8,128)S(1)} %fusion.4), kind=kOutput, calls=%fused_computation.1 | convolution fusion | flops 278802432 | bytes 5980160 | tf_op jit(solution)/shard_map/dot_general | solution.py:31
  96.3 2.8 %reshape.51 = bf16[4,2,2,128,384]{3,2,1,0,4:T(2,128)(2,1)S(1)} reshape(bf16[2048,384]{0,1:T(8,128)(2,1)} %fusion) | data formatting | bytes 3145728 | tf_op jit(solution)/shard_map/reshape | solution.py:147
  99.2 3.7 %copy.19 = bf16[4,2,2,128,384]{4,3,0,2,1:T(8,128)(2,1)} copy(bf16[4,2,2,128,384]{3,2,1,0,4:T(2,128)(2,1)S(1)} %reshape.51) | data formatting | bytes 3145728 | tf_op jit(solution)/shard_map/reshape | solution.py:147
  102.9 5.9 %all-to-all-start.1 = ((bf16[4,512,384]{2,1,0:T(8,128)(2,1)}), bf16[4,512,384]{2,1,0:T(8,128)(2,1)S(1)}, u32[]{:S(2)}, u32[]{:S(2)}) async-start(bf16[4,512,384]{2,1,0:T(8,128)(2,1)} %bitcast.17), calls=%async_computation.1 | async-start | bytes 3145728 | tf_op jit(solution)/shard_map/all_to_all | solution.py:14
  109.7 18.0 %all-to-all-done.1 = bf16[4,512,384]{2,1,0:T(8,128)(2,1)S(1)} async-done(((bf16[4,512,384]{2,1,0:T(8,128)(2,1)}), bf16[4,512,384]{2,1,0:T(8,128)(2,1)S(1)}, u32[]{:S(2)}, u32[]{:S(2)}) %all-to-all-start.1) | async-done | bytes 1572896 | tf_op jit(solution)/shard_map/all_to_all | solution.py:14
  128.8 9.1 %all-to-all-start.2 = ((bf16[24,16,512]{2,1,0:T(8,128)(2,1)}), bf16[24,16,512]{2,1,0:T(8,128)(2,1)S(1)}, u32[]{:S(2)}, u32[]{:S(2)}) async-start(bf16[24,16,512]{2,1,0:T(8,128)(2,1)} %bitcast.20), calls=%async_computation.2 | async-start | bytes 786432 | tf_op jit(solution)/shard_map/all_to_all | solution.py:14
  138.1 3.0 %collective-permute-start.3 = (bf16[512,256]{1,0:T(8,128)(2,1)S(1)}, bf16[512,256]{1,0:T(8,128)(2,1)S(1)}, u32[]{:S(2)}, u32[]{:S(2)}) collective-permute-start(bf16[512,256]{1,0:T(8,128)(2,1)S(1)} %convolution_convert_fusion.3), channel_id=1, source_target_pairs={{0,4},{1,5},{2,6},{3,7},{4,8},{5,9},{6,10},{7,11},{8,12},{9,13},{1... | collective-permute-start | bytes 786440 | tf_op jit(solution)/shard_map/ppermute | solution.py:23
  141.4 2.8 %collective-permute-start.4 = (bf16[512,256]{1,0:T(8,128)(2,1)S(1)}, bf16[512,256]{1,0:T(8,128)(2,1)S(1)}, u32[]{:S(2)}, u32[]{:S(2)}) collective-permute-start(bf16[512,256]{1,0:T(8,128)(2,1)S(1)} %convolution_convert_fusion.2), channel_id=1, source_target_pairs={{0,8},{1,9},{2,10},{3,11},{4,12},{5,13},{6,14},{7,15},{8,16},{9,17... | collective-permute-start | bytes 786440 | tf_op jit(solution)/shard_map/ppermute | solution.py:23
  144.5 3.9 %collective-permute-start.5 = (bf16[512,256]{1,0:T(8,128)(2,1)S(1)}, bf16[512,256]{1,0:T(8,128)(2,1)S(1)}, u32[]{:S(2)}, u32[]{:S(2)}) collective-permute-start(bf16[512,256]{1,0:T(8,128)(2,1)S(1)} %convolution_convert_fusion.1), channel_id=1, source_target_pairs={{0,28},{1,29},{2,30},{3,31},{4,0},{5,1},{6,2},{7,3},{8,4},{9,5},{1... | collective-permute-start | bytes 786440 | tf_op jit(solution)/shard_map/ppermute | solution.py:23
  149.3 11.7 %collective-permute-done.4 = bf16[512,256]{1,0:T(8,128)(2,1)S(1)} collective-permute-done((bf16[512,256]{1,0:T(8,128)(2,1)S(1)}, bf16[512,256]{1,0:T(8,128)(2,1)S(1)}, u32[]{:S(2)}, u32[]{:S(2)}) %collective-permute-start.4) | collective-permute-done | bytes 262176 | tf_op jit(solution)/shard_map/ppermute | solution.py:23
  161.3 2.8 %collective-permute-start.6 = (bf16[2,64,256]{2,1,0:T(8,128)(2,1)S(1)}, bf16[2,64,256]{2,1,0:T(8,128)(2,1)S(1)}, u32[]{:S(2)}, u32[]{:S(2)}) collective-permute-start(bf16[2,64,256]{2,1,0:T(8,128)(2,1)S(1)} %get-tuple-element.7), channel_id=1, source_target_pairs={{0,1},{1,2},{2,3},{3,0},{4,5},{5,6},{6,7},{7,4},{8,9},{9,10},{10,1... | collective-permute-start | bytes 196616 | tf_op jit(solution)/shard_map/ppermute | solution.py:23
  164.2 4.0 %collective-permute-start.7 = (bf16[2,64,256]{2,1,0:T(8,128)(2,1)S(1)}, bf16[2,64,256]{2,1,0:T(8,128)(2,1)S(1)}, u32[]{:S(2)}, u32[]{:S(2)}) collective-permute-start(bf16[2,64,256]{2,1,0:T(8,128)(2,1)S(1)} %get-tuple-element.9), channel_id=1, source_target_pairs={{0,2},{1,3},{2,0},{3,1},{4,6},{5,7},{6,4},{7,5},{8,10},{9,11},{10,... | collective-permute-start | bytes 196616 | tf_op jit(solution)/shard_map/ppermute | solution.py:23
  168.2 3.0 %collective-permute-start.8 = (bf16[2,64,256]{2,1,0:T(8,128)(2,1)S(1)}, bf16[2,64,256]{2,1,0:T(8,128)(2,1)S(1)}, u32[]{:S(2)}, u32[]{:S(2)}) collective-permute-start(bf16[2,64,256]{2,1,0:T(8,128)(2,1)S(1)} %get-tuple-element.8), channel_id=1, source_target_pairs={{0,3},{1,0},{2,1},{3,2},{4,7},{5,4},{6,5},{7,6},{8,11},{9,8},{10,9... | collective-permute-start | bytes 196616 | tf_op jit(solution)/shard_map/ppermute | solution.py:23
  172.6 7.6 %all-to-all-start.3 = ((bf16[8,64,256]{2,1,0:T(8,128)(2,1)}), bf16[8,64,256]{2,1,0:T(8,128)(2,1)S(1)}, u32[]{:S(2)}, u32[]{:S(2)}) async-start(bf16[8,64,256]{2,1,0:T(8,128)(2,1)} %bitcast.23), calls=%async_computation.3 | async-start | bytes 524288 | tf_op jit(solution)/shard_map/all_to_all | solution.py:14
  182.2 3.0 %all-to-all-done.3 = bf16[8,64,256]{2,1,0:T(8,128)(2,1)S(1)} async-done(((bf16[8,64,256]{2,1,0:T(8,128)(2,1)}), bf16[8,64,256]{2,1,0:T(8,128)(2,1)S(1)}, u32[]{:S(2)}, u32[]{:S(2)}) %all-to-all-start.3) | async-done | bytes 262176 | tf_op jit(solution)/shard_map/all_to_all | solution.py:14
  185.3 4.9 %collective-permute-done.9 = bf16[64,256]{1,0:T(8,128)(2,1)S(1)} collective-permute-done((bf16[64,256]{1,0:T(8,128)(2,1)S(1)}, bf16[64,256]{1,0:T(8,128)(2,1)S(1)}, u32[]{:S(2)}, u32[]{:S(2)}) %collective-permute-start.9) | collective-permute-done | bytes 32800 | tf_op jit(solution)/shard_map/ppermute | solution.py:23
  (63 shorter events, 22.5 us)
Async XLA Ops:
  0.0 108.8 %copy-start = (bf16[2048,32]{0,1:T(8,128)(2,1)S(1)}, bf16[2048,32]{0,1:T(8,128)(2,1)}, u32[]{:S(2)}) copy-start(bf16[2048,32]{0,1:T(8,128)(2,1)} %param.18) | copy-start | bytes 393220
  3.8 18.3 %copy-start.1 = (bf16[1,2048,176]{1,2,0:T(8,128)(2,1)S(1)}, bf16[1,2048,176]{1,2,0:T(8,128)(2,1)}, u32[]{:S(2)}) copy-start(bf16[1,2048,176]{1,2,0:T(8,128)(2,1)} %param.15) | copy-start | bytes 2162692
  3.8 18.3 %copy-start.2 = (bf16[1,2048,176]{1,2,0:T(8,128)(2,1)S(1)}, bf16[1,2048,176]{1,2,0:T(8,128)(2,1)}, u32[]{:S(2)}) copy-start(bf16[1,2048,176]{1,2,0:T(8,128)(2,1)} %param.16) | copy-start | bytes 2162692
  6.8 48.4 %all-to-all-start = ((bf16[24,16,1024]{2,1,0:T(8,128)(2,1)}), bf16[24,16,1024]{2,1,0:T(8,128)(2,1)S(1)}, u32[]{:S(2)}, u32[]{:S(2)}) async-start(bf16[24,16,1024]{2,1,0:T(8,128)(2,1)} %bitcast.10), calls=%async_computation | async-start | bytes 1572864 | tf_op jit(solution)/shard_map/all_to_all | solution.py:14
  24.8 51.5 %collective-permute-start.2 = (bf16[528,2048]{1,0:T(8,128)(2,1)}, bf16[528,2048]{1,0:T(8,128)(2,1)}, u32[]{:S(2)}, u32[]{:S(2)}) collective-permute-start(bf16[528,2048]{1,0:T(8,128)(2,1)} %pad_maximum_fusion), channel_id=1, source_target_pairs={{0,1},{1,0},{2,3},{3,2},{4,5},{5,4},{6,7},{7,6},{8,9},{9,8},{10,11... | collective-permute-start | bytes 6488072 | tf_op jit(solution)/shard_map/ppermute | solution.py:23
  56.1 25.4 %collective-permute-start = (bf16[384,512]{1,0:T(8,128)(2,1)}, bf16[384,512]{1,0:T(8,128)(2,1)}, u32[]{:S(2)}, u32[]{:S(2)}) collective-permute-start(bf16[384,512]{1,0:T(8,128)(2,1)} %get-tuple-element.6), channel_id=1, source_target_pairs={{0,4},{1,5},{2,6},{3,7},{4,8},{5,9},{6,10},{7,11},{8,12},{9,13},{1... | collective-permute-start | bytes 1179656 | tf_op jit(solution)/shard_map/ppermute | solution.py:23
  58.7 19.0 %copy-start.4 = (bf16[384,512]{1,0:T(8,128)(2,1)S(1)}, bf16[384,512]{1,0:T(8,128)(2,1)}, u32[]{:S(2)}) copy-start(bf16[384,512]{1,0:T(8,128)(2,1)} %get-tuple-element.5) | copy-start | bytes 1179652
  77.7 12.4 %collective-permute-start.1 = (bf16[384,512]{1,0:T(8,128)(2,1)S(1)}, bf16[384,512]{1,0:T(8,128)(2,1)S(1)}, u32[]{:S(2)}, u32[]{:S(2)}) collective-permute-start(bf16[384,512]{1,0:T(8,128)(2,1)S(1)} %copy-done.4), channel_id=1, source_target_pairs={{0,28},{1,29},{2,30},{3,31},{4,0},{5,1},{6,2},{7,3},{8,4},{9,5},{1... | collective-permute-start | bytes 1179656 | tf_op jit(solution)/shard_map/ppermute | solution.py:23
  81.6 8.9 %copy-start.3 = (bf16[1,176,2048]{2,1,0:T(8,128)(2,1)S(1)}, bf16[1,176,2048]{2,1,0:T(8,128)(2,1)}, u32[]{:S(2)}) copy-start(bf16[1,176,2048]{2,1,0:T(8,128)(2,1)} %param.17) | copy-start | bytes 2162692
  102.8 5.9 %copy-start.6 = (bf16[32,2048]{1,0:T(8,128)(2,1)S(1)}, bf16[32,2048]{1,0:T(8,128)(2,1)}, u32[]{:S(2)}) copy-start(bf16[32,2048]{1,0:T(8,128)(2,1)} %param.20) | copy-start | bytes 393220
  102.9 6.4 %copy-start.5 = (bf16[2048,32]{0,1:T(8,128)(2,1)S(1)}, bf16[2048,32]{0,1:T(8,128)(2,1)}, u32[]{:S(2)}) copy-start(bf16[2048,32]{0,1:T(8,128)(2,1)} %param.19) | copy-start | bytes 393220
  102.9 24.8 %all-to-all-start.1 = ((bf16[4,512,384]{2,1,0:T(8,128)(2,1)}), bf16[4,512,384]{2,1,0:T(8,128)(2,1)S(1)}, u32[]{:S(2)}, u32[]{:S(2)}) async-start(bf16[4,512,384]{2,1,0:T(8,128)(2,1)} %bitcast.17), calls=%async_computation.1 | async-start | bytes 3145728 | tf_op jit(solution)/shard_map/all_to_all | solution.py:14
  109.7 38.8 %copy-start.7 = (f32[256,2]{0,1:T(2,128)S(1)}, f32[256,2]{0,1:T(2,128)}, u32[]{:S(2)}) copy-start(f32[256,2]{0,1:T(2,128)} %param.14) | copy-start | bytes 6148
  128.8 42.4 %all-to-all-start.2 = ((bf16[24,16,512]{2,1,0:T(8,128)(2,1)}), bf16[24,16,512]{2,1,0:T(8,128)(2,1)S(1)}, u32[]{:S(2)}, u32[]{:S(2)}) async-start(bf16[24,16,512]{2,1,0:T(8,128)(2,1)} %bitcast.20), calls=%async_computation.2 | async-start | bytes 786432 | tf_op jit(solution)/shard_map/all_to_all | solution.py:14
  138.1 11.1 %collective-permute-start.3 = (bf16[512,256]{1,0:T(8,128)(2,1)S(1)}, bf16[512,256]{1,0:T(8,128)(2,1)S(1)}, u32[]{:S(2)}, u32[]{:S(2)}) collective-permute-start(bf16[512,256]{1,0:T(8,128)(2,1)S(1)} %convolution_convert_fusion.3), channel_id=1, source_target_pairs={{0,4},{1,5},{2,6},{3,7},{4,8},{5,9},{6,10},{7,11},{8,12},{9,13},{1... | collective-permute-start | bytes 786440 | tf_op jit(solution)/shard_map/ppermute | solution.py:23
  141.4 19.6 %collective-permute-start.4 = (bf16[512,256]{1,0:T(8,128)(2,1)S(1)}, bf16[512,256]{1,0:T(8,128)(2,1)S(1)}, u32[]{:S(2)}, u32[]{:S(2)}) collective-permute-start(bf16[512,256]{1,0:T(8,128)(2,1)S(1)} %convolution_convert_fusion.2), channel_id=1, source_target_pairs={{0,8},{1,9},{2,10},{3,11},{4,12},{5,13},{6,14},{7,15},{8,16},{9,17... | collective-permute-start | bytes 786440 | tf_op jit(solution)/shard_map/ppermute | solution.py:23
  144.5 16.5 %collective-permute-start.5 = (bf16[512,256]{1,0:T(8,128)(2,1)S(1)}, bf16[512,256]{1,0:T(8,128)(2,1)S(1)}, u32[]{:S(2)}, u32[]{:S(2)}) collective-permute-start(bf16[512,256]{1,0:T(8,128)(2,1)S(1)} %convolution_convert_fusion.1), channel_id=1, source_target_pairs={{0,28},{1,29},{2,30},{3,31},{4,0},{5,1},{6,2},{7,3},{8,4},{9,5},{1... | collective-permute-start | bytes 786440 | tf_op jit(solution)/shard_map/ppermute | solution.py:23
  148.4 31.7 %copy-start.8 = (f32[64]{0:T(128)S(1)}, f32[64]{0:T(128)}, u32[]{:S(2)}) copy-start(f32[64]{0:T(128)} %param.21) | copy-start | bytes 772
  161.3 18.9 %collective-permute-start.6 = (bf16[2,64,256]{2,1,0:T(8,128)(2,1)S(1)}, bf16[2,64,256]{2,1,0:T(8,128)(2,1)S(1)}, u32[]{:S(2)}, u32[]{:S(2)}) collective-permute-start(bf16[2,64,256]{2,1,0:T(8,128)(2,1)S(1)} %get-tuple-element.7), channel_id=1, source_target_pairs={{0,1},{1,2},{2,3},{3,0},{4,5},{5,6},{6,7},{7,4},{8,9},{9,10},{10,1... | collective-permute-start | bytes 196616 | tf_op jit(solution)/shard_map/ppermute | solution.py:23
  164.2 16.1 %collective-permute-start.7 = (bf16[2,64,256]{2,1,0:T(8,128)(2,1)S(1)}, bf16[2,64,256]{2,1,0:T(8,128)(2,1)S(1)}, u32[]{:S(2)}, u32[]{:S(2)}) collective-permute-start(bf16[2,64,256]{2,1,0:T(8,128)(2,1)S(1)} %get-tuple-element.9), channel_id=1, source_target_pairs={{0,2},{1,3},{2,0},{3,1},{4,6},{5,7},{6,4},{7,5},{8,10},{9,11},{10,... | collective-permute-start | bytes 196616 | tf_op jit(solution)/shard_map/ppermute | solution.py:23
  168.2 12.0 %collective-permute-start.8 = (bf16[2,64,256]{2,1,0:T(8,128)(2,1)S(1)}, bf16[2,64,256]{2,1,0:T(8,128)(2,1)S(1)}, u32[]{:S(2)}, u32[]{:S(2)}) collective-permute-start(bf16[2,64,256]{2,1,0:T(8,128)(2,1)S(1)} %get-tuple-element.8), channel_id=1, source_target_pairs={{0,3},{1,0},{2,1},{3,2},{4,7},{5,4},{6,5},{7,6},{8,11},{9,8},{10,9... | collective-permute-start | bytes 196616 | tf_op jit(solution)/shard_map/ppermute | solution.py:23
  172.6 12.6 %all-to-all-start.3 = ((bf16[8,64,256]{2,1,0:T(8,128)(2,1)}), bf16[8,64,256]{2,1,0:T(8,128)(2,1)S(1)}, u32[]{:S(2)}, u32[]{:S(2)}) async-start(bf16[8,64,256]{2,1,0:T(8,128)(2,1)} %bitcast.23), calls=%async_computation.3 | async-start | bytes 524288 | tf_op jit(solution)/shard_map/all_to_all | solution.py:14
  180.3 9.9 %collective-permute-start.9 = (bf16[64,256]{1,0:T(8,128)(2,1)S(1)}, bf16[64,256]{1,0:T(8,128)(2,1)S(1)}, u32[]{:S(2)}, u32[]{:S(2)}) collective-permute-start(bf16[64,256]{1,0:T(8,128)(2,1)S(1)} %dynamic-slice_bitcast_fusion.3), channel_id=1, source_target_pairs={{0,16},{1,17},{2,18},{3,19},{4,20},{5,21},{6,22},{7,23},{8,24},{9,... | collective-permute-start | bytes 98312 | tf_op jit(solution)/shard_map/ppermute | solution.py:23

commit v3 on v2

--- a/solution.py
+++ b/solution.py
@@ -1,6 +1,8 @@
 import jax
 import jax.numpy as jnp
 from jax import lax
+from jax.experimental import pallas as pl
+from jax.experimental.pallas import tpu as pltpu
 from jax.sharding import Mesh
 from jax.sharding import PartitionSpec as P
 
@@ -56,6 +58,67 @@
     return jnp.concatenate(
         [lax.dynamic_slice_in_dim(weight, start, size, 1) for start in starts], axis=1
     )
+
+
+def ffn_kernel(
+    place, near_rows, below, above, gate, up, down, first, second, out_0, out_1, out_2, out_3
+):
+    odd_y, half_x = place[0], place[1]
+    width = near_rows.shape[1]
+    half = width // 2
+    near = pl.multiple_of(odd_y * width, 128)
+    beside = pl.multiple_of((1 - odd_y) * width, 128)
+
+    def product(ref, start, count):
+        rows = pl.ds(start, count)
+        return (
+            dot(near_rows[...], ref[rows, pl.ds(near, width)], 1, 1)
+            + dot(below[...], ref[rows, pl.ds(beside, half)], 1, 1)
+            + dot(above[...], ref[rows, pl.ds(pl.multiple_of(beside + half, 128), half)], 1, 1)
+        )
+
+    pieces = []
+    own = gate.shape[0]
+    hidden = silu_times(product(gate, 0, own), product(up, 0, own))
+    pieces.append((hidden, down, 0, own))
+    for ref in (first, second):
+        count = ref.shape[0] // 3
+        hidden = silu_times(product(ref, 0, count), product(ref, count, count))
+        pieces.append((hidden, ref, 2 * count, count))
+    for k, out in enumerate((out_0, out_1, out_2, out_3)):
+        y_bit, x_bit = odd_y ^ (k & 1), half_x ^ (k >> 1)
+        total = None
+        for hidden, ref, start, count in pieces:
+            picked = [
+                ref[
+                    pl.ds(start, count),
+                    pl.ds(pl.multiple_of(((2 * q + y_bit) * 2 + x_bit) * 128, 128), 128),
+                ]
+                for q in range(4)
+            ]
+            term = dot(hidden, jnp.concatenate(picked, axis=1), 1, 0)
+            total = term if total is None else total + term
+        out[...] = total.astype(jnp.bfloat16)
+
+
+def ffn(place, near_rows, below, above, gate, up, down, first, second):
+    rows = near_rows.shape[0]
+    wide = down.shape[1] // 4
+    in_vmem = pl.BlockSpec(memory_space=pltpu.VMEM)
+    units = gate.shape[0] + (first.shape[0] + second.shape[0]) // 3
+    return pl.pallas_call(
+        ffn_kernel,
+        out_shape=[jax.ShapeDtypeStruct((rows, wide), jnp.bfloat16)] * 4,
+        in_specs=[pl.BlockSpec(memory_space=pltpu.SMEM)] + [in_vmem] * 8,
+        out_specs=[in_vmem] * 4,
+        cost_estimate=pl.CostEstimate(
+            flops=6 * rows * units * down.shape[1],
+            bytes_accessed=2 * down.shape[1] * (3 * units + 2 * rows),
+            transcendentals=rows * units,
+        ),
+        compiler_params=pltpu.CompilerParams(vmem_limit_bytes=24 * 1024 * 1024),
+        name="ffn",
+    )(place, near_rows, below, above, gate, up, down, first, second)
 
 
 def local(
@@ -83,8 +146,14 @@
     odd_y, odd_x = lax.axis_index("yc"), lax.axis_index("xl")
     mod_y = lax.axis_index("yb") * 2 + odd_y
 
-    own_w = jnp.concatenate([expert_gate[0].T, expert_up[0].T, expert_down[0]], axis=0)
-    other_w = send(own_w, lambda y, x: (y, x ^ 1))
+    gate_t, up_t, down = expert_gate[0].T, expert_up[0].T, expert_down[0]
+    split = (hidden_part // 2 + 15) // 16 * 16
+
+    def packed(first, last):
+        return jnp.concatenate([w[first:last] for w in (gate_t, up_t, down)], axis=0)
+
+    first_w = send(packed(0, split), lambda y, x: (y, x ^ 1))
+    second_w = send(packed(split, hidden_part), lambda y, x: (y, x + (1 if x % 2 else -1)))
 
     values = tokens.astype(jnp.float32)
     factor = lax.rsqrt(jnp.mean(values * values, axis=-1, keepdims=True) + EPSILON)
@@ -132,23 +201,15 @@
 
     arrived = [send(landed[:, :wide], along_y(1)), send(landed[:, wide:], along_y(-1))]
 
-    def hidden_of(weights):
-        gate_up = weights[: 2 * hidden_part]
-        act = dot(side(gate_up, 0), landed, 1, 1)
-        beside = side(gate_up, 1)
-        for i in range(2):
-            act = act + dot(beside[:, i * wide : (i + 1) * wide], arrived[i], 1, 1)
-        return silu_times(act[:hidden_part], act[hidden_part:])
-
-    own_hidden = hidden_of(own_w)
-    other_hidden = hidden_of(other_w)
-    partial = dot(own_w[2 * hidden_part :], own_hidden, 0, 0)
-    partial = partial + dot(other_w[2 * hidden_part :], other_hidden, 0, 0)
-    partial = partial.astype(jnp.bfloat16).reshape(4, 2, 2, 2 * part, rows_mine)
-    partial = partial.transpose(1, 2, 0, 3, 4).reshape(4, wide, rows_mine)
-    near_terms = exchange(partial, ("yc", "xh"))
-    near_sum = total_of([near_terms[k] for k in range(4)])
-    returned = exchange(near_sum.T.reshape(experts, few, wide), "ep")
+    place = jnp.stack([odd_y, lax.axis_index("xh")])
+    out = ffn(place, landed, *arrived, gate_t, up_t, down, first_w, second_w)
+    back = [
+        send(out[1], lambda y, x: (y + 1, x)),
+        send(out[3], lambda y, x: (y + 1, x + 2)),
+        send(out[2], lambda y, x: (y, x + 2)),
+    ]
+    near_sum = total_of([out[0], *back])
+    returned = exchange(near_sum.reshape(experts, few, wide), "ep")
     returned = returned.reshape(rows_mine, wide)
     weight = routing_weight.T
     routed = sum(weight[c][None, :] * dot(returned, chosen[c], 0, 0) for c in range(2))

time: 192 us -> 166 us (0.86)
  waiting for transfers between devices: 90 us -> 65.2 us
  starting transfers between devices: 68.6 us -> 77.3 us
  matrix products: 12.9 us -> 4.67 us
  Pallas kernels: 0 us -> 6.39 us
  local copies, waits for them, and re-layouts: 9.97 us -> 4 us
  other arithmetic: 8.95 us -> 6.64 us
    all_to_all x4 -> x3, waiting for transfers between devices: 48 us -> 25.2 us  [exchange(): return lax.all_to_all(blocks, axes, split_axis=0, concat_axis=0, tiled=True)]
    ppermute x10 -> x14, starting transfers between devices: 30.7 us -> 44.4 us  [send(): return lax.ppermute(value, TP, pairs)]
    dot_general x18 -> x10, matrix products: 12.9 us -> 4.67 us  [dot(): lax.dot_general(left, right, (((left_dim,), (right_dim,)), ((), ())), pre...]
    reshape x2 -> x0, local copies, waits for them, and re-layouts: 6.5 us -> none  [local(): partial = partial.astype(jnp.bfloat16).reshape(4, 2, 2, 2 * part, rows_mine)]
    pallas_call x0 -> x1, Pallas kernels: none -> 6.39 us  [ffn(): pl.pallas_call(ffn_kernel, out_shape=[jax.ShapeDtypeStruct((rows, wide),...]
    all_to_all x4 -> x3, starting transfers between devices: 37.9 us -> 33 us  [exchange(): return lax.all_to_all(blocks, axes, split_axis=0, concat_axis=0, tiled=True)]
    unnamed x18 -> x32, local copies, waits for them, and re-layouts: 0.06 us -> 2.82 us
    ppermute x10 -> x14, waiting for transfers between devices: 42 us -> 39.9 us  [send(): return lax.ppermute(value, TP, pairs)]
  transfers between devices with their start and end apart: 14 -> 17, of which waited for: 8 -> 10; matrix products, arithmetic and copies ran while one was open for 5% -> 4% of each run, Pallas kernels for 0% -> 0%
where the time goes in v3:
time: 166 us; the launch traced here: 165 us
  starting transfers between devices  77.3 us (47%)
  waiting for transfers between devices  65.2 us (39%)
  other arithmetic  6.64 us (4%)
  Pallas kernels  6.39 us (4%)
  matrix products  4.67 us (3%)
  local copies, waits for them, and re-layouts  4 us (2%)
    ppermute x14, starting transfers between devices, send(): return lax.ppermute(value, TP, pairs)  44.4 us
    ppermute x14, waiting for transfers between devices, send(): return lax.ppermute(value, TP, pairs)  39.9 us
    all_to_all x3, starting transfers between devices, exchange(): return lax.all_to_all(blocks, axes, split_axis=0, concat_axis=0, tiled=True)  33 us
    all_to_all x3, waiting for transfers between devices, exchange(): return lax.all_to_all(blocks, axes, split_axis=0, concat_axis=0, tiled=True)  25.2 us
    pallas_call x1, Pallas kernels, ffn(): pl.pallas_call(ffn_kernel, out_shape=[jax.ShapeDtypeStruct((rows, wide),...  6.39 us
    dot_general x10, matrix products, dot(): lax.dot_general(left, right, (((left_dim,), (right_dim,)), ((), ())), pre...  4.67 us
  transfers between devices with their start and end apart: 17, of which 10 were waited for; matrix products, arithmetic and copies ran while one was open for 4% of the time, Pallas kernels for 0%

profile of v3, /device:TPU:40, one launch (start us, length us, event | category | flops | bytes accessed | tf_op | source)
XLA Modules:
  0.0 164.8 jit_solution(10639137054626104537)
XLA Ops:
  4.2 15.5 %all-to-all-start = ((bf16[24,16,1024]{2,1,0:T(8,128)(2,1)}), bf16[24,16,1024]{2,1,0:T(8,128)(2,1)S(1)}, u32[]{:S(2)}, u32[]{:S(2)}) async-start(bf16[24,16,1024]{2,1,0:T(8,128)(2,1)} %bitcast.8), calls=%async_computation | async-start | bytes 1572864 | tf_op jit(solution)/shard_map/all_to_all | solution.py:16
  22.0 3.4 %collective-permute-start.2 = (bf16[288,2048]{1,0:T(8,128)(2,1)}, bf16[288,2048]{1,0:T(8,128)(2,1)}, u32[]{:S(2)}, u32[]{:S(2)}) collective-permute-start(bf16[288,2048]{1,0:T(8,128)(2,1)} %pad_maximum_fusion), channel_id=1, source_target_pairs={{0,1},{1,0},{2,3},{3,2},{4,5},{5,4},{6,7},{7,6},{8,9},{9,8},{10,11... | collective-permute-start | bytes 3538952 | tf_op jit(solution)/shard_map/ppermute | solution.py:25
  26.5 4.0 %collective-permute-start.3 = (bf16[240,2048]{1,0:T(8,128)(2,1)}, bf16[240,2048]{1,0:T(8,128)(2,1)}, u32[]{:S(2)}, u32[]{:S(2)}) collective-permute-start(bf16[240,2048]{1,0:T(8,128)(2,1)} %pad_maximum_fusion.1), channel_id=1, source_target_pairs={{0,3},{1,2},{2,1},{3,0},{4,7},{5,6},{6,5},{7,4},{8,11},{9,10},{10,... | collective-permute-start | bytes 2949128 | tf_op jit(solution)/shard_map/ppermute | solution.py:25
  30.5 22.2 %all-to-all-done = bf16[24,16,1024]{2,1,0:T(8,128)(2,1)S(1)} async-done(((bf16[24,16,1024]{2,1,0:T(8,128)(2,1)}), bf16[24,16,1024]{2,1,0:T(8,128)(2,1)S(1)}, u32[]{:S(2)}, u32[]{:S(2)}) %all-to-all-start) | async-done | bytes 786464 | tf_op jit(solution)/shard_map/all_to_all | solution.py:16
  53.7 2.6 %collective-permute-start = (bf16[384,512]{1,0:T(8,128)(2,1)}, bf16[384,512]{1,0:T(8,128)(2,1)S(1)}, u32[]{:S(2)}, u32[]{:S(2)}) collective-permute-start(bf16[384,512]{1,0:T(8,128)(2,1)} %get-tuple-element.14), channel_id=1, source_target_pairs={{0,4},{1,5},{2,6},{3,7},{4,8},{5,9},{6,10},{7,11},{8,12},{9,13},{1... | collective-permute-start | bytes 1179656 | tf_op jit(solution)/shard_map/ppermute | solution.py:25
  56.3 3.3 %collective-permute-start.1 = (bf16[384,512]{1,0:T(8,128)(2,1)}, bf16[384,512]{1,0:T(8,128)(2,1)}, u32[]{:S(2)}, u32[]{:S(2)}) collective-permute-start(bf16[384,512]{1,0:T(8,128)(2,1)} %get-tuple-element.13), channel_id=1, source_target_pairs={{0,28},{1,29},{2,30},{3,31},{4,0},{5,1},{6,2},{7,3},{8,4},{9,5},{1... | collective-permute-start | bytes 1179656 | tf_op jit(solution)/shard_map/ppermute | solution.py:25
  59.6 5.3 %collective-permute-done.below = bf16[384,512]{1,0:T(8,128)(2,1)S(1)} collective-permute-done((bf16[384,512]{1,0:T(8,128)(2,1)}, bf16[384,512]{1,0:T(8,128)(2,1)S(1)}, u32[]{:S(2)}, u32[]{:S(2)}) %collective-permute-start) | collective-permute-done | bytes 393248 | tf_op jit(solution)/shard_map/ppermute | solution.py:25
  68.3 6.4 %ffn.1 = (bf16[384,512]{1,0:T(8,128)(2,1)S(1)}, bf16[384,512]{1,0:T(8,128)(2,1)}, bf16[384,512]{1,0:T(8,128)(2,1)}, bf16[384,512]{1,0:T(8,128)(2,1)}) custom-call(s32[2]{0:T(128)S(1)} %pad_add_fusion.place, bf16[384,1024]{1,0:T(8,128)(2,1)S(1)} %bitcast.58, bf16[384,512]{1,0:T(8,128)(2,1)S(1)} %copy-done.5, bf16[384,512]{1,0:T(8,128)(2,1)} %collective-permute-done.1.above, ...), custom_call_target="tpu_custom_call" | custom-call | flops 1660944384 | bytes 7471104 | tf_op jit(solution)/shard_map/ffn/pallas_call | solution.py:109
  74.7 2.7 %collective-permute-start.4 = (bf16[384,512]{1,0:T(8,128)(2,1)}, bf16[384,512]{1,0:T(8,128)(2,1)S(1)}, u32[]{:S(2)}, u32[]{:S(2)}) collective-permute-start(bf16[384,512]{1,0:T(8,128)(2,1)} %get-tuple-element.10), channel_id=1, source_target_pairs={{0,4},{1,5},{2,6},{3,7},{4,8},{5,9},{6,10},{7,11},{8,12},{9,13},{1... | collective-permute-start | bytes 1179656 | tf_op jit(solution)/shard_map/ppermute | solution.py:25
  77.4 5.9 %collective-permute-start.5 = (bf16[384,512]{1,0:T(8,128)(2,1)}, bf16[384,512]{1,0:T(8,128)(2,1)S(1)}, u32[]{:S(2)}, u32[]{:S(2)}) collective-permute-start(bf16[384,512]{1,0:T(8,128)(2,1)} %get-tuple-element.11), channel_id=1, source_target_pairs={{0,6},{1,7},{2,4},{3,5},{4,10},{5,11},{6,8},{7,9},{8,14},{9,15},{1... | collective-permute-start | bytes 1179656 | tf_op jit(solution)/shard_map/ppermute | solution.py:25
  83.3 2.4 %collective-permute-start.6 = (bf16[384,512]{1,0:T(8,128)(2,1)}, bf16[384,512]{1,0:T(8,128)(2,1)S(1)}, u32[]{:S(2)}, u32[]{:S(2)}) collective-permute-start(bf16[384,512]{1,0:T(8,128)(2,1)} %get-tuple-element.12), channel_id=1, source_target_pairs={{0,2},{1,3},{2,0},{3,1},{4,6},{5,7},{6,4},{7,5},{8,10},{9,11},{10,... | collective-permute-start | bytes 1179656 | tf_op jit(solution)/shard_map/ppermute | solution.py:25
  88.5 7.3 %collective-permute-done.5 = bf16[384,512]{1,0:T(8,128)(2,1)S(1)} collective-permute-done((bf16[384,512]{1,0:T(8,128)(2,1)}, bf16[384,512]{1,0:T(8,128)(2,1)S(1)}, u32[]{:S(2)}, u32[]{:S(2)}) %collective-permute-start.5) | collective-permute-done | bytes 393248 | tf_op jit(solution)/shard_map/ppermute | solution.py:25
  95.9 5.7 %collective-permute-done.6 = bf16[384,512]{1,0:T(8,128)(2,1)S(1)} collective-permute-done((bf16[384,512]{1,0:T(8,128)(2,1)}, bf16[384,512]{1,0:T(8,128)(2,1)S(1)}, u32[]{:S(2)}, u32[]{:S(2)}) %collective-permute-start.6) | collective-permute-done | bytes 393248 | tf_op jit(solution)/shard_map/ppermute | solution.py:25
  102.5 9.5 %all-to-all-start.1 = ((bf16[24,16,512]{2,1,0:T(8,128)(2,1)}), bf16[24,16,512]{2,1,0:T(8,128)(2,1)S(1)}, u32[]{:S(2)}, u32[]{:S(2)}) async-start(bf16[24,16,512]{2,1,0:T(8,128)(2,1)} %bitcast.19), calls=%async_computation.1 | async-start | bytes 786432 | tf_op jit(solution)/shard_map/all_to_all | solution.py:16
  112.3 2.2 %collective-permute-start.7 = (bf16[512,256]{1,0:T(8,128)(2,1)S(1)}, bf16[512,256]{1,0:T(8,128)(2,1)S(1)}, u32[]{:S(2)}, u32[]{:S(2)}) collective-permute-start(bf16[512,256]{1,0:T(8,128)(2,1)S(1)} %convolution_convert_fusion.3), channel_id=1, source_target_pairs={{0,4},{1,5},{2,6},{3,7},{4,8},{5,9},{6,10},{7,11},{8,12},{9,13},{1... | collective-permute-start | bytes 786440 | tf_op jit(solution)/shard_map/ppermute | solution.py:25
  114.7 5.1 %collective-permute-start.8 = (bf16[512,256]{1,0:T(8,128)(2,1)S(1)}, bf16[512,256]{1,0:T(8,128)(2,1)S(1)}, u32[]{:S(2)}, u32[]{:S(2)}) collective-permute-start(bf16[512,256]{1,0:T(8,128)(2,1)S(1)} %convolution_convert_fusion.2), channel_id=1, source_target_pairs={{0,8},{1,9},{2,10},{3,11},{4,12},{5,13},{6,14},{7,15},{8,16},{9,17... | collective-permute-start | bytes 786440 | tf_op jit(solution)/shard_map/ppermute | solution.py:25
  123.3 12.0 %collective-permute-done.8 = bf16[512,256]{1,0:T(8,128)(2,1)S(1)} collective-permute-done((bf16[512,256]{1,0:T(8,128)(2,1)S(1)}, bf16[512,256]{1,0:T(8,128)(2,1)S(1)}, u32[]{:S(2)}, u32[]{:S(2)}) %collective-permute-start.8) | collective-permute-done | bytes 262176 | tf_op jit(solution)/shard_map/ppermute | solution.py:25
  135.6 2.5 %collective-permute-start.10 = (bf16[2,64,256]{2,1,0:T(8,128)(2,1)S(1)}, bf16[2,64,256]{2,1,0:T(8,128)(2,1)S(1)}, u32[]{:S(2)}, u32[]{:S(2)}) collective-permute-start(bf16[2,64,256]{2,1,0:T(8,128)(2,1)S(1)} %get-tuple-element.15), channel_id=1, source_target_pairs={{0,1},{1,2},{2,3},{3,0},{4,5},{5,6},{6,7},{7,4},{8,9},{9,10},{10,1... | collective-permute-start | bytes 196616 | tf_op jit(solution)/shard_map/ppermute | solution.py:25
  138.2 3.9 %collective-permute-start.11 = (bf16[2,64,256]{2,1,0:T(8,128)(2,1)S(1)}, bf16[2,64,256]{2,1,0:T(8,128)(2,1)S(1)}, u32[]{:S(2)}, u32[]{:S(2)}) collective-permute-start(bf16[2,64,256]{2,1,0:T(8,128)(2,1)S(1)} %get-tuple-element.17), channel_id=1, source_target_pairs={{0,2},{1,3},{2,0},{3,1},{4,6},{5,7},{6,4},{7,5},{8,10},{9,11},{10,... | collective-permute-start | bytes 196616 | tf_op jit(solution)/shard_map/ppermute | solution.py:25
  142.1 2.6 %collective-permute-start.12 = (bf16[2,64,256]{2,1,0:T(8,128)(2,1)S(1)}, bf16[2,64,256]{2,1,0:T(8,128)(2,1)S(1)}, u32[]{:S(2)}, u32[]{:S(2)}) collective-permute-start(bf16[2,64,256]{2,1,0:T(8,128)(2,1)S(1)} %get-tuple-element.16), channel_id=1, source_target_pairs={{0,3},{1,0},{2,1},{3,2},{4,7},{5,4},{6,5},{7,6},{8,11},{9,8},{10,9... | collective-permute-start | bytes 196616 | tf_op jit(solution)/shard_map/ppermute | solution.py:25
  146.1 8.0 %all-to-all-start.2 = ((bf16[8,64,256]{2,1,0:T(8,128)(2,1)}), bf16[8,64,256]{2,1,0:T(8,128)(2,1)S(1)}, u32[]{:S(2)}, u32[]{:S(2)}) async-start(bf16[8,64,256]{2,1,0:T(8,128)(2,1)} %bitcast.22), calls=%async_computation.2 | async-start | bytes 524288 | tf_op jit(solution)/shard_map/all_to_all | solution.py:16
  154.2 1.9 %collective-permute-start.13 = (bf16[64,256]{1,0:T(8,128)(2,1)S(1)}, bf16[64,256]{1,0:T(8,128)(2,1)S(1)}, u32[]{:S(2)}, u32[]{:S(2)}) collective-permute-start(bf16[64,256]{1,0:T(8,128)(2,1)S(1)} %dynamic-slice_bitcast_fusion.3), channel_id=1, source_target_pairs={{0,16},{1,17},{2,18},{3,19},{4,20},{5,21},{6,22},{7,23},{8,24},{9,... | collective-permute-start | bytes 98312 | tf_op jit(solution)/shard_map/ppermute | solution.py:25
  156.1 3.0 %all-to-all-done.2 = bf16[8,64,256]{2,1,0:T(8,128)(2,1)S(1)} async-done(((bf16[8,64,256]{2,1,0:T(8,128)(2,1)}), bf16[8,64,256]{2,1,0:T(8,128)(2,1)S(1)}, u32[]{:S(2)}, u32[]{:S(2)}) %all-to-all-start.2) | async-done | bytes 262176 | tf_op jit(solution)/shard_map/all_to_all | solution.py:16
  159.2 4.9 %collective-permute-done.13 = bf16[64,256]{1,0:T(8,128)(2,1)S(1)} collective-permute-done((bf16[64,256]{1,0:T(8,128)(2,1)S(1)}, bf16[64,256]{1,0:T(8,128)(2,1)S(1)}, u32[]{:S(2)}, u32[]{:S(2)}) %collective-permute-start.13) | collective-permute-done | bytes 32800 | tf_op jit(solution)/shard_map/ppermute | solution.py:25
  (79 shorter events, 22.0 us)
Async XLA Ops:
  0.0 85.7 %copy-start = (bf16[2048,32]{0,1:T(8,128)(2,1)S(1)}, bf16[2048,32]{0,1:T(8,128)(2,1)}, u32[]{:S(2)}) copy-start(bf16[2048,32]{0,1:T(8,128)(2,1)} %param.18) | copy-start | bytes 393220
  2.9 16.8 %copy-start.1 = (bf16[1,2048,176]{1,2,0:T(8,128)(2,1)S(1)}, bf16[1,2048,176]{1,2,0:T(8,128)(2,1)}, u32[]{:S(2)}) copy-start(bf16[1,2048,176]{1,2,0:T(8,128)(2,1)} %param.15) | copy-start | bytes 2162692
  4.2 15.6 %copy-start.2 = (bf16[1,2048,176]{1,2,0:T(8,128)(2,1)S(1)}, bf16[1,2048,176]{1,2,0:T(8,128)(2,1)}, u32[]{:S(2)}) copy-start(bf16[1,2048,176]{1,2,0:T(8,128)(2,1)} %param.16) | copy-start | bytes 2162692
  4.2 48.5 %all-to-all-start = ((bf16[24,16,1024]{2,1,0:T(8,128)(2,1)}), bf16[24,16,1024]{2,1,0:T(8,128)(2,1)S(1)}, u32[]{:S(2)}, u32[]{:S(2)}) async-start(bf16[24,16,1024]{2,1,0:T(8,128)(2,1)} %bitcast.8), calls=%async_computation | async-start | bytes 1572864 | tf_op jit(solution)/shard_map/all_to_all | solution.py:16
  22.0 37.7 %collective-permute-start.2 = (bf16[288,2048]{1,0:T(8,128)(2,1)}, bf16[288,2048]{1,0:T(8,128)(2,1)}, u32[]{:S(2)}, u32[]{:S(2)}) collective-permute-start(bf16[288,2048]{1,0:T(8,128)(2,1)} %pad_maximum_fusion), channel_id=1, source_target_pairs={{0,1},{1,0},{2,3},{3,2},{4,5},{5,4},{6,7},{7,6},{8,9},{9,8},{10,11... | collective-permute-start | bytes 3538952 | tf_op jit(solution)/shard_map/ppermute | solution.py:25
  26.5 33.1 %collective-permute-start.3 = (bf16[240,2048]{1,0:T(8,128)(2,1)}, bf16[240,2048]{1,0:T(8,128)(2,1)}, u32[]{:S(2)}, u32[]{:S(2)}) collective-permute-start(bf16[240,2048]{1,0:T(8,128)(2,1)} %pad_maximum_fusion.1), channel_id=1, source_target_pairs={{0,3},{1,2},{2,1},{3,0},{4,7},{5,6},{6,5},{7,4},{8,11},{9,10},{10,... | collective-permute-start | bytes 2949128 | tf_op jit(solution)/shard_map/ppermute | solution.py:25
  53.7 11.2 %collective-permute-start = (bf16[384,512]{1,0:T(8,128)(2,1)}, bf16[384,512]{1,0:T(8,128)(2,1)S(1)}, u32[]{:S(2)}, u32[]{:S(2)}) collective-permute-start(bf16[384,512]{1,0:T(8,128)(2,1)} %get-tuple-element.14), channel_id=1, source_target_pairs={{0,4},{1,5},{2,6},{3,7},{4,8},{5,9},{6,10},{7,11},{8,12},{9,13},{1... | collective-permute-start | bytes 1179656 | tf_op jit(solution)/shard_map/ppermute | solution.py:25
  56.3 11.0 %collective-permute-start.1 = (bf16[384,512]{1,0:T(8,128)(2,1)}, bf16[384,512]{1,0:T(8,128)(2,1)}, u32[]{:S(2)}, u32[]{:S(2)}) collective-permute-start(bf16[384,512]{1,0:T(8,128)(2,1)} %get-tuple-element.13), channel_id=1, source_target_pairs={{0,28},{1,29},{2,30},{3,31},{4,0},{5,1},{6,2},{7,3},{8,4},{9,5},{1... | collective-permute-start | bytes 1179656 | tf_op jit(solution)/shard_map/ppermute | solution.py:25
  68.3 17.4 %copy-start.7 = (bf16[256,2048]{1,0:T(8,128)(2,1)S(1)}, bf16[256,2048]{1,0:T(8,128)(2,1)}, u32[]{:S(2)}) copy-start(bf16[256,2048]{1,0:T(8,128)(2,1)} %copy-done.6) | copy-start | bytes 3145732
  74.7 11.6 %copy-start.8 = (bf16[256,2048]{1,0:T(8,128)(2,1)S(1)}, bf16[256,2048]{1,0:T(8,128)(2,1)}, u32[]{:S(2)}) copy-start(bf16[256,2048]{1,0:T(8,128)(2,1)} %copy-done.6) | copy-start | bytes 3145732
  74.7 11.6 %copy-start.10 = (bf16[2048,32]{0,1:T(8,128)(2,1)S(1)}, bf16[2048,32]{0,1:T(8,128)(2,1)}, u32[]{:S(2)}) copy-start(bf16[2048,32]{0,1:T(8,128)(2,1)} %param.19) | copy-start | bytes 393220
  74.7 13.8 %collective-permute-start.4 = (bf16[384,512]{1,0:T(8,128)(2,1)}, bf16[384,512]{1,0:T(8,128)(2,1)S(1)}, u32[]{:S(2)}, u32[]{:S(2)}) collective-permute-start(bf16[384,512]{1,0:T(8,128)(2,1)} %get-tuple-element.10), channel_id=1, source_target_pairs={{0,4},{1,5},{2,6},{3,7},{4,8},{5,9},{6,10},{7,11},{8,12},{9,13},{1... | collective-permute-start | bytes 1179656 | tf_op jit(solution)/shard_map/ppermute | solution.py:25
  77.4 18.5 %collective-permute-start.5 = (bf16[384,512]{1,0:T(8,128)(2,1)}, bf16[384,512]{1,0:T(8,128)(2,1)S(1)}, u32[]{:S(2)}, u32[]{:S(2)}) collective-permute-start(bf16[384,512]{1,0:T(8,128)(2,1)} %get-tuple-element.11), channel_id=1, source_target_pairs={{0,6},{1,7},{2,4},{3,5},{4,10},{5,11},{6,8},{7,9},{8,14},{9,15},{1... | collective-permute-start | bytes 1179656 | tf_op jit(solution)/shard_map/ppermute | solution.py:25
  83.3 18.3 %collective-permute-start.6 = (bf16[384,512]{1,0:T(8,128)(2,1)}, bf16[384,512]{1,0:T(8,128)(2,1)S(1)}, u32[]{:S(2)}, u32[]{:S(2)}) collective-permute-start(bf16[384,512]{1,0:T(8,128)(2,1)} %get-tuple-element.12), channel_id=1, source_target_pairs={{0,2},{1,3},{2,0},{3,1},{4,6},{5,7},{6,4},{7,5},{8,10},{9,11},{10,... | collective-permute-start | bytes 1179656 | tf_op jit(solution)/shard_map/ppermute | solution.py:25
  102.5 19.5 %copy-start.14 = (f32[256,2]{0,1:T(2,128)S(1)}, f32[256,2]{0,1:T(2,128)}, u32[]{:S(2)}) copy-start(f32[256,2]{0,1:T(2,128)} %param.14) | copy-start | bytes 6148
  102.5 42.1 %all-to-all-start.1 = ((bf16[24,16,512]{2,1,0:T(8,128)(2,1)}), bf16[24,16,512]{2,1,0:T(8,128)(2,1)S(1)}, u32[]{:S(2)}, u32[]{:S(2)}) async-start(bf16[24,16,512]{2,1,0:T(8,128)(2,1)} %bitcast.19), calls=%async_computation.1 | async-start | bytes 786432 | tf_op jit(solution)/shard_map/all_to_all | solution.py:16
  112.3 11.1 %collective-permute-start.7 = (bf16[512,256]{1,0:T(8,128)(2,1)S(1)}, bf16[512,256]{1,0:T(8,128)(2,1)S(1)}, u32[]{:S(2)}, u32[]{:S(2)}) collective-permute-start(bf16[512,256]{1,0:T(8,128)(2,1)S(1)} %convolution_convert_fusion.3), channel_id=1, source_target_pairs={{0,4},{1,5},{2,6},{3,7},{4,8},{5,9},{6,10},{7,11},{8,12},{9,13},{1... | collective-permute-start | bytes 786440 | tf_op jit(solution)/shard_map/ppermute | solution.py:25
  114.7 20.6 %collective-permute-start.8 = (bf16[512,256]{1,0:T(8,128)(2,1)S(1)}, bf16[512,256]{1,0:T(8,128)(2,1)S(1)}, u32[]{:S(2)}, u32[]{:S(2)}) collective-permute-start(bf16[512,256]{1,0:T(8,128)(2,1)S(1)} %convolution_convert_fusion.2), channel_id=1, source_target_pairs={{0,8},{1,9},{2,10},{3,11},{4,12},{5,13},{6,14},{7,15},{8,16},{9,17... | collective-permute-start | bytes 786440 | tf_op jit(solution)/shard_map/ppermute | solution.py:25
  120.1 15.2 %collective-permute-start.9 = (bf16[512,256]{1,0:T(8,128)(2,1)S(1)}, bf16[512,256]{1,0:T(8,128)(2,1)S(1)}, u32[]{:S(2)}, u32[]{:S(2)}) collective-permute-start(bf16[512,256]{1,0:T(8,128)(2,1)S(1)} %convolution_convert_fusion.1), channel_id=1, source_target_pairs={{0,28},{1,29},{2,30},{3,31},{4,0},{5,1},{6,2},{7,3},{8,4},{9,5},{1... | collective-permute-start | bytes 786440 | tf_op jit(solution)/shard_map/ppermute | solution.py:25
  135.6 18.5 %collective-permute-start.10 = (bf16[2,64,256]{2,1,0:T(8,128)(2,1)S(1)}, bf16[2,64,256]{2,1,0:T(8,128)(2,1)S(1)}, u32[]{:S(2)}, u32[]{:S(2)}) collective-permute-start(bf16[2,64,256]{2,1,0:T(8,128)(2,1)S(1)} %get-tuple-element.15), channel_id=1, source_target_pairs={{0,1},{1,2},{2,3},{3,0},{4,5},{5,6},{6,7},{7,4},{8,9},{9,10},{10,1... | collective-permute-start | bytes 196616 | tf_op jit(solution)/shard_map/ppermute | solution.py:25
  138.2 16.0 %collective-permute-start.11 = (bf16[2,64,256]{2,1,0:T(8,128)(2,1)S(1)}, bf16[2,64,256]{2,1,0:T(8,128)(2,1)S(1)}, u32[]{:S(2)}, u32[]{:S(2)}) collective-permute-start(bf16[2,64,256]{2,1,0:T(8,128)(2,1)S(1)} %get-tuple-element.17), channel_id=1, source_target_pairs={{0,2},{1,3},{2,0},{3,1},{4,6},{5,7},{6,4},{7,5},{8,10},{9,11},{10,... | collective-permute-start | bytes 196616 | tf_op jit(solution)/shard_map/ppermute | solution.py:25
  142.1 12.0 %collective-permute-start.12 = (bf16[2,64,256]{2,1,0:T(8,128)(2,1)S(1)}, bf16[2,64,256]{2,1,0:T(8,128)(2,1)S(1)}, u32[]{:S(2)}, u32[]{:S(2)}) collective-permute-start(bf16[2,64,256]{2,1,0:T(8,128)(2,1)S(1)} %get-tuple-element.16), channel_id=1, source_target_pairs={{0,3},{1,0},{2,1},{3,2},{4,7},{5,4},{6,5},{7,6},{8,11},{9,8},{10,9... | collective-permute-start | bytes 196616 | tf_op jit(solution)/shard_map/ppermute | solution.py:25
  146.1 13.1 %all-to-all-start.2 = ((bf16[8,64,256]{2,1,0:T(8,128)(2,1)}), bf16[8,64,256]{2,1,0:T(8,128)(2,1)S(1)}, u32[]{:S(2)}, u32[]{:S(2)}) async-start(bf16[8,64,256]{2,1,0:T(8,128)(2,1)} %bitcast.22), calls=%async_computation.2 | async-start | bytes 524288 | tf_op jit(solution)/shard_map/all_to_all | solution.py:16
  154.2 9.9 %collective-permute-start.13 = (bf16[64,256]{1,0:T(8,128)(2,1)S(1)}, bf16[64,256]{1,0:T(8,128)(2,1)S(1)}, u32[]{:S(2)}, u32[]{:S(2)}) collective-permute-start(bf16[64,256]{1,0:T(8,128)(2,1)S(1)} %dynamic-slice_bitcast_fusion.3), channel_id=1, source_target_pairs={{0,16},{1,17},{2,18},{3,19},{4,20},{5,21},{6,22},{7,23},{8,24},{9,... | collective-permute-start | bytes 98312 | tf_op jit(solution)/shard_map/ppermute | solution.py:25
  (9 other events, 32.7 us)

commit v4 on v3

--- a/solution.py
+++ b/solution.py
@@ -61,9 +61,9 @@
 
 
 def ffn_kernel(
-    place, near_rows, below, above, gate, up, down, first, second, out_0, out_1, out_2, out_3
+    place, near_rows, below, above, gate, up, down, first, second, out
 ):
-    odd_y, half_x = place[0], place[1]
+    odd_y = place[0]
     width = near_rows.shape[1]
     half = width // 2
     near = pl.multiple_of(odd_y * width, 128)
@@ -85,32 +85,26 @@
         count = ref.shape[0] // 3
         hidden = silu_times(product(ref, 0, count), product(ref, count, count))
         pieces.append((hidden, ref, 2 * count, count))
-    for k, out in enumerate((out_0, out_1, out_2, out_3)):
-        y_bit, x_bit = odd_y ^ (k & 1), half_x ^ (k >> 1)
-        total = None
-        for hidden, ref, start, count in pieces:
-            picked = [
-                ref[
-                    pl.ds(start, count),
-                    pl.ds(pl.multiple_of(((2 * q + y_bit) * 2 + x_bit) * 128, 128), 128),
-                ]
-                for q in range(4)
-            ]
-            term = dot(hidden, jnp.concatenate(picked, axis=1), 1, 0)
-            total = term if total is None else total + term
-        out[...] = total.astype(jnp.bfloat16)
+    for q in range(4):
+        for y_bit in range(2):
+            columns_of = pl.ds((2 * q + y_bit) * 256, 256)
+            total = sum(
+                dot(hidden, ref[pl.ds(start, count), columns_of], 1, 0)
+                for hidden, ref, start, count in pieces
+            ).astype(jnp.bfloat16)
+            for x_bit in range(2):
+                out[2 * y_bit + x_bit, q] = total[:, x_bit * 128 : (x_bit + 1) * 128]
 
 
 def ffn(place, near_rows, below, above, gate, up, down, first, second):
     rows = near_rows.shape[0]
-    wide = down.shape[1] // 4
     in_vmem = pl.BlockSpec(memory_space=pltpu.VMEM)
     units = gate.shape[0] + (first.shape[0] + second.shape[0]) // 3
     return pl.pallas_call(
         ffn_kernel,
-        out_shape=[jax.ShapeDtypeStruct((rows, wide), jnp.bfloat16)] * 4,
+        out_shape=jax.ShapeDtypeStruct((4, 4, rows, down.shape[1] // 16), jnp.bfloat16),
         in_specs=[pl.BlockSpec(memory_space=pltpu.SMEM)] + [in_vmem] * 8,
-        out_specs=[in_vmem] * 4,
+        out_specs=in_vmem,
         cost_estimate=pl.CostEstimate(
             flops=6 * rows * units * down.shape[1],
             bytes_accessed=2 * down.shape[1] * (3 * units + 2 * rows),
@@ -201,22 +195,18 @@
 
     arrived = [send(landed[:, :wide], along_y(1)), send(landed[:, wide:], along_y(-1))]
 
-    place = jnp.stack([odd_y, lax.axis_index("xh")])
-    out = ffn(place, landed, *arrived, gate_t, up_t, down, first_w, second_w)
-    back = [
-        send(out[1], lambda y, x: (y + 1, x)),
-        send(out[3], lambda y, x: (y + 1, x + 2)),
-        send(out[2], lambda y, x: (y, x + 2)),
-    ]
-    near_sum = total_of([out[0], *back])
-    returned = exchange(near_sum.reshape(experts, few, wide), "ep")
-    returned = returned.reshape(rows_mine, wide)
+    partial = ffn(odd_y[None], landed, *arrived, gate_t, up_t, down, first_w, second_w)
+    near_terms = exchange(partial, ("yc", "xh"))
+    near_sum = total_of([near_terms[k] for k in range(4)])
+    far_terms = exchange(near_sum, ("ya", "yb"))
+    expert_out = total_of([far_terms[k] for k in range(4)])
+    returned = exchange(expert_out.reshape(experts, few, 2 * part), "ep")
+    returned = returned.reshape(rows_mine, 2 * part)
     weight = routing_weight.T
     routed = sum(weight[c][None, :] * dot(returned, chosen[c], 0, 0) for c in range(2))
-    pieces = exchange(
-        routed.astype(jnp.bfloat16).reshape(8, part, group_tokens), ("ya", "yb", "xl")
-    )
-    routed = pieces.astype(jnp.float32).sum(axis=0)
+    keep = lax.dynamic_slice_in_dim(routed, odd_x * part, part, 0)
+    give = lax.dynamic_slice_in_dim(routed, (1 - odd_x) * part, part, 0)
+    routed = keep + send(give.astype(jnp.bfloat16), lambda y, x: (y, x ^ 1)).astype(jnp.float32)
     gate_factor = jax.nn.sigmoid(dense_gate)[:, None]
     return (routed + gate_factor * dense_out).astype(jnp.bfloat16).T
 

time: 166 us -> 160 us (0.964)
  the two profiles are of different devices: /device:TPU:40 before, /device:TPU:26 now
where the time goes in v4:
time: 160 us
  starting transfers between devices  70 us (44%)
  waiting for transfers between devices  68.6 us (43%)
  other arithmetic  9.3 us (6%)
  Pallas kernels  6.56 us (4%)
  matrix products  3.77 us (2%)
    all_to_all x4, waiting for transfers between devices, exchange(): return lax.all_to_all(blocks, axes, split_axis=0, concat_axis=0, tiled=True)  47.7 us
    ppermute x12, starting transfers between devices, send(): return lax.ppermute(value, TP, pairs)  37.7 us
    all_to_all x4, starting transfers between devices, exchange(): return lax.all_to_all(blocks, axes, split_axis=0, concat_axis=0, tiled=True)  32.2 us
    ppermute x12, waiting for transfers between devices, send(): return lax.ppermute(value, TP, pairs)  21 us
    pallas_call x1, Pallas kernels, ffn(): pl.pallas_call(ffn_kernel, out_shape=jax.ShapeDtypeStruct((4, 4, rows, do...  6.56 us
    dot_general x10, matrix products, dot(): lax.dot_general(left, right, (((left_dim,), (right_dim,)), ((), ())), pre...  3.77 us
  transfers between devices with their start and end apart: 16, of which 7 were waited for; matrix products, arithmetic and copies ran while one was open for 4% of the time, Pallas kernels for 0%

profile of v4, /device:TPU:26, one launch (start us, length us, event | category | flops | bytes accessed | tf_op | source)
XLA Modules:
  0.0 159.5 jit_solution(5792218806105839621)
XLA Ops:
  6.2 15.5 %all-to-all-start = ((bf16[24,16,1024]{2,1,0:T(8,128)(2,1)}), bf16[24,16,1024]{2,1,0:T(8,128)(2,1)S(1)}, u32[]{:S(2)}, u32[]{:S(2)}) async-start(bf16[24,16,1024]{2,1,0:T(8,128)(2,1)} %bitcast.66), calls=%async_computation | async-start | bytes 1572864 | tf_op jit(solution)/shard_map/all_to_all | solution.py:16
  23.0 2.4 %collective-permute-start.2 = (bf16[288,2048]{1,0:T(8,128)(2,1)}, bf16[288,2048]{1,0:T(8,128)(2,1)}, u32[]{:S(2)}, u32[]{:S(2)}) collective-permute-start(bf16[288,2048]{1,0:T(8,128)(2,1)} %pad_maximum_fusion), channel_id=1, source_target_pairs={{0,1},{1,0},{2,3},{3,2},{4,5},{5,4},{6,7},{7,6},{8,9},{9,8},{10,11... | collective-permute-start | bytes 3538952 | tf_op jit(solution)/shard_map/ppermute | solution.py:25
  26.6 4.1 %collective-permute-start.3 = (bf16[240,2048]{1,0:T(8,128)(2,1)}, bf16[240,2048]{1,0:T(8,128)(2,1)}, u32[]{:S(2)}, u32[]{:S(2)}) collective-permute-start(bf16[240,2048]{1,0:T(8,128)(2,1)} %pad_maximum_fusion.1), channel_id=1, source_target_pairs={{0,3},{1,2},{2,1},{3,0},{4,7},{5,6},{6,5},{7,4},{8,11},{9,10},{10,... | collective-permute-start | bytes 2949128 | tf_op jit(solution)/shard_map/ppermute | solution.py:25
  30.7 24.1 %all-to-all-done = bf16[24,16,1024]{2,1,0:T(8,128)(2,1)S(1)} async-done(((bf16[24,16,1024]{2,1,0:T(8,128)(2,1)}), bf16[24,16,1024]{2,1,0:T(8,128)(2,1)S(1)}, u32[]{:S(2)}, u32[]{:S(2)}) %all-to-all-start) | async-done | bytes 786464 | tf_op jit(solution)/shard_map/all_to_all | solution.py:16
  54.8 4.7 %collective-permute-start = (bf16[384,512]{1,0:T(8,128)(2,1)S(1)}, bf16[384,512]{1,0:T(8,128)(2,1)S(1)}, u32[]{:S(2)}, u32[]{:S(2)}) collective-permute-start(bf16[384,512]{1,0:T(8,128)(2,1)S(1)} %get-tuple-element.6), channel_id=1, source_target_pairs={{0,4},{1,5},{2,6},{3,7},{4,8},{5,9},{6,10},{7,11},{8,12},{9,13},{1... | collective-permute-start | bytes 1179656 | tf_op jit(solution)/shard_map/ppermute | solution.py:25
  59.5 1.9 %collective-permute-start.1 = (bf16[384,512]{1,0:T(8,128)(2,1)S(1)}, bf16[384,512]{1,0:T(8,128)(2,1)S(1)}, u32[]{:S(2)}, u32[]{:S(2)}) collective-permute-start(bf16[384,512]{1,0:T(8,128)(2,1)S(1)} %get-tuple-element.5), channel_id=1, source_target_pairs={{0,28},{1,29},{2,30},{3,31},{4,0},{5,1},{6,2},{7,3},{8,4},{9,5},{1... | collective-permute-start | bytes 1179656 | tf_op jit(solution)/shard_map/ppermute | solution.py:25
  61.5 4.6 %collective-permute-done.below = bf16[384,512]{1,0:T(8,128)(2,1)S(1)} collective-permute-done((bf16[384,512]{1,0:T(8,128)(2,1)S(1)}, bf16[384,512]{1,0:T(8,128)(2,1)S(1)}, u32[]{:S(2)}, u32[]{:S(2)}) %collective-permute-start) | collective-permute-done | bytes 393248 | tf_op jit(solution)/shard_map/ppermute | solution.py:25
  66.1 5.3 %collective-permute-done.1.above = bf16[384,512]{1,0:T(8,128)(2,1)S(1)} collective-permute-done((bf16[384,512]{1,0:T(8,128)(2,1)S(1)}, bf16[384,512]{1,0:T(8,128)(2,1)S(1)}, u32[]{:S(2)}, u32[]{:S(2)}) %collective-permute-start.1) | collective-permute-done | bytes 393248 | tf_op jit(solution)/shard_map/ppermute | solution.py:25
  71.5 6.6 %ffn.1 = bf16[4,4,384,128]{3,2,1,0:T(8,128)(2,1)} custom-call(s32[1]{0:T(128)} %bitcast.2.place, bf16[384,1024]{1,0:T(8,128)(2,1)S(1)} %bitcast.58, bf16[384,512]{1,0:T(8,128)(2,1)S(1)} %collective-permute-done.below, bf16[384,512]{1,0:T(8,128)(2,1)S(1)} %collective-permute-done.1.above, bf16[176,2048]{1,0:T(8,128)(2,1)S(1)} %bitcast.61, ...), custom_call_target="tpu_custom_call" | custom-call | flops 1660944384 | bytes 7471104 | tf_op jit(solution)/shard_map/ffn/pallas_call | solution.py:103
  78.0 5.0 %all-to-all-start.1 = ((bf16[4,4,384,128]{3,2,1,0:T(8,128)(2,1)}), bf16[4,4,384,128]{3,2,1,0:T(8,128)(2,1)S(1)}, u32[]{:S(2)}, u32[]{:S(2)}) async-start(bf16[4,4,384,128]{3,2,1,0:T(8,128)(2,1)} %ffn.1), calls=%async_computation.1 | async-start | bytes 3145728 | tf_op jit(solution)/shard_map/all_to_all | solution.py:16
  84.6 1.9 %collective-permute-start.7 = (bf16[512,256]{1,0:T(8,128)(2,1)S(1)}, bf16[512,256]{1,0:T(8,128)(2,1)S(1)}, u32[]{:S(2)}, u32[]{:S(2)}) collective-permute-start(bf16[512,256]{1,0:T(8,128)(2,1)S(1)} %convolution_convert_fusion.1), channel_id=1, source_target_pairs={{0,28},{1,29},{2,30},{3,31},{4,0},{5,1},{6,2},{7,3},{8,4},{9,5},{1... | collective-permute-start | bytes 786440 | tf_op jit(solution)/shard_map/ppermute | solution.py:25
  86.8 1.9 %collective-permute-start.6 = (bf16[512,256]{1,0:T(8,128)(2,1)S(1)}, bf16[512,256]{1,0:T(8,128)(2,1)S(1)}, u32[]{:S(2)}, u32[]{:S(2)}) collective-permute-start(bf16[512,256]{1,0:T(8,128)(2,1)S(1)} %convolution_convert_fusion.2), channel_id=1, source_target_pairs={{0,8},{1,9},{2,10},{3,11},{4,12},{5,13},{6,14},{7,15},{8,16},{9,17... | collective-permute-start | bytes 786440 | tf_op jit(solution)/shard_map/ppermute | solution.py:25
  89.0 5.1 %collective-permute-start.5 = (bf16[512,256]{1,0:T(8,128)(2,1)S(1)}, bf16[512,256]{1,0:T(8,128)(2,1)S(1)}, u32[]{:S(2)}, u32[]{:S(2)}) collective-permute-start(bf16[512,256]{1,0:T(8,128)(2,1)S(1)} %convolution_convert_fusion.3), channel_id=1, source_target_pairs={{0,4},{1,5},{2,6},{3,7},{4,8},{5,9},{6,10},{7,11},{8,12},{9,13},{1... | collective-permute-start | bytes 786440 | tf_op jit(solution)/shard_map/ppermute | solution.py:25
  94.2 14.1 %all-to-all-done.1 = bf16[4,4,384,128]{3,2,1,0:T(8,128)(2,1)S(1)} async-done(((bf16[4,4,384,128]{3,2,1,0:T(8,128)(2,1)}), bf16[4,4,384,128]{3,2,1,0:T(8,128)(2,1)S(1)}, u32[]{:S(2)}, u32[]{:S(2)}) %all-to-all-start.1) | async-done | bytes 1572896 | tf_op jit(solution)/shard_map/all_to_all | solution.py:16
  109.3 4.2 %all-to-all-start.2 = ((bf16[4,384,128]{2,1,0:T(8,128)(2,1)}), bf16[4,384,128]{2,1,0:T(8,128)(2,1)S(1)}, u32[]{:S(2)}, u32[]{:S(2)}) async-start(bf16[4,384,128]{2,1,0:T(8,128)(2,1)} %fusion.7), calls=%async_computation.2 | async-start | bytes 786432 | tf_op jit(solution)/shard_map/all_to_all | solution.py:16
  113.5 7.3 %collective-permute-done.5 = bf16[512,256]{1,0:T(8,128)(2,1)S(1)} collective-permute-done((bf16[512,256]{1,0:T(8,128)(2,1)S(1)}, bf16[512,256]{1,0:T(8,128)(2,1)S(1)}, u32[]{:S(2)}, u32[]{:S(2)}) %collective-permute-start.5) | collective-permute-done | bytes 262176 | tf_op jit(solution)/shard_map/ppermute | solution.py:25
  121.1 3.3 %collective-permute-start.10 = (bf16[2,64,256]{2,1,0:T(8,128)(2,1)S(1)}, bf16[2,64,256]{2,1,0:T(8,128)(2,1)S(1)}, u32[]{:S(2)}, u32[]{:S(2)}) collective-permute-start(bf16[2,64,256]{2,1,0:T(8,128)(2,1)S(1)} %get-tuple-element.8), channel_id=1, source_target_pairs={{0,3},{1,0},{2,1},{3,2},{4,7},{5,4},{6,5},{7,6},{8,11},{9,8},{10,9... | collective-permute-start | bytes 196616 | tf_op jit(solution)/shard_map/ppermute | solution.py:25
  124.5 4.5 %collective-permute-start.9 = (bf16[2,64,256]{2,1,0:T(8,128)(2,1)S(1)}, bf16[2,64,256]{2,1,0:T(8,128)(2,1)S(1)}, u32[]{:S(2)}, u32[]{:S(2)}) collective-permute-start(bf16[2,64,256]{2,1,0:T(8,128)(2,1)S(1)} %get-tuple-element.9), channel_id=1, source_target_pairs={{0,2},{1,3},{2,0},{3,1},{4,6},{5,7},{6,4},{7,5},{8,10},{9,11},{10,... | collective-permute-start | bytes 196616 | tf_op jit(solution)/shard_map/ppermute | solution.py:25
  129.0 3.7 %collective-permute-start.8 = (bf16[2,64,256]{2,1,0:T(8,128)(2,1)S(1)}, bf16[2,64,256]{2,1,0:T(8,128)(2,1)S(1)}, u32[]{:S(2)}, u32[]{:S(2)}) collective-permute-start(bf16[2,64,256]{2,1,0:T(8,128)(2,1)S(1)} %get-tuple-element.7), channel_id=1, source_target_pairs={{0,1},{1,2},{2,3},{3,0},{4,5},{5,6},{6,7},{7,4},{8,9},{9,10},{10,1... | collective-permute-start | bytes 196616 | tf_op jit(solution)/shard_map/ppermute | solution.py:25
  133.5 7.6 %all-to-all-start.3 = ((bf16[24,16,128]{2,1,0:T(8,128)(2,1)}), bf16[24,16,128]{2,1,0:T(8,128)(2,1)S(1)}, u32[]{:S(2)}, u32[]{:S(2)}) async-start(bf16[24,16,128]{2,1,0:T(8,128)(2,1)} %bitcast.19), calls=%async_computation.3 | async-start | bytes 196608 | tf_op jit(solution)/shard_map/all_to_all | solution.py:16
  141.1 1.9 %collective-permute-start.11 = (bf16[64,256]{1,0:T(8,128)(2,1)S(1)}, bf16[64,256]{1,0:T(8,128)(2,1)S(1)}, u32[]{:S(2)}, u32[]{:S(2)}) collective-permute-start(bf16[64,256]{1,0:T(8,128)(2,1)S(1)} %dynamic-slice_bitcast_fusion.3), channel_id=1, source_target_pairs={{0,16},{1,17},{2,18},{3,19},{4,20},{5,21},{6,22},{7,23},{8,24},{9,... | collective-permute-start | bytes 98312 | tf_op jit(solution)/shard_map/ppermute | solution.py:25
  143.1 9.5 %all-to-all-done.3 = bf16[24,16,128]{2,1,0:T(8,128)(2,1)S(1)} async-done(((bf16[24,16,128]{2,1,0:T(8,128)(2,1)}), bf16[24,16,128]{2,1,0:T(8,128)(2,1)S(1)}, u32[]{:S(2)}, u32[]{:S(2)}) %all-to-all-start.3) | async-done | bytes 98336 | tf_op jit(solution)/shard_map/all_to_all | solution.py:16
  153.0 2.1 %collective-permute-start.4 = (bf16[64,256]{1,0:T(8,128)(2,1)S(1)}, bf16[64,256]{1,0:T(8,128)(2,1)S(1)}, u32[]{:S(2)}, u32[]{:S(2)}) collective-permute-start(bf16[64,256]{1,0:T(8,128)(2,1)S(1)} %dynamic-slice_convert_fusion), channel_id=1, source_target_pairs={{0,1},{1,0},{2,3},{3,2},{4,5},{5,4},{6,7},{7,6},{8,9},{9,8},{10,11... | collective-permute-start | bytes 98312 | tf_op jit(solution)/shard_map/ppermute | solution.py:25
  155.2 3.6 %collective-permute-done.4 = bf16[64,256]{1,0:T(8,128)(2,1)S(1)} collective-permute-done((bf16[64,256]{1,0:T(8,128)(2,1)S(1)}, bf16[64,256]{1,0:T(8,128)(2,1)S(1)}, u32[]{:S(2)}, u32[]{:S(2)}) %collective-permute-start.4) | collective-permute-done | bytes 32800 | tf_op jit(solution)/shard_map/ppermute | solution.py:25
  (67 shorter events, 13.9 us)
Async XLA Ops:
  0.0 83.0 %copy-start = (bf16[2048,32]{0,1:T(8,128)(2,1)S(1)}, bf16[2048,32]{0,1:T(8,128)(2,1)}, u32[]{:S(2)}) copy-start(bf16[2048,32]{0,1:T(8,128)(2,1)} %param.18) | copy-start | bytes 393220
  4.9 16.8 %copy-start.2 = (bf16[1,2048,176]{1,2,0:T(8,128)(2,1)S(1)}, bf16[1,2048,176]{1,2,0:T(8,128)(2,1)}, u32[]{:S(2)}) copy-start(bf16[1,2048,176]{1,2,0:T(8,128)(2,1)} %param.16) | copy-start | bytes 2162692
  4.9 16.9 %copy-start.1 = (bf16[1,2048,176]{1,2,0:T(8,128)(2,1)S(1)}, bf16[1,2048,176]{1,2,0:T(8,128)(2,1)}, u32[]{:S(2)}) copy-start(bf16[1,2048,176]{1,2,0:T(8,128)(2,1)} %param.15) | copy-start | bytes 2162692
  6.2 15.6 %copy-start.3 = (bf16[1,176,2048]{2,1,0:T(8,128)(2,1)S(1)}, bf16[1,176,2048]{2,1,0:T(8,128)(2,1)}, u32[]{:S(2)}) copy-start(bf16[1,176,2048]{2,1,0:T(8,128)(2,1)} %param.17) | copy-start | bytes 2162692
  6.2 48.5 %all-to-all-start = ((bf16[24,16,1024]{2,1,0:T(8,128)(2,1)}), bf16[24,16,1024]{2,1,0:T(8,128)(2,1)S(1)}, u32[]{:S(2)}, u32[]{:S(2)}) async-start(bf16[24,16,1024]{2,1,0:T(8,128)(2,1)} %bitcast.66), calls=%async_computation | async-start | bytes 1572864 | tf_op jit(solution)/shard_map/all_to_all | solution.py:16
  23.0 38.5 %collective-permute-start.2 = (bf16[288,2048]{1,0:T(8,128)(2,1)}, bf16[288,2048]{1,0:T(8,128)(2,1)}, u32[]{:S(2)}, u32[]{:S(2)}) collective-permute-start(bf16[288,2048]{1,0:T(8,128)(2,1)} %pad_maximum_fusion), channel_id=1, source_target_pairs={{0,1},{1,0},{2,3},{3,2},{4,5},{5,4},{6,7},{7,6},{8,9},{9,8},{10,11... | collective-permute-start | bytes 3538952 | tf_op jit(solution)/shard_map/ppermute | solution.py:25
  26.6 34.9 %collective-permute-start.3 = (bf16[240,2048]{1,0:T(8,128)(2,1)}, bf16[240,2048]{1,0:T(8,128)(2,1)}, u32[]{:S(2)}, u32[]{:S(2)}) collective-permute-start(bf16[240,2048]{1,0:T(8,128)(2,1)} %pad_maximum_fusion.1), channel_id=1, source_target_pairs={{0,3},{1,2},{2,1},{3,0},{4,7},{5,6},{6,5},{7,4},{8,11},{9,10},{10,... | collective-permute-start | bytes 2949128 | tf_op jit(solution)/shard_map/ppermute | solution.py:25
  54.8 11.3 %collective-permute-start = (bf16[384,512]{1,0:T(8,128)(2,1)S(1)}, bf16[384,512]{1,0:T(8,128)(2,1)S(1)}, u32[]{:S(2)}, u32[]{:S(2)}) collective-permute-start(bf16[384,512]{1,0:T(8,128)(2,1)S(1)} %get-tuple-element.6), channel_id=1, source_target_pairs={{0,4},{1,5},{2,6},{3,7},{4,8},{5,9},{6,10},{7,11},{8,12},{9,13},{1... | collective-permute-start | bytes 1179656 | tf_op jit(solution)/shard_map/ppermute | solution.py:25
  59.5 11.9 %collective-permute-start.1 = (bf16[384,512]{1,0:T(8,128)(2,1)S(1)}, bf16[384,512]{1,0:T(8,128)(2,1)S(1)}, u32[]{:S(2)}, u32[]{:S(2)}) collective-permute-start(bf16[384,512]{1,0:T(8,128)(2,1)S(1)} %get-tuple-element.5), channel_id=1, source_target_pairs={{0,28},{1,29},{2,30},{3,31},{4,0},{5,1},{6,2},{7,3},{8,4},{9,5},{1... | collective-permute-start | bytes 1179656 | tf_op jit(solution)/shard_map/ppermute | solution.py:25
  78.0 5.0 %copy-start.8 = (bf16[32,2048]{1,0:T(8,128)(2,1)S(1)}, bf16[32,2048]{1,0:T(8,128)(2,1)}, u32[]{:S(2)}) copy-start(bf16[32,2048]{1,0:T(8,128)(2,1)} %param.20) | copy-start | bytes 393220
  78.0 5.0 %copy-start.5 = (bf16[256,2048]{1,0:T(8,128)(2,1)S(1)}, bf16[256,2048]{1,0:T(8,128)(2,1)}, u32[]{:S(2)}) copy-start(bf16[256,2048]{1,0:T(8,128)(2,1)} %copy-done.4) | copy-start | bytes 3145732
  78.0 30.3 %all-to-all-start.1 = ((bf16[4,4,384,128]{3,2,1,0:T(8,128)(2,1)}), bf16[4,4,384,128]{3,2,1,0:T(8,128)(2,1)S(1)}, u32[]{:S(2)}, u32[]{:S(2)}) async-start(bf16[4,4,384,128]{3,2,1,0:T(8,128)(2,1)} %ffn.1), calls=%async_computation.1 | async-start | bytes 3145728 | tf_op jit(solution)/shard_map/all_to_all | solution.py:16
  84.6 28.8 %collective-permute-start.7 = (bf16[512,256]{1,0:T(8,128)(2,1)S(1)}, bf16[512,256]{1,0:T(8,128)(2,1)S(1)}, u32[]{:S(2)}, u32[]{:S(2)}) collective-permute-start(bf16[512,256]{1,0:T(8,128)(2,1)S(1)} %convolution_convert_fusion.1), channel_id=1, source_target_pairs={{0,28},{1,29},{2,30},{3,31},{4,0},{5,1},{6,2},{7,3},{8,4},{9,5},{1... | collective-permute-start | bytes 786440 | tf_op jit(solution)/shard_map/ppermute | solution.py:25
  86.8 26.7 %collective-permute-start.6 = (bf16[512,256]{1,0:T(8,128)(2,1)S(1)}, bf16[512,256]{1,0:T(8,128)(2,1)S(1)}, u32[]{:S(2)}, u32[]{:S(2)}) collective-permute-start(bf16[512,256]{1,0:T(8,128)(2,1)S(1)} %convolution_convert_fusion.2), channel_id=1, source_target_pairs={{0,8},{1,9},{2,10},{3,11},{4,12},{5,13},{6,14},{7,15},{8,16},{9,17... | collective-permute-start | bytes 786440 | tf_op jit(solution)/shard_map/ppermute | solution.py:25
  88.7 24.7 %copy-start.9 = (f32[256,2]{0,1:T(2,128)S(1)}, f32[256,2]{0,1:T(2,128)}, u32[]{:S(2)}) copy-start(f32[256,2]{0,1:T(2,128)} %param.14) | copy-start | bytes 6148
  89.0 31.8 %collective-permute-start.5 = (bf16[512,256]{1,0:T(8,128)(2,1)S(1)}, bf16[512,256]{1,0:T(8,128)(2,1)S(1)}, u32[]{:S(2)}, u32[]{:S(2)}) collective-permute-start(bf16[512,256]{1,0:T(8,128)(2,1)S(1)} %convolution_convert_fusion.3), channel_id=1, source_target_pairs={{0,4},{1,5},{2,6},{3,7},{4,8},{5,9},{6,10},{7,11},{8,12},{9,13},{1... | collective-permute-start | bytes 786440 | tf_op jit(solution)/shard_map/ppermute | solution.py:25
  109.3 23.5 %all-to-all-start.2 = ((bf16[4,384,128]{2,1,0:T(8,128)(2,1)}), bf16[4,384,128]{2,1,0:T(8,128)(2,1)S(1)}, u32[]{:S(2)}, u32[]{:S(2)}) async-start(bf16[4,384,128]{2,1,0:T(8,128)(2,1)} %fusion.7), calls=%async_computation.2 | async-start | bytes 786432 | tf_op jit(solution)/shard_map/all_to_all | solution.py:16
  120.8 34.3 %copy-start.10 = (f32[64]{0:T(128)S(1)}, f32[64]{0:T(128)}, u32[]{:S(2)}) copy-start(f32[64]{0:T(128)} %param.21) | copy-start | bytes 772
  121.1 19.9 %collective-permute-start.10 = (bf16[2,64,256]{2,1,0:T(8,128)(2,1)S(1)}, bf16[2,64,256]{2,1,0:T(8,128)(2,1)S(1)}, u32[]{:S(2)}, u32[]{:S(2)}) collective-permute-start(bf16[2,64,256]{2,1,0:T(8,128)(2,1)S(1)} %get-tuple-element.8), channel_id=1, source_target_pairs={{0,3},{1,0},{2,1},{3,2},{4,7},{5,4},{6,5},{7,6},{8,11},{9,8},{10,9... | collective-permute-start | bytes 196616 | tf_op jit(solution)/shard_map/ppermute | solution.py:25
  124.5 16.6 %collective-permute-start.9 = (bf16[2,64,256]{2,1,0:T(8,128)(2,1)S(1)}, bf16[2,64,256]{2,1,0:T(8,128)(2,1)S(1)}, u32[]{:S(2)}, u32[]{:S(2)}) collective-permute-start(bf16[2,64,256]{2,1,0:T(8,128)(2,1)S(1)} %get-tuple-element.9), channel_id=1, source_target_pairs={{0,2},{1,3},{2,0},{3,1},{4,6},{5,7},{6,4},{7,5},{8,10},{9,11},{10,... | collective-permute-start | bytes 196616 | tf_op jit(solution)/shard_map/ppermute | solution.py:25
  129.0 12.0 %collective-permute-start.8 = (bf16[2,64,256]{2,1,0:T(8,128)(2,1)S(1)}, bf16[2,64,256]{2,1,0:T(8,128)(2,1)S(1)}, u32[]{:S(2)}, u32[]{:S(2)}) collective-permute-start(bf16[2,64,256]{2,1,0:T(8,128)(2,1)S(1)} %get-tuple-element.7), channel_id=1, source_target_pairs={{0,1},{1,2},{2,3},{3,0},{4,5},{5,6},{6,7},{7,4},{8,9},{9,10},{10,1... | collective-permute-start | bytes 196616 | tf_op jit(solution)/shard_map/ppermute | solution.py:25
  133.5 19.0 %all-to-all-start.3 = ((bf16[24,16,128]{2,1,0:T(8,128)(2,1)}), bf16[24,16,128]{2,1,0:T(8,128)(2,1)S(1)}, u32[]{:S(2)}, u32[]{:S(2)}) async-start(bf16[24,16,128]{2,1,0:T(8,128)(2,1)} %bitcast.19), calls=%async_computation.3 | async-start | bytes 196608 | tf_op jit(solution)/shard_map/all_to_all | solution.py:16
  141.1 14.0 %collective-permute-start.11 = (bf16[64,256]{1,0:T(8,128)(2,1)S(1)}, bf16[64,256]{1,0:T(8,128)(2,1)S(1)}, u32[]{:S(2)}, u32[]{:S(2)}) collective-permute-start(bf16[64,256]{1,0:T(8,128)(2,1)S(1)} %dynamic-slice_bitcast_fusion.3), channel_id=1, source_target_pairs={{0,16},{1,17},{2,18},{3,19},{4,20},{5,21},{6,22},{7,23},{8,24},{9,... | collective-permute-start | bytes 98312 | tf_op jit(solution)/shard_map/ppermute | solution.py:25
  153.0 5.8 %collective-permute-start.4 = (bf16[64,256]{1,0:T(8,128)(2,1)S(1)}, bf16[64,256]{1,0:T(8,128)(2,1)S(1)}, u32[]{:S(2)}, u32[]{:S(2)}) collective-permute-start(bf16[64,256]{1,0:T(8,128)(2,1)S(1)} %dynamic-slice_convert_fusion), channel_id=1, source_target_pairs={{0,1},{1,0},{2,3},{3,2},{4,5},{5,4},{6,7},{7,6},{8,9},{9,8},{10,11... | collective-permute-start | bytes 98312 | tf_op jit(solution)/shard_map/ppermute | solution.py:25
  (3 other events, 6.1 us)

commit v5 on v4

--- a/solution.py
+++ b/solution.py
@@ -60,59 +60,70 @@
     )
 
 
+def landed_kernel(odd_y, rows, gate, up, first, second, *outs):
+    width = rows.shape[1]
+    columns_of = pl.ds(pl.multiple_of(odd_y[0] * width, 128), width)
+    for ref, out in zip((gate, up, first, second), outs):
+        out[...] = dot(ref[pl.ds(0, out.shape[0]), columns_of], rows[...], 1, 1)
+
+
 def ffn_kernel(
-    place, near_rows, below, above, gate, up, down, first, second, out
+    odd_y, below, above, gate, up, down, first, second, act_0, act_1, act_2, act_3, out
 ):
-    odd_y = place[0]
-    width = near_rows.shape[1]
-    half = width // 2
-    near = pl.multiple_of(odd_y * width, 128)
-    beside = pl.multiple_of((1 - odd_y) * width, 128)
-
-    def product(ref, start, count):
-        rows = pl.ds(start, count)
-        return (
-            dot(near_rows[...], ref[rows, pl.ds(near, width)], 1, 1)
-            + dot(below[...], ref[rows, pl.ds(beside, half)], 1, 1)
-            + dot(above[...], ref[rows, pl.ds(pl.multiple_of(beside + half, 128), half)], 1, 1)
-        )
-
-    pieces = []
-    own = gate.shape[0]
-    hidden = silu_times(product(gate, 0, own), product(up, 0, own))
-    pieces.append((hidden, down, 0, own))
-    for ref in (first, second):
+    half = below.shape[1]
+    beside = (1 - odd_y[0]) * 2 * half
+    low = pl.ds(pl.multiple_of(beside, 128), half)
+    high = pl.ds(pl.multiple_of(beside + half, 128), half)
+
+    def with_beside(act, ref):
+        rows = pl.ds(0, act.shape[0])
+        return act[...] + dot(ref[rows, low], below[...], 1, 1) + dot(ref[rows, high], above[...], 1, 1)
+
+    hidden = [silu_times(with_beside(act_0, gate), with_beside(act_1, up))]
+    downs = [(down, 0, down.shape[0])]
+    for act, ref in ((act_2, first), (act_3, second)):
         count = ref.shape[0] // 3
-        hidden = silu_times(product(ref, 0, count), product(ref, count, count))
-        pieces.append((hidden, ref, 2 * count, count))
+        both = with_beside(act, ref)
+        hidden.append(silu_times(both[:count], both[count:]))
+        downs.append((ref, 2 * count, count))
+    hidden = jnp.concatenate(hidden, axis=0)
     for q in range(4):
         for y_bit in range(2):
             columns_of = pl.ds((2 * q + y_bit) * 256, 256)
-            total = sum(
-                dot(hidden, ref[pl.ds(start, count), columns_of], 1, 0)
-                for hidden, ref, start, count in pieces
-            ).astype(jnp.bfloat16)
+            weights = [ref[pl.ds(start, count), columns_of] for ref, start, count in downs]
+            total = dot(hidden, jnp.concatenate(weights, axis=0), 0, 0).astype(jnp.bfloat16)
             for x_bit in range(2):
                 out[2 * y_bit + x_bit, q] = total[:, x_bit * 128 : (x_bit + 1) * 128]
 
 
-def ffn(place, near_rows, below, above, gate, up, down, first, second):
-    rows = near_rows.shape[0]
+def on_core(kernel, flops, moved, out_shape, *operands):
     in_vmem = pl.BlockSpec(memory_space=pltpu.VMEM)
+    return pl.pallas_call(
+        kernel,
+        out_shape=out_shape,
+        in_specs=[pl.BlockSpec(memory_space=pltpu.SMEM)] + [in_vmem] * (len(operands) - 1),
+        out_specs=jax.tree.map(lambda _: in_vmem, out_shape),
+        cost_estimate=pl.CostEstimate(flops=flops, bytes_accessed=moved, transcendentals=0),
+        compiler_params=pltpu.CompilerParams(vmem_limit_bytes=24 * 1024 * 1024),
+    )(*operands)
+
+
+def acts_of_landed(odd_y, rows, gate, up, first, second):
+    counts = (gate.shape[0], up.shape[0], first.shape[0] // 3 * 2, second.shape[0] // 3 * 2)
+    shapes = [jax.ShapeDtypeStruct((count, rows.shape[0]), jnp.float32) for count in counts]
+    flops = 2 * rows.size * sum(counts)
+    return on_core(
+        landed_kernel, flops, 6 * rows.size, shapes, odd_y, rows, gate, up, first, second
+    )
+
+
+def ffn(odd_y, below, above, gate, up, down, first, second, acts):
+    rows = below.shape[0]
     units = gate.shape[0] + (first.shape[0] + second.shape[0]) // 3
-    return pl.pallas_call(
-        ffn_kernel,
-        out_shape=jax.ShapeDtypeStruct((4, 4, rows, down.shape[1] // 16), jnp.bfloat16),
-        in_specs=[pl.BlockSpec(memory_space=pltpu.SMEM)] + [in_vmem] * 8,
-        out_specs=in_vmem,
-        cost_estimate=pl.CostEstimate(
-            flops=6 * rows * units * down.shape[1],
-            bytes_accessed=2 * down.shape[1] * (3 * units + 2 * rows),
-            transcendentals=rows * units,
-        ),
-        compiler_params=pltpu.CompilerParams(vmem_limit_bytes=24 * 1024 * 1024),
-        name="ffn",
-    )(place, near_rows, below, above, gate, up, down, first, second)
+    shape = jax.ShapeDtypeStruct((4, 4, rows, down.shape[1] // 16), jnp.bfloat16)
+    flops = 4 * rows * units * down.shape[1]
+    operands = (odd_y, below, above, gate, up, down, first, second, *acts)
+    return on_core(ffn_kernel, flops, 6 * units * down.shape[1], shape, *operands)
 
 
 def local(
@@ -195,7 +206,8 @@
 
     arrived = [send(landed[:, :wide], along_y(1)), send(landed[:, wide:], along_y(-1))]
 
-    partial = ffn(odd_y[None], landed, *arrived, gate_t, up_t, down, first_w, second_w)
+    acts = acts_of_landed(odd_y[None], landed, gate_t, up_t, first_w, second_w)
+    partial = ffn(odd_y[None], *arrived, gate_t, up_t, down, first_w, second_w, acts)
     near_terms = exchange(partial, ("yc", "xh"))
     near_sum = total_of([near_terms[k] for k in range(4)])
     far_terms = exchange(near_sum, ("ya", "yb"))

time: 160 us -> 160 us (level)
  waiting for transfers between devices: 68.6 us -> 65 us
    ppermute x12, waiting for transfers between devices: 21 us -> 18.5 us  [send(): return lax.ppermute(value, TP, pairs)]
    pallas_call x1 -> x2, Pallas kernels: 6.56 us -> 6.87 us  [on_core(): pl.pallas_call(kernel, out_shape=out_shape, in_specs=[pl.BlockSpec(memory...]
  transfers between devices with their start and end apart: 16 -> 16, of which waited for: 7 -> 7; matrix products, arithmetic and copies ran while one was open for 4% -> 6% of each run, Pallas kernels for 0% -> 2%
where the time goes in v5:
time: 160 us; the launch traced here: 159 us
  starting transfers between devices  70.1 us (44%)
  waiting for transfers between devices  65 us (41%)
  other arithmetic  9.3 us (6%)
  Pallas kernels  6.87 us (4%)
  matrix products  4.74 us (3%)
  local copies, waits for them, and re-layouts  1.96 us (1%)
    all_to_all x4, waiting for transfers between devices, exchange(): return lax.all_to_all(blocks, axes, split_axis=0, concat_axis=0, tiled=True)  46.5 us
    ppermute x12, starting transfers between devices, send(): return lax.ppermute(value, TP, pairs)  37.7 us
    all_to_all x4, starting transfers between devices, exchange(): return lax.all_to_all(blocks, axes, split_axis=0, concat_axis=0, tiled=True)  32.4 us
    ppermute x12, waiting for transfers between devices, send(): return lax.ppermute(value, TP, pairs)  18.5 us
    pallas_call x2, Pallas kernels, on_core(): pl.pallas_call(kernel, out_shape=out_shape, in_specs=[pl.BlockSpec(memory...  6.87 us
    dot_general x10, matrix products, dot(): lax.dot_general(left, right, (((left_dim,), (right_dim,)), ((), ())), pre...  4.74 us
  transfers between devices with their start and end apart: 16, of which 7 were waited for; matrix products, arithmetic and copies ran while one was open for 6% of the time, Pallas kernels for 2%

profile of v5, /device:TPU:26, one launch (start us, length us, event | category | flops | bytes accessed | tf_op | source)
XLA Modules:
  0.0 158.5 jit_solution(10456841072761629636)
XLA Ops:
  6.3 15.5 %all-to-all-start = ((bf16[24,16,1024]{2,1,0:T(8,128)(2,1)}), bf16[24,16,1024]{2,1,0:T(8,128)(2,1)S(1)}, u32[]{:S(2)}, u32[]{:S(2)}) async-start(bf16[24,16,1024]{2,1,0:T(8,128)(2,1)} %bitcast.68), calls=%async_computation | async-start | bytes 1572864 | tf_op jit(solution)/shard_map/all_to_all | solution.py:16
  23.1 2.4 %collective-permute-start.2 = (bf16[288,2048]{1,0:T(8,128)(2,1)}, bf16[288,2048]{1,0:T(8,128)(2,1)S(1)}, u32[]{:S(2)}, u32[]{:S(2)}) collective-permute-start(bf16[288,2048]{1,0:T(8,128)(2,1)} %pad_maximum_fusion), channel_id=1, source_target_pairs={{0,1},{1,0},{2,3},{3,2},{4,5},{5,4},{6,7},{7,6},{8,9},{9,8},{10,11... | collective-permute-start | bytes 3538952 | tf_op jit(solution)/shard_map/ppermute | solution.py:25
  27.6 4.1 %collective-permute-start.3 = (bf16[240,2048]{1,0:T(8,128)(2,1)}, bf16[240,2048]{1,0:T(8,128)(2,1)}, u32[]{:S(2)}, u32[]{:S(2)}) collective-permute-start(bf16[240,2048]{1,0:T(8,128)(2,1)} %pad_maximum_fusion.1), channel_id=1, source_target_pairs={{0,3},{1,2},{2,1},{3,0},{4,7},{5,6},{6,5},{7,4},{8,11},{9,10},{10,... | collective-permute-start | bytes 2949128 | tf_op jit(solution)/shard_map/ppermute | solution.py:25
  31.7 23.1 %all-to-all-done = bf16[24,16,1024]{2,1,0:T(8,128)(2,1)S(1)} async-done(((bf16[24,16,1024]{2,1,0:T(8,128)(2,1)}), bf16[24,16,1024]{2,1,0:T(8,128)(2,1)S(1)}, u32[]{:S(2)}, u32[]{:S(2)}) %all-to-all-start) | async-done | bytes 786464 | tf_op jit(solution)/shard_map/all_to_all | solution.py:16
  54.9 4.7 %collective-permute-start = (bf16[384,512]{1,0:T(8,128)(2,1)S(1)}, bf16[384,512]{1,0:T(8,128)(2,1)S(1)}, u32[]{:S(2)}, u32[]{:S(2)}) collective-permute-start(bf16[384,512]{1,0:T(8,128)(2,1)S(1)} %get-tuple-element.14), channel_id=1, source_target_pairs={{0,4},{1,5},{2,6},{3,7},{4,8},{5,9},{6,10},{7,11},{8,12},{9,13},{1... | collective-permute-start | bytes 1179656 | tf_op jit(solution)/shard_map/ppermute | solution.py:25
  59.6 1.9 %collective-permute-start.1 = (bf16[384,512]{1,0:T(8,128)(2,1)S(1)}, bf16[384,512]{1,0:T(8,128)(2,1)S(1)}, u32[]{:S(2)}, u32[]{:S(2)}) collective-permute-start(bf16[384,512]{1,0:T(8,128)(2,1)S(1)} %get-tuple-element.13), channel_id=1, source_target_pairs={{0,28},{1,29},{2,30},{3,31},{4,0},{5,1},{6,2},{7,3},{8,4},{9,5},{1... | collective-permute-start | bytes 1179656 | tf_op jit(solution)/shard_map/ppermute | solution.py:25
  61.5 2.4 %shard_map.109 = (f32[176,384]{1,0:T(8,128)S(1)}, f32[176,384]{1,0:T(8,128)S(1)}, f32[192,384]{1,0:T(8,128)S(1)}, f32[160,384]{1,0:T(8,128)S(1)}) custom-call(s32[1]{0:T(128)} %bitcast.2.odd_y, bf16[384,1024]{1,0:T(8,128)(2,1)S(1)} %bitcast.58, bf16[176,2048]{1,0:T(8,128)(2,1)S(1)} %bitcast.61, bf16[176,2048]{1,0:T(8,128)(2,1)S(1)} %bitcast.65, ...), custom_call_target="tpu_custom_call" | custom-call | flops 553648128 | bytes 2359296 | tf_op jit(solution)/shard_map/pallas_call | solution.py:101
  64.0 2.2 %collective-permute-done.below = bf16[384,512]{1,0:T(8,128)(2,1)S(1)} collective-permute-done((bf16[384,512]{1,0:T(8,128)(2,1)S(1)}, bf16[384,512]{1,0:T(8,128)(2,1)S(1)}, u32[]{:S(2)}, u32[]{:S(2)}) %collective-permute-start) | collective-permute-done | bytes 393248 | tf_op jit(solution)/shard_map/ppermute | solution.py:25
  66.2 5.3 %collective-permute-done.1.above = bf16[384,512]{1,0:T(8,128)(2,1)S(1)} collective-permute-done((bf16[384,512]{1,0:T(8,128)(2,1)S(1)}, bf16[384,512]{1,0:T(8,128)(2,1)S(1)}, u32[]{:S(2)}, u32[]{:S(2)}) %collective-permute-start.1) | collective-permute-done | bytes 393248 | tf_op jit(solution)/shard_map/ppermute | solution.py:25
  71.5 4.5 %shard_map.110 = bf16[4,4,384,128]{3,2,1,0:T(8,128)(2,1)} custom-call(s32[1]{0:T(128)} %bitcast.2.odd_y, bf16[384,512]{1,0:T(8,128)(2,1)S(1)} %collective-permute-done.below, bf16[384,512]{1,0:T(8,128)(2,1)S(1)} %collective-permute-done.1.above, bf16[176,2048]{1,0:T(8,128)(2,1)S(1)} %bitcast.62, bf16[176,2048]{1,0:T(8,128)(2,1)S(1)} %bitcast.66, ...), custom_call_target="tpu_custom_call" | custom-call | flops 1107296256 | bytes 4325376 | tf_op jit(solution)/shard_map/pallas_call | solution.py:101
  76.0 5.0 %all-to-all-start.1 = ((bf16[4,4,384,128]{3,2,1,0:T(8,128)(2,1)}), bf16[4,4,384,128]{3,2,1,0:T(8,128)(2,1)S(1)}, u32[]{:S(2)}, u32[]{:S(2)}) async-start(bf16[4,4,384,128]{3,2,1,0:T(8,128)(2,1)} %shard_map.110), calls=%async_computation.1 | async-start | bytes 3145728 | tf_op jit(solution)/shard_map/all_to_all | solution.py:16
  82.7 1.9 %collective-permute-start.7 = (bf16[512,256]{1,0:T(8,128)(2,1)S(1)}, bf16[512,256]{1,0:T(8,128)(2,1)S(1)}, u32[]{:S(2)}, u32[]{:S(2)}) collective-permute-start(bf16[512,256]{1,0:T(8,128)(2,1)S(1)} %convolution_convert_fusion.1), channel_id=1, source_target_pairs={{0,28},{1,29},{2,30},{3,31},{4,0},{5,1},{6,2},{7,3},{8,4},{9,5},{1... | collective-permute-start | bytes 786440 | tf_op jit(solution)/shard_map/ppermute | solution.py:25
  84.9 1.9 %collective-permute-start.6 = (bf16[512,256]{1,0:T(8,128)(2,1)S(1)}, bf16[512,256]{1,0:T(8,128)(2,1)S(1)}, u32[]{:S(2)}, u32[]{:S(2)}) collective-permute-start(bf16[512,256]{1,0:T(8,128)(2,1)S(1)} %convolution_convert_fusion.2), channel_id=1, source_target_pairs={{0,8},{1,9},{2,10},{3,11},{4,12},{5,13},{6,14},{7,15},{8,16},{9,17... | collective-permute-start | bytes 786440 | tf_op jit(solution)/shard_map/ppermute | solution.py:25
  87.1 5.1 %collective-permute-start.5 = (bf16[512,256]{1,0:T(8,128)(2,1)S(1)}, bf16[512,256]{1,0:T(8,128)(2,1)}, u32[]{:S(2)}, u32[]{:S(2)}) collective-permute-start(bf16[512,256]{1,0:T(8,128)(2,1)S(1)} %convolution_convert_fusion.3), channel_id=1, source_target_pairs={{0,4},{1,5},{2,6},{3,7},{4,8},{5,9},{6,10},{7,11},{8,12},{9,13},{1... | collective-permute-start | bytes 786440 | tf_op jit(solution)/shard_map/ppermute | solution.py:25
  92.3 13.9 %all-to-all-done.1 = bf16[4,4,384,128]{3,2,1,0:T(8,128)(2,1)S(1)} async-done(((bf16[4,4,384,128]{3,2,1,0:T(8,128)(2,1)}), bf16[4,4,384,128]{3,2,1,0:T(8,128)(2,1)S(1)}, u32[]{:S(2)}, u32[]{:S(2)}) %all-to-all-start.1) | async-done | bytes 1572896 | tf_op jit(solution)/shard_map/all_to_all | solution.py:16
  107.2 4.3 %all-to-all-start.2 = ((bf16[4,384,128]{2,1,0:T(8,128)(2,1)}), bf16[4,384,128]{2,1,0:T(8,128)(2,1)S(1)}, u32[]{:S(2)}, u32[]{:S(2)}) async-start(bf16[4,384,128]{2,1,0:T(8,128)(2,1)} %fusion.7), calls=%async_computation.2 | async-start | bytes 786432 | tf_op jit(solution)/shard_map/all_to_all | solution.py:16
  111.5 7.3 %collective-permute-done.5 = bf16[512,256]{1,0:T(8,128)(2,1)} collective-permute-done((bf16[512,256]{1,0:T(8,128)(2,1)S(1)}, bf16[512,256]{1,0:T(8,128)(2,1)}, u32[]{:S(2)}, u32[]{:S(2)}) %collective-permute-start.5) | collective-permute-done | bytes 262176 | tf_op jit(solution)/shard_map/ppermute | solution.py:25
  120.2 3.3 %collective-permute-start.10 = (bf16[2,64,256]{2,1,0:T(8,128)(2,1)S(1)}, bf16[2,64,256]{2,1,0:T(8,128)(2,1)S(1)}, u32[]{:S(2)}, u32[]{:S(2)}) collective-permute-start(bf16[2,64,256]{2,1,0:T(8,128)(2,1)S(1)} %get-tuple-element.16), channel_id=1, source_target_pairs={{0,3},{1,0},{2,1},{3,2},{4,7},{5,4},{6,5},{7,6},{8,11},{9,8},{10,9... | collective-permute-start | bytes 196616 | tf_op jit(solution)/shard_map/ppermute | solution.py:25
  123.5 4.5 %collective-permute-start.9 = (bf16[2,64,256]{2,1,0:T(8,128)(2,1)S(1)}, bf16[2,64,256]{2,1,0:T(8,128)(2,1)S(1)}, u32[]{:S(2)}, u32[]{:S(2)}) collective-permute-start(bf16[2,64,256]{2,1,0:T(8,128)(2,1)S(1)} %get-tuple-element.17), channel_id=1, source_target_pairs={{0,2},{1,3},{2,0},{3,1},{4,6},{5,7},{6,4},{7,5},{8,10},{9,11},{10,... | collective-permute-start | bytes 196616 | tf_op jit(solution)/shard_map/ppermute | solution.py:25
  128.1 3.7 %collective-permute-start.8 = (bf16[2,64,256]{2,1,0:T(8,128)(2,1)S(1)}, bf16[2,64,256]{2,1,0:T(8,128)(2,1)S(1)}, u32[]{:S(2)}, u32[]{:S(2)}) collective-permute-start(bf16[2,64,256]{2,1,0:T(8,128)(2,1)S(1)} %get-tuple-element.15), channel_id=1, source_target_pairs={{0,1},{1,2},{2,3},{3,0},{4,5},{5,6},{6,7},{7,4},{8,9},{9,10},{10,1... | collective-permute-start | bytes 196616 | tf_op jit(solution)/shard_map/ppermute | solution.py:25
  132.5 7.6 %all-to-all-start.3 = ((bf16[24,16,128]{2,1,0:T(8,128)(2,1)}), bf16[24,16,128]{2,1,0:T(8,128)(2,1)S(1)}, u32[]{:S(2)}, u32[]{:S(2)}) async-start(bf16[24,16,128]{2,1,0:T(8,128)(2,1)} %bitcast.19), calls=%async_computation.3 | async-start | bytes 196608 | tf_op jit(solution)/shard_map/all_to_all | solution.py:16
  142.1 9.5 %all-to-all-done.3 = bf16[24,16,128]{2,1,0:T(8,128)(2,1)S(1)} async-done(((bf16[24,16,128]{2,1,0:T(8,128)(2,1)}), bf16[24,16,128]{2,1,0:T(8,128)(2,1)S(1)}, u32[]{:S(2)}, u32[]{:S(2)}) %all-to-all-start.3) | async-done | bytes 98336 | tf_op jit(solution)/shard_map/all_to_all | solution.py:16
  152.0 2.1 %collective-permute-start.4 = (bf16[64,256]{1,0:T(8,128)(2,1)S(1)}, bf16[64,256]{1,0:T(8,128)(2,1)S(1)}, u32[]{:S(2)}, u32[]{:S(2)}) collective-permute-start(bf16[64,256]{1,0:T(8,128)(2,1)S(1)} %dynamic-slice_convert_fusion), channel_id=1, source_target_pairs={{0,1},{1,0},{2,3},{3,2},{4,5},{5,4},{6,7},{7,6},{8,9},{9,8},{10,11... | collective-permute-start | bytes 98312 | tf_op jit(solution)/shard_map/ppermute | solution.py:25
  154.2 3.6 %collective-permute-done.4 = bf16[64,256]{1,0:T(8,128)(2,1)S(1)} collective-permute-done((bf16[64,256]{1,0:T(8,128)(2,1)S(1)}, bf16[64,256]{1,0:T(8,128)(2,1)S(1)}, u32[]{:S(2)}, u32[]{:S(2)}) %collective-permute-start.4) | collective-permute-done | bytes 32800 | tf_op jit(solution)/shard_map/ppermute | solution.py:25
  (82 shorter events, 17.9 us)
Async XLA Ops:
  0.0 81.6 %copy-start = (bf16[2048,32]{0,1:T(8,128)(2,1)S(1)}, bf16[2048,32]{0,1:T(8,128)(2,1)}, u32[]{:S(2)}) copy-start(bf16[2048,32]{0,1:T(8,128)(2,1)} %param.18) | copy-start | bytes 393220
  4.9 16.9 %copy-start.1 = (bf16[1,2048,176]{1,2,0:T(8,128)(2,1)S(1)}, bf16[1,2048,176]{1,2,0:T(8,128)(2,1)}, u32[]{:S(2)}) copy-start(bf16[1,2048,176]{1,2,0:T(8,128)(2,1)} %param.15) | copy-start | bytes 2162692
  6.3 48.6 %all-to-all-start = ((bf16[24,16,1024]{2,1,0:T(8,128)(2,1)}), bf16[24,16,1024]{2,1,0:T(8,128)(2,1)S(1)}, u32[]{:S(2)}, u32[]{:S(2)}) async-start(bf16[24,16,1024]{2,1,0:T(8,128)(2,1)} %bitcast.68), calls=%async_computation | async-start | bytes 1572864 | tf_op jit(solution)/shard_map/all_to_all | solution.py:16
  23.1 38.5 %collective-permute-start.2 = (bf16[288,2048]{1,0:T(8,128)(2,1)}, bf16[288,2048]{1,0:T(8,128)(2,1)S(1)}, u32[]{:S(2)}, u32[]{:S(2)}) collective-permute-start(bf16[288,2048]{1,0:T(8,128)(2,1)} %pad_maximum_fusion), channel_id=1, source_target_pairs={{0,1},{1,0},{2,3},{3,2},{4,5},{5,4},{6,7},{7,6},{8,9},{9,8},{10,11... | collective-permute-start | bytes 3538952 | tf_op jit(solution)/shard_map/ppermute | solution.py:25
  27.6 33.9 %collective-permute-start.3 = (bf16[240,2048]{1,0:T(8,128)(2,1)}, bf16[240,2048]{1,0:T(8,128)(2,1)}, u32[]{:S(2)}, u32[]{:S(2)}) collective-permute-start(bf16[240,2048]{1,0:T(8,128)(2,1)} %pad_maximum_fusion.1), channel_id=1, source_target_pairs={{0,3},{1,2},{2,1},{3,0},{4,7},{5,6},{6,5},{7,4},{8,11},{9,10},{10,... | collective-permute-start | bytes 2949128 | tf_op jit(solution)/shard_map/ppermute | solution.py:25
  54.9 11.3 %collective-permute-start = (bf16[384,512]{1,0:T(8,128)(2,1)S(1)}, bf16[384,512]{1,0:T(8,128)(2,1)S(1)}, u32[]{:S(2)}, u32[]{:S(2)}) collective-permute-start(bf16[384,512]{1,0:T(8,128)(2,1)S(1)} %get-tuple-element.14), channel_id=1, source_target_pairs={{0,4},{1,5},{2,6},{3,7},{4,8},{5,9},{6,10},{7,11},{8,12},{9,13},{1... | collective-permute-start | bytes 1179656 | tf_op jit(solution)/shard_map/ppermute | solution.py:25
  59.6 11.9 %collective-permute-start.1 = (bf16[384,512]{1,0:T(8,128)(2,1)S(1)}, bf16[384,512]{1,0:T(8,128)(2,1)S(1)}, u32[]{:S(2)}, u32[]{:S(2)}) collective-permute-start(bf16[384,512]{1,0:T(8,128)(2,1)S(1)} %get-tuple-element.13), channel_id=1, source_target_pairs={{0,28},{1,29},{2,30},{3,31},{4,0},{5,1},{6,2},{7,3},{8,4},{9,5},{1... | collective-permute-start | bytes 1179656 | tf_op jit(solution)/shard_map/ppermute | solution.py:25
  76.0 30.2 %all-to-all-start.1 = ((bf16[4,4,384,128]{3,2,1,0:T(8,128)(2,1)}), bf16[4,4,384,128]{3,2,1,0:T(8,128)(2,1)S(1)}, u32[]{:S(2)}, u32[]{:S(2)}) async-start(bf16[4,4,384,128]{3,2,1,0:T(8,128)(2,1)} %shard_map.110), calls=%async_computation.1 | async-start | bytes 3145728 | tf_op jit(solution)/shard_map/all_to_all | solution.py:16
  82.7 28.8 %collective-permute-start.7 = (bf16[512,256]{1,0:T(8,128)(2,1)S(1)}, bf16[512,256]{1,0:T(8,128)(2,1)S(1)}, u32[]{:S(2)}, u32[]{:S(2)}) collective-permute-start(bf16[512,256]{1,0:T(8,128)(2,1)S(1)} %convolution_convert_fusion.1), channel_id=1, source_target_pairs={{0,28},{1,29},{2,30},{3,31},{4,0},{5,1},{6,2},{7,3},{8,4},{9,5},{1... | collective-permute-start | bytes 786440 | tf_op jit(solution)/shard_map/ppermute | solution.py:25
  84.9 26.6 %collective-permute-start.6 = (bf16[512,256]{1,0:T(8,128)(2,1)S(1)}, bf16[512,256]{1,0:T(8,128)(2,1)S(1)}, u32[]{:S(2)}, u32[]{:S(2)}) collective-permute-start(bf16[512,256]{1,0:T(8,128)(2,1)S(1)} %convolution_convert_fusion.2), channel_id=1, source_target_pairs={{0,8},{1,9},{2,10},{3,11},{4,12},{5,13},{6,14},{7,15},{8,16},{9,17... | collective-permute-start | bytes 786440 | tf_op jit(solution)/shard_map/ppermute | solution.py:25
  86.8 24.7 %copy-start.16 = (f32[256,2]{0,1:T(2,128)S(1)}, f32[256,2]{0,1:T(2,128)}, u32[]{:S(2)}) copy-start(f32[256,2]{0,1:T(2,128)} %param.14) | copy-start | bytes 6148
  86.9 32.0 %copy-start.10 = (bf16[32,256]{1,0:T(8,128)(2,1)S(1)}, bf16[32,256]{1,0:T(8,128)(2,1)}, u32[]{:S(2)}) copy-start(bf16[32,256]{1,0:T(8,128)(2,1)} %get-tuple-element.18) | copy-start | bytes 49156
  86.9 32.0 %copy-start.11 = (bf16[32,256]{1,0:T(8,128)(2,1)S(1)}, bf16[32,256]{1,0:T(8,128)(2,1)}, u32[]{:S(2)}) copy-start(bf16[32,256]{1,0:T(8,128)(2,1)} %get-tuple-element.23) | copy-start | bytes 49156
  87.1 31.7 %collective-permute-start.5 = (bf16[512,256]{1,0:T(8,128)(2,1)S(1)}, bf16[512,256]{1,0:T(8,128)(2,1)}, u32[]{:S(2)}, u32[]{:S(2)}) collective-permute-start(bf16[512,256]{1,0:T(8,128)(2,1)S(1)} %convolution_convert_fusion.3), channel_id=1, source_target_pairs={{0,4},{1,5},{2,6},{3,7},{4,8},{5,9},{6,10},{7,11},{8,12},{9,13},{1... | collective-permute-start | bytes 786440 | tf_op jit(solution)/shard_map/ppermute | solution.py:25
  107.2 44.4 %copy-start.15 = (s32[1,256]{1,0:T(1,128)S(1)}, s32[1,256]{1,0:T(1,128)}, u32[]{:S(2)}) copy-start(s32[1,256]{1,0:T(1,128)} %copy-done.14) | copy-start | bytes 3076
  107.2 24.6 %all-to-all-start.2 = ((bf16[4,384,128]{2,1,0:T(8,128)(2,1)}), bf16[4,384,128]{2,1,0:T(8,128)(2,1)S(1)}, u32[]{:S(2)}, u32[]{:S(2)}) async-start(bf16[4,384,128]{2,1,0:T(8,128)(2,1)} %fusion.7), calls=%async_computation.2 | async-start | bytes 786432 | tf_op jit(solution)/shard_map/all_to_all | solution.py:16
  111.5 40.3 %copy-start.13 = (s32[1,256]{1,0:T(1,128)S(1)}, s32[1,256]{1,0:T(1,128)}, u32[]{:S(2)}) copy-start(s32[1,256]{1,0:T(1,128)} %copy-done.12) | copy-start | bytes 3076
  118.9 35.3 %copy-start.17 = (f32[64]{0:T(128)S(1)}, f32[64]{0:T(128)}, u32[]{:S(2)}) copy-start(f32[64]{0:T(128)} %param.21) | copy-start | bytes 772
  120.2 19.9 %collective-permute-start.10 = (bf16[2,64,256]{2,1,0:T(8,128)(2,1)S(1)}, bf16[2,64,256]{2,1,0:T(8,128)(2,1)S(1)}, u32[]{:S(2)}, u32[]{:S(2)}) collective-permute-start(bf16[2,64,256]{2,1,0:T(8,128)(2,1)S(1)} %get-tuple-element.16), channel_id=1, source_target_pairs={{0,3},{1,0},{2,1},{3,2},{4,7},{5,4},{6,5},{7,6},{8,11},{9,8},{10,9... | collective-permute-start | bytes 196616 | tf_op jit(solution)/shard_map/ppermute | solution.py:25
  123.5 16.6 %collective-permute-start.9 = (bf16[2,64,256]{2,1,0:T(8,128)(2,1)S(1)}, bf16[2,64,256]{2,1,0:T(8,128)(2,1)S(1)}, u32[]{:S(2)}, u32[]{:S(2)}) collective-permute-start(bf16[2,64,256]{2,1,0:T(8,128)(2,1)S(1)} %get-tuple-element.17), channel_id=1, source_target_pairs={{0,2},{1,3},{2,0},{3,1},{4,6},{5,7},{6,4},{7,5},{8,10},{9,11},{10,... | collective-permute-start | bytes 196616 | tf_op jit(solution)/shard_map/ppermute | solution.py:25
  128.1 12.0 %collective-permute-start.8 = (bf16[2,64,256]{2,1,0:T(8,128)(2,1)S(1)}, bf16[2,64,256]{2,1,0:T(8,128)(2,1)S(1)}, u32[]{:S(2)}, u32[]{:S(2)}) collective-permute-start(bf16[2,64,256]{2,1,0:T(8,128)(2,1)S(1)} %get-tuple-element.15), channel_id=1, source_target_pairs={{0,1},{1,2},{2,3},{3,0},{4,5},{5,6},{6,7},{7,4},{8,9},{9,10},{10,1... | collective-permute-start | bytes 196616 | tf_op jit(solution)/shard_map/ppermute | solution.py:25
  132.5 19.1 %all-to-all-start.3 = ((bf16[24,16,128]{2,1,0:T(8,128)(2,1)}), bf16[24,16,128]{2,1,0:T(8,128)(2,1)S(1)}, u32[]{:S(2)}, u32[]{:S(2)}) async-start(bf16[24,16,128]{2,1,0:T(8,128)(2,1)} %bitcast.19), calls=%async_computation.3 | async-start | bytes 196608 | tf_op jit(solution)/shard_map/all_to_all | solution.py:16
  140.1 14.0 %collective-permute-start.11 = (bf16[64,256]{1,0:T(8,128)(2,1)S(1)}, bf16[64,256]{1,0:T(8,128)(2,1)S(1)}, u32[]{:S(2)}, u32[]{:S(2)}) collective-permute-start(bf16[64,256]{1,0:T(8,128)(2,1)S(1)} %dynamic-slice_bitcast_fusion.3), channel_id=1, source_target_pairs={{0,16},{1,17},{2,18},{3,19},{4,20},{5,21},{6,22},{7,23},{8,24},{9,... | collective-permute-start | bytes 98312 | tf_op jit(solution)/shard_map/ppermute | solution.py:25
  152.0 5.8 %collective-permute-start.4 = (bf16[64,256]{1,0:T(8,128)(2,1)S(1)}, bf16[64,256]{1,0:T(8,128)(2,1)S(1)}, u32[]{:S(2)}, u32[]{:S(2)}) collective-permute-start(bf16[64,256]{1,0:T(8,128)(2,1)S(1)} %dynamic-slice_convert_fusion), channel_id=1, source_target_pairs={{0,1},{1,0},{2,3},{3,2},{4,5},{5,4},{6,7},{7,6},{8,9},{9,8},{10,11... | collective-permute-start | bytes 98312 | tf_op jit(solution)/shard_map/ppermute | solution.py:25
  (10 other events, 64.1 us)

commit v6 on v5

--- a/solution.py
+++ b/solution.py
@@ -93,7 +93,8 @@
             weights = [ref[pl.ds(start, count), columns_of] for ref, start, count in downs]
             total = dot(hidden, jnp.concatenate(weights, axis=0), 0, 0).astype(jnp.bfloat16)
             for x_bit in range(2):
-                out[2 * y_bit + x_bit, q] = total[:, x_bit * 128 : (x_bit + 1) * 128]
+                piece = total[:, x_bit * 128 : (x_bit + 1) * 128]
+                out[2 * y_bit + x_bit, :, q * 128 : (q + 1) * 128] = piece
 
 
 def on_core(kernel, flops, moved, out_shape, *operands):
@@ -120,7 +121,7 @@
 def ffn(odd_y, below, above, gate, up, down, first, second, acts):
     rows = below.shape[0]
     units = gate.shape[0] + (first.shape[0] + second.shape[0]) // 3
-    shape = jax.ShapeDtypeStruct((4, 4, rows, down.shape[1] // 16), jnp.bfloat16)
+    shape = jax.ShapeDtypeStruct((4, rows, down.shape[1] // 4), jnp.bfloat16)
     flops = 4 * rows * units * down.shape[1]
     operands = (odd_y, below, above, gate, up, down, first, second, *acts)
     return on_core(ffn_kernel, flops, 6 * units * down.shape[1], shape, *operands)
@@ -204,21 +205,23 @@
     dense_theirs = send(dense_theirs, along_y(4))
     dense_out = dense_mine.astype(jnp.float32) + dense_theirs.astype(jnp.float32)
 
-    arrived = [send(landed[:, :wide], along_y(1)), send(landed[:, wide:], along_y(-1))]
+    arrived = [
+        send(landed[:, :wide], lambda y, x: (y ^ 1, x)),
+        send(landed[:, wide:], lambda y, x: (y + (1 if y % 2 else -1), x)),
+    ]
 
     acts = acts_of_landed(odd_y[None], landed, gate_t, up_t, first_w, second_w)
     partial = ffn(odd_y[None], *arrived, gate_t, up_t, down, first_w, second_w, acts)
     near_terms = exchange(partial, ("yc", "xh"))
     near_sum = total_of([near_terms[k] for k in range(4)])
-    far_terms = exchange(near_sum, ("ya", "yb"))
-    expert_out = total_of([far_terms[k] for k in range(4)])
-    returned = exchange(expert_out.reshape(experts, few, 2 * part), "ep")
-    returned = returned.reshape(rows_mine, 2 * part)
+    returned = exchange(near_sum.reshape(experts, few, wide), "ep")
+    returned = returned.reshape(rows_mine, wide)
     weight = routing_weight.T
     routed = sum(weight[c][None, :] * dot(returned, chosen[c], 0, 0) for c in range(2))
-    keep = lax.dynamic_slice_in_dim(routed, odd_x * part, part, 0)
-    give = lax.dynamic_slice_in_dim(routed, (1 - odd_x) * part, part, 0)
-    routed = keep + send(give.astype(jnp.bfloat16), lambda y, x: (y, x ^ 1)).astype(jnp.float32)
+    pieces = exchange(
+        routed.astype(jnp.bfloat16).reshape(8, part, group_tokens), ("ya", "yb", "xl")
+    )
+    routed = pieces.astype(jnp.float32).sum(axis=0)
     gate_factor = jax.nn.sigmoid(dense_gate)[:, None]
     return (routed + gate_factor * dense_out).astype(jnp.bfloat16).T
 

time: 160 us -> 161 us (level)
  the two profiles are of different devices: /device:TPU:26 before, /device:TPU:40 now
where the time goes in v6:
time: 161 us; the launch traced here: 160 us
  starting transfers between devices  71.6 us (44%)
  waiting for transfers between devices  65.6 us (41%)
  other arithmetic  8.57 us (5%)
  Pallas kernels  6.84 us (4%)
  matrix products  4.7 us (3%)
  local copies, waits for them, and re-layouts  1.75 us (1%)
    all_to_all x4, waiting for transfers between devices, exchange(): return lax.all_to_all(blocks, axes, split_axis=0, concat_axis=0, tiled=True)  41.3 us
    all_to_all x4, starting transfers between devices, exchange(): return lax.all_to_all(blocks, axes, split_axis=0, concat_axis=0, tiled=True)  37.9 us
    ppermute x11, starting transfers between devices, send(): return lax.ppermute(value, TP, pairs)  33.7 us
    ppermute x11, waiting for transfers between devices, send(): return lax.ppermute(value, TP, pairs)  24.3 us
    pallas_call x2, Pallas kernels, on_core(): pl.pallas_call(kernel, out_shape=out_shape, in_specs=[pl.BlockSpec(memory...  6.84 us
    dot_general x10, matrix products, dot(): lax.dot_general(left, right, (((left_dim,), (right_dim,)), ((), ())), pre...  4.7 us
  transfers between devices with their start and end apart: 15, of which 8 were waited for; matrix products, arithmetic and copies ran while one was open for 4% of the time, Pallas kernels for 2%

profile of v6, /device:TPU:40, one launch (start us, length us, event | category | flops | bytes accessed | tf_op | source)
XLA Modules:
  0.0 159.5 jit_solution(16703819032617009258)
XLA Ops:
  6.2 15.5 %all-to-all-start = ((bf16[24,16,1024]{2,1,0:T(8,128)(2,1)}), bf16[24,16,1024]{2,1,0:T(8,128)(2,1)S(1)}, u32[]{:S(2)}, u32[]{:S(2)}) async-start(bf16[24,16,1024]{2,1,0:T(8,128)(2,1)} %bitcast.67), calls=%async_computation | async-start | bytes 1572864 | tf_op jit(solution)/shard_map/all_to_all | solution.py:16
  22.9 3.4 %collective-permute-start.2 = (bf16[288,2048]{1,0:T(8,128)(2,1)}, bf16[288,2048]{1,0:T(8,128)(2,1)S(1)}, u32[]{:S(2)}, u32[]{:S(2)}) collective-permute-start(bf16[288,2048]{1,0:T(8,128)(2,1)} %pad_maximum_fusion), channel_id=1, source_target_pairs={{0,1},{1,0},{2,3},{3,2},{4,5},{5,4},{6,7},{7,6},{8,9},{9,8},{10,11... | collective-permute-start | bytes 3538952 | tf_op jit(solution)/shard_map/ppermute | solution.py:25
  28.4 4.0 %collective-permute-start.3 = (bf16[240,2048]{1,0:T(8,128)(2,1)}, bf16[240,2048]{1,0:T(8,128)(2,1)}, u32[]{:S(2)}, u32[]{:S(2)}) collective-permute-start(bf16[240,2048]{1,0:T(8,128)(2,1)} %pad_maximum_fusion.1), channel_id=1, source_target_pairs={{0,3},{1,2},{2,1},{3,0},{4,7},{5,6},{6,5},{7,4},{8,11},{9,10},{10,... | collective-permute-start | bytes 2949128 | tf_op jit(solution)/shard_map/ppermute | solution.py:25
  32.4 22.3 %all-to-all-done = bf16[24,16,1024]{2,1,0:T(8,128)(2,1)S(1)} async-done(((bf16[24,16,1024]{2,1,0:T(8,128)(2,1)}), bf16[24,16,1024]{2,1,0:T(8,128)(2,1)S(1)}, u32[]{:S(2)}, u32[]{:S(2)}) %all-to-all-start) | async-done | bytes 786464 | tf_op jit(solution)/shard_map/all_to_all | solution.py:16
  54.8 3.3 %collective-permute-start = (bf16[384,512]{1,0:T(8,128)(2,1)S(1)}, bf16[384,512]{1,0:T(8,128)(2,1)S(1)}, u32[]{:S(2)}, u32[]{:S(2)}) collective-permute-start(bf16[384,512]{1,0:T(8,128)(2,1)S(1)} %get-tuple-element.14), channel_id=1, source_target_pairs={{0,4},{1,5},{2,6},{3,7},{4,0},{5,1},{6,2},{7,3},{8,12},{9,13},{10,... | collective-permute-start | bytes 1179656 | tf_op jit(solution)/shard_map/ppermute | solution.py:25
  58.1 1.9 %collective-permute-start.1 = (bf16[384,512]{1,0:T(8,128)(2,1)S(1)}, bf16[384,512]{1,0:T(8,128)(2,1)S(1)}, u32[]{:S(2)}, u32[]{:S(2)}) collective-permute-start(bf16[384,512]{1,0:T(8,128)(2,1)S(1)} %get-tuple-element.13), channel_id=1, source_target_pairs={{0,28},{1,29},{2,30},{3,31},{4,8},{5,9},{6,10},{7,11},{8,4},{9,5},... | collective-permute-start | bytes 1179656 | tf_op jit(solution)/shard_map/ppermute | solution.py:25
  60.0 2.4 %shard_map.109 = (f32[176,384]{1,0:T(8,128)S(1)}, f32[176,384]{1,0:T(8,128)S(1)}, f32[192,384]{1,0:T(8,128)S(1)}, f32[160,384]{1,0:T(8,128)S(1)}) custom-call(s32[1]{0:T(128)} %bitcast.2.odd_y, bf16[384,1024]{1,0:T(8,128)(2,1)S(1)} %bitcast.57, bf16[176,2048]{1,0:T(8,128)(2,1)S(1)} %bitcast.60, bf16[176,2048]{1,0:T(8,128)(2,1)S(1)} %bitcast.64, ...), custom_call_target="tpu_custom_call" | custom-call | flops 553648128 | bytes 2359296 | tf_op jit(solution)/shard_map/pallas_call | solution.py:102
  62.5 3.4 %collective-permute-done.below = bf16[384,512]{1,0:T(8,128)(2,1)S(1)} collective-permute-done((bf16[384,512]{1,0:T(8,128)(2,1)S(1)}, bf16[384,512]{1,0:T(8,128)(2,1)S(1)}, u32[]{:S(2)}, u32[]{:S(2)}) %collective-permute-start) | collective-permute-done | bytes 393248 | tf_op jit(solution)/shard_map/ppermute | solution.py:25
  65.8 3.0 %collective-permute-done.1.above = bf16[384,512]{1,0:T(8,128)(2,1)S(1)} collective-permute-done((bf16[384,512]{1,0:T(8,128)(2,1)S(1)}, bf16[384,512]{1,0:T(8,128)(2,1)S(1)}, u32[]{:S(2)}, u32[]{:S(2)}) %collective-permute-start.1) | collective-permute-done | bytes 393248 | tf_op jit(solution)/shard_map/ppermute | solution.py:25
  68.8 4.4 %shard_map.110 = bf16[4,384,512]{2,1,0:T(8,128)(2,1)} custom-call(s32[1]{0:T(128)} %bitcast.2.odd_y, bf16[384,512]{1,0:T(8,128)(2,1)S(1)} %collective-permute-done.below, bf16[384,512]{1,0:T(8,128)(2,1)S(1)} %collective-permute-done.1.above, bf16[176,2048]{1,0:T(8,128)(2,1)S(1)} %bitcast.61, bf16[176,2048]{1,0:T(8,128)(2,1)S(1)} %bitcast.65, ...), custom_call_target="tpu_custom_call" | custom-call | flops 1107296256 | bytes 4325376 | tf_op jit(solution)/shard_map/pallas_call | solution.py:102
  73.2 6.3 %all-to-all-start.1 = ((bf16[4,384,512]{2,1,0:T(8,128)(2,1)}), bf16[4,384,512]{2,1,0:T(8,128)(2,1)S(1)}, u32[]{:S(2)}, u32[]{:S(2)}) async-start(bf16[4,384,512]{2,1,0:T(8,128)(2,1)} %shard_map.110), calls=%async_computation.1 | async-start | bytes 3145728 | tf_op jit(solution)/shard_map/all_to_all | solution.py:16
  80.9 15.9 %all-to-all-done.1 = bf16[4,384,512]{2,1,0:T(8,128)(2,1)S(1)} async-done(((bf16[4,384,512]{2,1,0:T(8,128)(2,1)}), bf16[4,384,512]{2,1,0:T(8,128)(2,1)S(1)}, u32[]{:S(2)}, u32[]{:S(2)}) %all-to-all-start.1) | async-done | bytes 1572896 | tf_op jit(solution)/shard_map/all_to_all | solution.py:16
  97.8 8.4 %all-to-all-start.2 = ((bf16[24,16,512]{2,1,0:T(8,128)(2,1)}), bf16[24,16,512]{2,1,0:T(8,128)(2,1)S(1)}, u32[]{:S(2)}, u32[]{:S(2)}) async-start(bf16[24,16,512]{2,1,0:T(8,128)(2,1)} %bitcast.18), calls=%async_computation.2 | async-start | bytes 786432 | tf_op jit(solution)/shard_map/all_to_all | solution.py:16
  106.4 2.6 %collective-permute-start.4 = (bf16[512,256]{1,0:T(8,128)(2,1)S(1)}, bf16[512,256]{1,0:T(8,128)(2,1)S(1)}, u32[]{:S(2)}, u32[]{:S(2)}) collective-permute-start(bf16[512,256]{1,0:T(8,128)(2,1)S(1)} %convolution_convert_fusion.3), channel_id=1, source_target_pairs={{0,4},{1,5},{2,6},{3,7},{4,8},{5,9},{6,10},{7,11},{8,12},{9,13},{1... | collective-permute-start | bytes 786440 | tf_op jit(solution)/shard_map/ppermute | solution.py:25
  109.3 2.8 %collective-permute-start.5 = (bf16[512,256]{1,0:T(8,128)(2,1)S(1)}, bf16[512,256]{1,0:T(8,128)(2,1)S(1)}, u32[]{:S(2)}, u32[]{:S(2)}) collective-permute-start(bf16[512,256]{1,0:T(8,128)(2,1)S(1)} %convolution_convert_fusion.2), channel_id=1, source_target_pairs={{0,8},{1,9},{2,10},{3,11},{4,12},{5,13},{6,14},{7,15},{8,16},{9,17... | collective-permute-start | bytes 786440 | tf_op jit(solution)/shard_map/ppermute | solution.py:25
  112.4 3.9 %collective-permute-start.6 = (bf16[512,256]{1,0:T(8,128)(2,1)S(1)}, bf16[512,256]{1,0:T(8,128)(2,1)S(1)}, u32[]{:S(2)}, u32[]{:S(2)}) collective-permute-start(bf16[512,256]{1,0:T(8,128)(2,1)S(1)} %convolution_convert_fusion.1), channel_id=1, source_target_pairs={{0,28},{1,29},{2,30},{3,31},{4,0},{5,1},{6,2},{7,3},{8,4},{9,5},{1... | collective-permute-start | bytes 786440 | tf_op jit(solution)/shard_map/ppermute | solution.py:25
  117.5 11.8 %collective-permute-done.5 = bf16[512,256]{1,0:T(8,128)(2,1)S(1)} collective-permute-done((bf16[512,256]{1,0:T(8,128)(2,1)S(1)}, bf16[512,256]{1,0:T(8,128)(2,1)S(1)}, u32[]{:S(2)}, u32[]{:S(2)}) %collective-permute-start.5) | collective-permute-done | bytes 262176 | tf_op jit(solution)/shard_map/ppermute | solution.py:25
  129.6 2.9 %collective-permute-start.7 = (bf16[2,64,256]{2,1,0:T(8,128)(2,1)S(1)}, bf16[2,64,256]{2,1,0:T(8,128)(2,1)S(1)}, u32[]{:S(2)}, u32[]{:S(2)}) collective-permute-start(bf16[2,64,256]{2,1,0:T(8,128)(2,1)S(1)} %get-tuple-element.15), channel_id=1, source_target_pairs={{0,1},{1,2},{2,3},{3,0},{4,5},{5,6},{6,7},{7,4},{8,9},{9,10},{10,1... | collective-permute-start | bytes 196616 | tf_op jit(solution)/shard_map/ppermute | solution.py:25
  132.6 4.0 %collective-permute-start.8 = (bf16[2,64,256]{2,1,0:T(8,128)(2,1)S(1)}, bf16[2,64,256]{2,1,0:T(8,128)(2,1)S(1)}, u32[]{:S(2)}, u32[]{:S(2)}) collective-permute-start(bf16[2,64,256]{2,1,0:T(8,128)(2,1)S(1)} %get-tuple-element.17), channel_id=1, source_target_pairs={{0,2},{1,3},{2,0},{3,1},{4,6},{5,7},{6,4},{7,5},{8,10},{9,11},{10,... | collective-permute-start | bytes 196616 | tf_op jit(solution)/shard_map/ppermute | solution.py:25
  136.6 2.9 %collective-permute-start.9 = (bf16[2,64,256]{2,1,0:T(8,128)(2,1)S(1)}, bf16[2,64,256]{2,1,0:T(8,128)(2,1)S(1)}, u32[]{:S(2)}, u32[]{:S(2)}) collective-permute-start(bf16[2,64,256]{2,1,0:T(8,128)(2,1)S(1)} %get-tuple-element.16), channel_id=1, source_target_pairs={{0,3},{1,0},{2,1},{3,2},{4,7},{5,4},{6,5},{7,6},{8,11},{9,8},{10,9... | collective-permute-start | bytes 196616 | tf_op jit(solution)/shard_map/ppermute | solution.py:25
  140.9 7.7 %all-to-all-start.3 = ((bf16[8,64,256]{2,1,0:T(8,128)(2,1)}), bf16[8,64,256]{2,1,0:T(8,128)(2,1)S(1)}, u32[]{:S(2)}, u32[]{:S(2)}) async-start(bf16[8,64,256]{2,1,0:T(8,128)(2,1)} %bitcast.21), calls=%async_computation.3 | async-start | bytes 524288 | tf_op jit(solution)/shard_map/all_to_all | solution.py:16
  148.7 1.9 %collective-permute-start.10 = (bf16[64,256]{1,0:T(8,128)(2,1)S(1)}, bf16[64,256]{1,0:T(8,128)(2,1)S(1)}, u32[]{:S(2)}, u32[]{:S(2)}) collective-permute-start(bf16[64,256]{1,0:T(8,128)(2,1)S(1)} %dynamic-slice_bitcast_fusion.3), channel_id=1, source_target_pairs={{0,16},{1,17},{2,18},{3,19},{4,20},{5,21},{6,22},{7,23},{8,24},{9,... | collective-permute-start | bytes 98312 | tf_op jit(solution)/shard_map/ppermute | solution.py:25
  150.7 3.0 %all-to-all-done.3 = bf16[8,64,256]{2,1,0:T(8,128)(2,1)S(1)} async-done(((bf16[8,64,256]{2,1,0:T(8,128)(2,1)}), bf16[8,64,256]{2,1,0:T(8,128)(2,1)S(1)}, u32[]{:S(2)}, u32[]{:S(2)}) %all-to-all-start.3) | async-done | bytes 262176 | tf_op jit(solution)/shard_map/all_to_all | solution.py:16
  153.8 5.1 %collective-permute-done.10 = bf16[64,256]{1,0:T(8,128)(2,1)S(1)} collective-permute-done((bf16[64,256]{1,0:T(8,128)(2,1)S(1)}, bf16[64,256]{1,0:T(8,128)(2,1)S(1)}, u32[]{:S(2)}, u32[]{:S(2)}) %collective-permute-start.10) | collective-permute-done | bytes 32800 | tf_op jit(solution)/shard_map/ppermute | solution.py:25
  (67 shorter events, 16.2 us)
Async XLA Ops:
  0.0 79.6 %copy-start = (bf16[2048,32]{0,1:T(8,128)(2,1)S(1)}, bf16[2048,32]{0,1:T(8,128)(2,1)}, u32[]{:S(2)}) copy-start(bf16[2048,32]{0,1:T(8,128)(2,1)} %param.18) | copy-start | bytes 393220
  4.9 16.8 %copy-start.1 = (bf16[1,2048,176]{1,2,0:T(8,128)(2,1)S(1)}, bf16[1,2048,176]{1,2,0:T(8,128)(2,1)}, u32[]{:S(2)}) copy-start(bf16[1,2048,176]{1,2,0:T(8,128)(2,1)} %param.15) | copy-start | bytes 2162692
  4.9 16.9 %copy-start.2 = (bf16[1,2048,176]{1,2,0:T(8,128)(2,1)S(1)}, bf16[1,2048,176]{1,2,0:T(8,128)(2,1)}, u32[]{:S(2)}) copy-start(bf16[1,2048,176]{1,2,0:T(8,128)(2,1)} %param.16) | copy-start | bytes 2162692
  6.2 15.6 %copy-start.3 = (bf16[1,176,2048]{2,1,0:T(8,128)(2,1)S(1)}, bf16[1,176,2048]{2,1,0:T(8,128)(2,1)}, u32[]{:S(2)}) copy-start(bf16[1,176,2048]{2,1,0:T(8,128)(2,1)} %param.17) | copy-start | bytes 2162692
  6.2 48.5 %all-to-all-start = ((bf16[24,16,1024]{2,1,0:T(8,128)(2,1)}), bf16[24,16,1024]{2,1,0:T(8,128)(2,1)S(1)}, u32[]{:S(2)}, u32[]{:S(2)}) async-start(bf16[24,16,1024]{2,1,0:T(8,128)(2,1)} %bitcast.67), calls=%async_computation | async-start | bytes 1572864 | tf_op jit(solution)/shard_map/all_to_all | solution.py:16
  22.9 37.1 %collective-permute-start.2 = (bf16[288,2048]{1,0:T(8,128)(2,1)}, bf16[288,2048]{1,0:T(8,128)(2,1)S(1)}, u32[]{:S(2)}, u32[]{:S(2)}) collective-permute-start(bf16[288,2048]{1,0:T(8,128)(2,1)} %pad_maximum_fusion), channel_id=1, source_target_pairs={{0,1},{1,0},{2,3},{3,2},{4,5},{5,4},{6,7},{7,6},{8,9},{9,8},{10,11... | collective-permute-start | bytes 3538952 | tf_op jit(solution)/shard_map/ppermute | solution.py:25
  28.4 31.6 %collective-permute-start.3 = (bf16[240,2048]{1,0:T(8,128)(2,1)}, bf16[240,2048]{1,0:T(8,128)(2,1)}, u32[]{:S(2)}, u32[]{:S(2)}) collective-permute-start(bf16[240,2048]{1,0:T(8,128)(2,1)} %pad_maximum_fusion.1), channel_id=1, source_target_pairs={{0,3},{1,2},{2,1},{3,0},{4,7},{5,6},{6,5},{7,4},{8,11},{9,10},{10,... | collective-permute-start | bytes 2949128 | tf_op jit(solution)/shard_map/ppermute | solution.py:25
  54.8 11.0 %collective-permute-start = (bf16[384,512]{1,0:T(8,128)(2,1)S(1)}, bf16[384,512]{1,0:T(8,128)(2,1)S(1)}, u32[]{:S(2)}, u32[]{:S(2)}) collective-permute-start(bf16[384,512]{1,0:T(8,128)(2,1)S(1)} %get-tuple-element.14), channel_id=1, source_target_pairs={{0,4},{1,5},{2,6},{3,7},{4,0},{5,1},{6,2},{7,3},{8,12},{9,13},{10,... | collective-permute-start | bytes 1179656 | tf_op jit(solution)/shard_map/ppermute | solution.py:25
  58.1 10.7 %collective-permute-start.1 = (bf16[384,512]{1,0:T(8,128)(2,1)S(1)}, bf16[384,512]{1,0:T(8,128)(2,1)S(1)}, u32[]{:S(2)}, u32[]{:S(2)}) collective-permute-start(bf16[384,512]{1,0:T(8,128)(2,1)S(1)} %get-tuple-element.13), channel_id=1, source_target_pairs={{0,28},{1,29},{2,30},{3,31},{4,8},{5,9},{6,10},{7,11},{8,4},{9,5},... | collective-permute-start | bytes 1179656 | tf_op jit(solution)/shard_map/ppermute | solution.py:25
  60.0 8.8 %copy-start.4 = (bf16[1,176,2048]{2,1,0:T(8,128)(2,1)S(1)}, bf16[1,176,2048]{2,1,0:T(8,128)(2,1)}, u32[]{:S(2)}) copy-start(bf16[1,176,2048]{2,1,0:T(8,128)(2,1)} %param.17) | copy-start | bytes 2162692
  73.2 6.3 %copy-start.9 = (bf16[32,2048]{1,0:T(8,128)(2,1)S(1)}, bf16[32,2048]{1,0:T(8,128)(2,1)}, u32[]{:S(2)}) copy-start(bf16[32,2048]{1,0:T(8,128)(2,1)} %param.20) | copy-start | bytes 393220
  73.2 6.4 %copy-start.6 = (bf16[256,2048]{1,0:T(8,128)(2,1)S(1)}, bf16[256,2048]{1,0:T(8,128)(2,1)}, u32[]{:S(2)}) copy-start(bf16[256,2048]{1,0:T(8,128)(2,1)} %copy-done.5) | copy-start | bytes 3145732
  73.2 23.6 %all-to-all-start.1 = ((bf16[4,384,512]{2,1,0:T(8,128)(2,1)}), bf16[4,384,512]{2,1,0:T(8,128)(2,1)S(1)}, u32[]{:S(2)}, u32[]{:S(2)}) async-start(bf16[4,384,512]{2,1,0:T(8,128)(2,1)} %shard_map.110), calls=%async_computation.1 | async-start | bytes 3145728 | tf_op jit(solution)/shard_map/all_to_all | solution.py:16
  80.9 35.5 %copy-start.10 = (f32[256,2]{0,1:T(2,128)S(1)}, f32[256,2]{0,1:T(2,128)}, u32[]{:S(2)}) copy-start(f32[256,2]{0,1:T(2,128)} %param.14) | copy-start | bytes 6148
  97.8 41.8 %all-to-all-start.2 = ((bf16[24,16,512]{2,1,0:T(8,128)(2,1)}), bf16[24,16,512]{2,1,0:T(8,128)(2,1)S(1)}, u32[]{:S(2)}, u32[]{:S(2)}) async-start(bf16[24,16,512]{2,1,0:T(8,128)(2,1)} %bitcast.18), calls=%async_computation.2 | async-start | bytes 786432 | tf_op jit(solution)/shard_map/all_to_all | solution.py:16
  106.4 11.1 %collective-permute-start.4 = (bf16[512,256]{1,0:T(8,128)(2,1)S(1)}, bf16[512,256]{1,0:T(8,128)(2,1)S(1)}, u32[]{:S(2)}, u32[]{:S(2)}) collective-permute-start(bf16[512,256]{1,0:T(8,128)(2,1)S(1)} %convolution_convert_fusion.3), channel_id=1, source_target_pairs={{0,4},{1,5},{2,6},{3,7},{4,8},{5,9},{6,10},{7,11},{8,12},{9,13},{1... | collective-permute-start | bytes 786440 | tf_op jit(solution)/shard_map/ppermute | solution.py:25
  109.3 20.0 %collective-permute-start.5 = (bf16[512,256]{1,0:T(8,128)(2,1)S(1)}, bf16[512,256]{1,0:T(8,128)(2,1)S(1)}, u32[]{:S(2)}, u32[]{:S(2)}) collective-permute-start(bf16[512,256]{1,0:T(8,128)(2,1)S(1)} %convolution_convert_fusion.2), channel_id=1, source_target_pairs={{0,8},{1,9},{2,10},{3,11},{4,12},{5,13},{6,14},{7,15},{8,16},{9,17... | collective-permute-start | bytes 786440 | tf_op jit(solution)/shard_map/ppermute | solution.py:25
  112.4 16.9 %collective-permute-start.6 = (bf16[512,256]{1,0:T(8,128)(2,1)S(1)}, bf16[512,256]{1,0:T(8,128)(2,1)S(1)}, u32[]{:S(2)}, u32[]{:S(2)}) collective-permute-start(bf16[512,256]{1,0:T(8,128)(2,1)S(1)} %convolution_convert_fusion.1), channel_id=1, source_target_pairs={{0,28},{1,29},{2,30},{3,31},{4,0},{5,1},{6,2},{7,3},{8,4},{9,5},{1... | collective-permute-start | bytes 786440 | tf_op jit(solution)/shard_map/ppermute | solution.py:25
  129.6 19.0 %copy-start.11 = (f32[64]{0:T(128)S(1)}, f32[64]{0:T(128)}, u32[]{:S(2)}) copy-start(f32[64]{0:T(128)} %param.21) | copy-start | bytes 772
  129.6 19.0 %collective-permute-start.7 = (bf16[2,64,256]{2,1,0:T(8,128)(2,1)S(1)}, bf16[2,64,256]{2,1,0:T(8,128)(2,1)S(1)}, u32[]{:S(2)}, u32[]{:S(2)}) collective-permute-start(bf16[2,64,256]{2,1,0:T(8,128)(2,1)S(1)} %get-tuple-element.15), channel_id=1, source_target_pairs={{0,1},{1,2},{2,3},{3,0},{4,5},{5,6},{6,7},{7,4},{8,9},{9,10},{10,1... | collective-permute-start | bytes 196616 | tf_op jit(solution)/shard_map/ppermute | solution.py:25
  132.6 16.1 %collective-permute-start.8 = (bf16[2,64,256]{2,1,0:T(8,128)(2,1)S(1)}, bf16[2,64,256]{2,1,0:T(8,128)(2,1)S(1)}, u32[]{:S(2)}, u32[]{:S(2)}) collective-permute-start(bf16[2,64,256]{2,1,0:T(8,128)(2,1)S(1)} %get-tuple-element.17), channel_id=1, source_target_pairs={{0,2},{1,3},{2,0},{3,1},{4,6},{5,7},{6,4},{7,5},{8,10},{9,11},{10,... | collective-permute-start | bytes 196616 | tf_op jit(solution)/shard_map/ppermute | solution.py:25
  136.6 12.1 %collective-permute-start.9 = (bf16[2,64,256]{2,1,0:T(8,128)(2,1)S(1)}, bf16[2,64,256]{2,1,0:T(8,128)(2,1)S(1)}, u32[]{:S(2)}, u32[]{:S(2)}) collective-permute-start(bf16[2,64,256]{2,1,0:T(8,128)(2,1)S(1)} %get-tuple-element.16), channel_id=1, source_target_pairs={{0,3},{1,0},{2,1},{3,2},{4,7},{5,4},{6,5},{7,6},{8,11},{9,8},{10,9... | collective-permute-start | bytes 196616 | tf_op jit(solution)/shard_map/ppermute | solution.py:25
  140.9 12.8 %all-to-all-start.3 = ((bf16[8,64,256]{2,1,0:T(8,128)(2,1)}), bf16[8,64,256]{2,1,0:T(8,128)(2,1)S(1)}, u32[]{:S(2)}, u32[]{:S(2)}) async-start(bf16[8,64,256]{2,1,0:T(8,128)(2,1)} %bitcast.21), calls=%async_computation.3 | async-start | bytes 524288 | tf_op jit(solution)/shard_map/all_to_all | solution.py:16
  148.7 10.1 %collective-permute-start.10 = (bf16[64,256]{1,0:T(8,128)(2,1)S(1)}, bf16[64,256]{1,0:T(8,128)(2,1)S(1)}, u32[]{:S(2)}, u32[]{:S(2)}) collective-permute-start(bf16[64,256]{1,0:T(8,128)(2,1)S(1)} %dynamic-slice_bitcast_fusion.3), channel_id=1, source_target_pairs={{0,16},{1,17},{2,18},{3,19},{4,20},{5,21},{6,22},{7,23},{8,24},{9,... | collective-permute-start | bytes 98312 | tf_op jit(solution)/shard_map/ppermute | solution.py:25
  (3 other events, 6.1 us)

commit v7 on v6

--- a/solution.py
+++ b/solution.py
@@ -35,17 +35,6 @@
     )
 
 
-def slots_of(ids, experts):
-    tokens = ids.shape[1]
-    named = ids[:, None, :] == jnp.arange(experts, dtype=jnp.int32)[None, :, None]
-    count = (named[0] | named[1]).astype(jnp.bfloat16)
-    before = lax.broadcasted_iota(jnp.int32, (tokens, tokens), 0) < lax.broadcasted_iota(
-        jnp.int32, (tokens, tokens), 1
-    )
-    earlier = dot(count, before.astype(jnp.bfloat16), 1, 0).astype(jnp.int32)
-    return jnp.sum(jnp.where(named, earlier[None], 0), axis=1)
-
-
 def silu_times(gate_act, up_act):
     return (jax.nn.silu(gate_act) * up_act).astype(jnp.bfloat16)
 
@@ -58,6 +47,35 @@
     return jnp.concatenate(
         [lax.dynamic_slice_in_dim(weight, start, size, 1) for start in starts], axis=1
     )
+
+
+def front_kernel(where, ids, tokens, gain, rows, factors, places):
+    experts = 32
+    count, width = tokens.shape[0], rows.shape[1]
+    few = rows.shape[0] // 24
+    values = tokens[...].astype(jnp.float32)
+    factor = lax.rsqrt(jnp.mean(values * values, axis=-1, keepdims=True) + EPSILON)
+    factors[...] = factor
+    mine = pl.ds(pl.multiple_of(where[0] * width, 128), width)
+    normed = (tokens[:, mine].astype(jnp.float32) * factor * gain[:, mine]).astype(jnp.bfloat16)
+    expert_no = lax.broadcasted_iota(jnp.int32, (experts, count), 0)
+    named = [ids[c : c + 1, :] == expert_no for c in range(2)]
+    ones = jnp.where(named[0] | named[1], 1.0, 0.0).astype(jnp.bfloat16)
+    from_token = lax.broadcasted_iota(jnp.int32, (count, count), 0)
+    to_token = lax.broadcasted_iota(jnp.int32, (count, count), 1)
+    before = jnp.where(from_token < to_token, 1.0, 0.0).astype(jnp.bfloat16)
+    earlier = dot(ones, before, 1, 0)
+    slot_no = lax.broadcasted_iota(jnp.int32, (rows.shape[0], count), 0)
+    hits = None
+    for c in range(2):
+        slot = jnp.sum(jnp.where(named[c], earlier, 0.0), axis=0, keepdims=True)
+        shifted = slot.astype(jnp.int32) - where[1] * few
+        place = jnp.where((shifted >= 0) & (shifted < few), ids[c : c + 1, :] * few + shifted, -1)
+        places[c : c + 1, :] = place
+        hit = place == slot_no
+        hits = hit if hits is None else hits | hit
+    chosen = jnp.where(hits, 1.0, 0.0).astype(jnp.bfloat16)
+    rows[...] = dot(chosen, normed, 1, 0).astype(jnp.bfloat16)
 
 
 def landed_kernel(odd_y, rows, gate, up, first, second, *outs):
@@ -107,6 +125,17 @@
         cost_estimate=pl.CostEstimate(flops=flops, bytes_accessed=moved, transcendentals=0),
         compiler_params=pltpu.CompilerParams(vmem_limit_bytes=24 * 1024 * 1024),
     )(*operands)
+
+
+def front(where, ids, tokens, gain, rows, width):
+    count = tokens.shape[0]
+    shapes = [
+        jax.ShapeDtypeStruct((rows, width), jnp.bfloat16),
+        jax.ShapeDtypeStruct((count, 1), jnp.float32),
+        jax.ShapeDtypeStruct((2, count), jnp.int32),
+    ]
+    flops = 2 * rows * count * width
+    return on_core(front_kernel, flops, 2 * tokens.size, shapes, where, ids, tokens, gain)
 
 
 def acts_of_landed(odd_y, rows, gate, up, first, second):
@@ -161,19 +190,13 @@
     first_w = send(packed(0, split), lambda y, x: (y, x ^ 1))
     second_w = send(packed(split, hidden_part), lambda y, x: (y, x + (1 if x % 2 else -1)))
 
-    values = tokens.astype(jnp.float32)
-    factor = lax.rsqrt(jnp.mean(values * values, axis=-1, keepdims=True) + EPSILON)
-    normed = (values * factor * norm_gain[None, :]).astype(jnp.bfloat16)
-    ids = expert_ids.T
-    shifted = slots_of(ids, experts) - odd_x * few
-    places = jnp.where((shifted >= 0) & (shifted < few), ids * few + shifted, -1)
+    where = jnp.stack([odd_y, odd_x])
+    outgoing, factor, places = front(
+        where, expert_ids.T, tokens, norm_gain[None, :], rows_mine, 2 * wide
+    )
+    normed = (tokens.astype(jnp.float32) * factor * norm_gain[None, :]).astype(jnp.bfloat16)
     slot_no = lax.broadcasted_iota(jnp.int32, (rows_mine, group_tokens), 0)
     chosen = [(places[c][None, :] == slot_no).astype(jnp.bfloat16) for c in range(2)]
-
-    def side(weight, other):
-        return lax.dynamic_slice_in_dim(weight, (odd_y ^ other) * 2 * wide, 2 * wide, 1)
-
-    outgoing = dot(chosen[0] + chosen[1], side(normed, 0), 1, 0).astype(jnp.bfloat16)
     landed = exchange(outgoing.reshape(experts, few, 2 * wide), "ep")
     landed = landed.reshape(rows_mine, 2 * wide)
 

time: 161 us -> 156 us (0.969)
  the two profiles are of different devices: /device:TPU:40 before, /device:TPU:1 now
where the time goes in v7:
time: 156 us; the launch traced here: 153 us
  starting transfers between devices  82.3 us (53%)
  waiting for transfers between devices  48.7 us (31%)
  Pallas kernels  8.02 us (5%)
  local copies, waits for them, and re-layouts  5.76 us (4%)
  other arithmetic  4.07 us (3%)
  matrix products  3.35 us (2%)
    ppermute x11, starting transfers between devices, send(): return lax.ppermute(value, TP, pairs)  42.3 us
    all_to_all x4, starting transfers between devices, exchange(): return lax.all_to_all(blocks, axes, split_axis=0, concat_axis=0, tiled=True)  39.9 us
    all_to_all x4, waiting for transfers between devices, exchange(): return lax.all_to_all(blocks, axes, split_axis=0, concat_axis=0, tiled=True)  36.5 us
    ppermute x11, waiting for transfers between devices, send(): return lax.ppermute(value, TP, pairs)  12.2 us
    pallas_call x3, Pallas kernels, on_core(): pl.pallas_call(kernel, out_shape=out_shape, in_specs=[pl.BlockSpec(memory...  8.02 us
    unnamed x34, local copies, waits for them, and re-layouts  4.49 us
    dot_general x8, matrix products, dot(): lax.dot_general(left, right, (((left_dim,), (right_dim,)), ((), ())), pre...  3.35 us
  transfers between devices with their start and end apart: 15, of which 7 were waited for; matrix products, arithmetic and copies ran while one was open for 5% of the time, Pallas kernels for 2%

profile of v7, /device:TPU:1, one launch (start us, length us, event | category | flops | bytes accessed | tf_op | source)
XLA Modules:
  0.0 152.7 jit_solution(1122771066926901565)
XLA Ops:
  0.1 1.3 copy-done.5
  5.5 16.8 %all-to-all-start = ((bf16[24,16,1024]{2,1,0:T(8,128)(2,1)}), bf16[24,16,1024]{2,1,0:T(8,128)(2,1)S(1)}, u32[]{:S(2)}, u32[]{:S(2)}) async-start(bf16[24,16,1024]{2,1,0:T(8,128)(2,1)} %bitcast.63), calls=%async_computation | async-start | bytes 1572864 | tf_op jit(solution)/shard_map/all_to_all | solution.py:16
  23.6 3.1 %collective-permute-start.2 = (bf16[288,2048]{1,0:T(8,128)(2,1)}, bf16[288,2048]{1,0:T(8,128)(2,1)S(1)}, u32[]{:S(2)}, u32[]{:S(2)}) collective-permute-start(bf16[288,2048]{1,0:T(8,128)(2,1)} %pad_maximum_fusion), channel_id=1, source_target_pairs={{0,1},{1,0},{2,3},{3,2},{4,5},{5,4},{6,7},{7,6},{8,9},{9,8},{10,11... | collective-permute-start | bytes 3538952 | tf_op jit(solution)/shard_map/ppermute | solution.py:25
  28.8 3.7 %collective-permute-start.3 = (bf16[240,2048]{1,0:T(8,128)(2,1)}, bf16[240,2048]{1,0:T(8,128)(2,1)}, u32[]{:S(2)}, u32[]{:S(2)}) collective-permute-start(bf16[240,2048]{1,0:T(8,128)(2,1)} %pad_maximum_fusion.1), channel_id=1, source_target_pairs={{0,3},{1,2},{2,1},{3,0},{4,7},{5,6},{6,5},{7,4},{8,11},{9,10},{10,... | collective-permute-start | bytes 2949128 | tf_op jit(solution)/shard_map/ppermute | solution.py:25
  32.6 20.6 %all-to-all-done = bf16[24,16,1024]{2,1,0:T(8,128)(2,1)S(1)} async-done(((bf16[24,16,1024]{2,1,0:T(8,128)(2,1)}), bf16[24,16,1024]{2,1,0:T(8,128)(2,1)S(1)}, u32[]{:S(2)}, u32[]{:S(2)}) %all-to-all-start) | async-done | bytes 786464 | tf_op jit(solution)/shard_map/all_to_all | solution.py:16
  53.2 3.2 %collective-permute-start = (bf16[384,512]{1,0:T(8,128)(2,1)S(1)}, bf16[384,512]{1,0:T(8,128)(2,1)S(1)}, u32[]{:S(2)}, u32[]{:S(2)}) collective-permute-start(bf16[384,512]{1,0:T(8,128)(2,1)S(1)} %get-tuple-element.20), channel_id=1, source_target_pairs={{0,4},{1,5},{2,6},{3,7},{4,0},{5,1},{6,2},{7,3},{8,12},{9,13},{10,... | collective-permute-start | bytes 1179656 | tf_op jit(solution)/shard_map/ppermute | solution.py:25
  56.4 5.0 %collective-permute-start.1 = (bf16[384,512]{1,0:T(8,128)(2,1)S(1)}, bf16[384,512]{1,0:T(8,128)(2,1)S(1)}, u32[]{:S(2)}, u32[]{:S(2)}) collective-permute-start(bf16[384,512]{1,0:T(8,128)(2,1)S(1)} %get-tuple-element.19), channel_id=1, source_target_pairs={{0,28},{1,29},{2,30},{3,31},{4,8},{5,9},{6,10},{7,11},{8,4},{9,5},... | collective-permute-start | bytes 1179656 | tf_op jit(solution)/shard_map/ppermute | solution.py:25
  61.5 2.3 %shard_map.110 = (f32[176,384]{1,0:T(8,128)S(1)}, f32[176,384]{1,0:T(8,128)S(1)}, f32[192,384]{1,0:T(8,128)S(1)}, f32[160,384]{1,0:T(8,128)S(1)}) custom-call(s32[1]{0:T(128)} %bitcast.2.odd_y, bf16[384,1024]{1,0:T(8,128)(2,1)S(1)} %bitcast.53, bf16[176,2048]{1,0:T(8,128)(2,1)S(1)} %bitcast.56, bf16[176,2048]{1,0:T(8,128)(2,1)S(1)} %bitcast.60, ...), custom_call_target="tpu_custom_call" | custom-call | flops 553648128 | bytes 2359296 | tf_op jit(solution)/shard_map/pallas_call | solution.py:120
  63.8 4.4 %collective-permute-done.1.above = bf16[384,512]{1,0:T(8,128)(2,1)S(1)} collective-permute-done((bf16[384,512]{1,0:T(8,128)(2,1)S(1)}, bf16[384,512]{1,0:T(8,128)(2,1)S(1)}, u32[]{:S(2)}, u32[]{:S(2)}) %collective-permute-start.1) | collective-permute-done | bytes 393248 | tf_op jit(solution)/shard_map/ppermute | solution.py:25
  68.2 4.4 %shard_map.111 = bf16[4,384,512]{2,1,0:T(8,128)(2,1)} custom-call(s32[1]{0:T(128)} %bitcast.2.odd_y, bf16[384,512]{1,0:T(8,128)(2,1)S(1)} %collective-permute-done.below, bf16[384,512]{1,0:T(8,128)(2,1)S(1)} %collective-permute-done.1.above, bf16[176,2048]{1,0:T(8,128)(2,1)S(1)} %bitcast.57, bf16[176,2048]{1,0:T(8,128)(2,1)S(1)} %bitcast.61, ...), custom_call_target="tpu_custom_call" | custom-call | flops 1107296256 | bytes 4325376 | tf_op jit(solution)/shard_map/pallas_call | solution.py:120
  72.7 4.2 %all-to-all-start.1 = ((bf16[4,384,512]{2,1,0:T(8,128)(2,1)}), bf16[4,384,512]{2,1,0:T(8,128)(2,1)S(1)}, u32[]{:S(2)}, u32[]{:S(2)}) async-start(bf16[4,384,512]{2,1,0:T(8,128)(2,1)} %shard_map.111), calls=%async_computation.1 | async-start | bytes 3145728 | tf_op jit(solution)/shard_map/all_to_all | solution.py:16
  78.5 3.4 %collective-permute-start.4 = (bf16[512,256]{1,0:T(8,128)(2,1)S(1)}, bf16[512,256]{1,0:T(8,128)(2,1)S(1)}, u32[]{:S(2)}, u32[]{:S(2)}) collective-permute-start(bf16[512,256]{1,0:T(8,128)(2,1)S(1)} %convolution_convert_fusion.2), channel_id=1, source_target_pairs={{0,4},{1,5},{2,6},{3,7},{4,8},{5,9},{6,10},{7,11},{8,12},{9,13},{1... | collective-permute-start | bytes 786440 | tf_op jit(solution)/shard_map/ppermute | solution.py:25
  81.8 15.2 %all-to-all-done.1 = bf16[4,384,512]{2,1,0:T(8,128)(2,1)S(1)} async-done(((bf16[4,384,512]{2,1,0:T(8,128)(2,1)}), bf16[4,384,512]{2,1,0:T(8,128)(2,1)S(1)}, u32[]{:S(2)}, u32[]{:S(2)}) %all-to-all-start.1) | async-done | bytes 1572896 | tf_op jit(solution)/shard_map/all_to_all | solution.py:16
  98.0 9.1 %all-to-all-start.2 = ((bf16[24,16,512]{2,1,0:T(8,128)(2,1)}), bf16[24,16,512]{2,1,0:T(8,128)(2,1)S(1)}, u32[]{:S(2)}, u32[]{:S(2)}) async-start(bf16[24,16,512]{2,1,0:T(8,128)(2,1)} %bitcast.17), calls=%async_computation.2 | async-start | bytes 786432 | tf_op jit(solution)/shard_map/all_to_all | solution.py:16
  107.4 4.2 %collective-permute-start.5 = (bf16[512,256]{1,0:T(8,128)(2,1)S(1)}, bf16[512,256]{1,0:T(8,128)(2,1)S(1)}, u32[]{:S(2)}, u32[]{:S(2)}) collective-permute-start(bf16[512,256]{1,0:T(8,128)(2,1)S(1)} %convolution_convert_fusion.1), channel_id=1, source_target_pairs={{0,8},{1,9},{2,10},{3,11},{4,12},{5,13},{6,14},{7,15},{8,16},{9,17... | collective-permute-start | bytes 786440 | tf_op jit(solution)/shard_map/ppermute | solution.py:25
  111.9 3.4 %collective-permute-start.6 = (bf16[512,256]{1,0:T(8,128)(2,1)S(1)}, bf16[512,256]{1,0:T(8,128)(2,1)S(1)}, u32[]{:S(2)}, u32[]{:S(2)}) collective-permute-start(bf16[512,256]{1,0:T(8,128)(2,1)S(1)} %convolution_convert_fusion), channel_id=1, source_target_pairs={{0,28},{1,29},{2,30},{3,31},{4,0},{5,1},{6,2},{7,3},{8,4},{9,5},{1... | collective-permute-start | bytes 786440 | tf_op jit(solution)/shard_map/ppermute | solution.py:25
  115.4 4.3 %collective-permute-done.5 = bf16[512,256]{1,0:T(8,128)(2,1)S(1)} collective-permute-done((bf16[512,256]{1,0:T(8,128)(2,1)S(1)}, bf16[512,256]{1,0:T(8,128)(2,1)S(1)}, u32[]{:S(2)}, u32[]{:S(2)}) %collective-permute-start.5) | collective-permute-done | bytes 262176 | tf_op jit(solution)/shard_map/ppermute | solution.py:25
  119.7 1.4 collective-permute-done.6
  121.5 2.2 %collective-permute-start.7 = (bf16[2,64,256]{2,1,0:T(8,128)(2,1)S(1)}, bf16[2,64,256]{2,1,0:T(8,128)(2,1)S(1)}, u32[]{:S(2)}, u32[]{:S(2)}) collective-permute-start(bf16[2,64,256]{2,1,0:T(8,128)(2,1)S(1)} %get-tuple-element.21), channel_id=1, source_target_pairs={{0,1},{1,2},{2,3},{3,0},{4,5},{5,6},{6,7},{7,4},{8,9},{9,10},{10,1... | collective-permute-start | bytes 196616 | tf_op jit(solution)/shard_map/ppermute | solution.py:25
  123.7 3.7 %collective-permute-start.8 = (bf16[2,64,256]{2,1,0:T(8,128)(2,1)S(1)}, bf16[2,64,256]{2,1,0:T(8,128)(2,1)S(1)}, u32[]{:S(2)}, u32[]{:S(2)}) collective-permute-start(bf16[2,64,256]{2,1,0:T(8,128)(2,1)S(1)} %get-tuple-element.23), channel_id=1, source_target_pairs={{0,2},{1,3},{2,0},{3,1},{4,6},{5,7},{6,4},{7,5},{8,10},{9,11},{10,... | collective-permute-start | bytes 196616 | tf_op jit(solution)/shard_map/ppermute | solution.py:25
  127.5 3.1 %collective-permute-start.9 = (bf16[2,64,256]{2,1,0:T(8,128)(2,1)S(1)}, bf16[2,64,256]{2,1,0:T(8,128)(2,1)S(1)}, u32[]{:S(2)}, u32[]{:S(2)}) collective-permute-start(bf16[2,64,256]{2,1,0:T(8,128)(2,1)S(1)} %get-tuple-element.22), channel_id=1, source_target_pairs={{0,3},{1,0},{2,1},{3,2},{4,7},{5,4},{6,5},{7,6},{8,11},{9,8},{10,9... | collective-permute-start | bytes 196616 | tf_op jit(solution)/shard_map/ppermute | solution.py:25
  132.0 9.8 %all-to-all-start.3 = ((bf16[8,64,256]{2,1,0:T(8,128)(2,1)}), bf16[8,64,256]{2,1,0:T(8,128)(2,1)S(1)}, u32[]{:S(2)}, u32[]{:S(2)}) async-start(bf16[8,64,256]{2,1,0:T(8,128)(2,1)} %bitcast.22), calls=%async_computation.3 | async-start | bytes 524288 | tf_op jit(solution)/shard_map/all_to_all | solution.py:16
  141.9 7.3 %collective-permute-start.10 = (bf16[64,256]{1,0:T(8,128)(2,1)S(1)}, bf16[64,256]{1,0:T(8,128)(2,1)S(1)}, u32[]{:S(2)}, u32[]{:S(2)}) collective-permute-start(bf16[64,256]{1,0:T(8,128)(2,1)S(1)} %dynamic-slice_bitcast_fusion.3), channel_id=1, source_target_pairs={{0,16},{1,17},{2,18},{3,19},{4,20},{5,21},{6,22},{7,23},{8,24},{9,... | collective-permute-start | bytes 98312 | tf_op jit(solution)/shard_map/ppermute | solution.py:25
  150.0 2.0 %collective-permute-done.10 = bf16[64,256]{1,0:T(8,128)(2,1)S(1)} collective-permute-done((bf16[64,256]{1,0:T(8,128)(2,1)S(1)}, bf16[64,256]{1,0:T(8,128)(2,1)S(1)}, u32[]{:S(2)}, u32[]{:S(2)}) %collective-permute-start.10) | collective-permute-done | bytes 32800 | tf_op jit(solution)/shard_map/ppermute | solution.py:25
  (72 shorter events, 13.8 us)
Async XLA Ops:
  0.0 77.0 %copy-start = (bf16[2048,32]{0,1:T(8,128)(2,1)S(1)}, bf16[2048,32]{0,1:T(8,128)(2,1)}, u32[]{:S(2)}) copy-start(bf16[2048,32]{0,1:T(8,128)(2,1)} %param.18) | copy-start | bytes 393220
  0.0 22.4 %copy-start.1 = (bf16[1,2048,176]{1,2,0:T(8,128)(2,1)S(1)}, bf16[1,2048,176]{1,2,0:T(8,128)(2,1)}, u32[]{:S(2)}) copy-start(bf16[1,2048,176]{1,2,0:T(8,128)(2,1)} %param.15) | copy-start | bytes 2162692
  2.8 19.6 %copy-start.2 = (bf16[1,2048,176]{1,2,0:T(8,128)(2,1)S(1)}, bf16[1,2048,176]{1,2,0:T(8,128)(2,1)}, u32[]{:S(2)}) copy-start(bf16[1,2048,176]{1,2,0:T(8,128)(2,1)} %param.16) | copy-start | bytes 2162692
  5.5 16.9 %copy-start.3 = (bf16[1,176,2048]{2,1,0:T(8,128)(2,1)S(1)}, bf16[1,176,2048]{2,1,0:T(8,128)(2,1)}, u32[]{:S(2)}) copy-start(bf16[1,176,2048]{2,1,0:T(8,128)(2,1)} %param.17) | copy-start | bytes 2162692
  5.5 47.6 %all-to-all-start = ((bf16[24,16,1024]{2,1,0:T(8,128)(2,1)}), bf16[24,16,1024]{2,1,0:T(8,128)(2,1)S(1)}, u32[]{:S(2)}, u32[]{:S(2)}) async-start(bf16[24,16,1024]{2,1,0:T(8,128)(2,1)} %bitcast.63), calls=%async_computation | async-start | bytes 1572864 | tf_op jit(solution)/shard_map/all_to_all | solution.py:16
  23.6 37.8 %collective-permute-start.2 = (bf16[288,2048]{1,0:T(8,128)(2,1)}, bf16[288,2048]{1,0:T(8,128)(2,1)S(1)}, u32[]{:S(2)}, u32[]{:S(2)}) collective-permute-start(bf16[288,2048]{1,0:T(8,128)(2,1)} %pad_maximum_fusion), channel_id=1, source_target_pairs={{0,1},{1,0},{2,3},{3,2},{4,5},{5,4},{6,7},{7,6},{8,9},{9,8},{10,11... | collective-permute-start | bytes 3538952 | tf_op jit(solution)/shard_map/ppermute | solution.py:25
  28.8 32.6 %collective-permute-start.3 = (bf16[240,2048]{1,0:T(8,128)(2,1)}, bf16[240,2048]{1,0:T(8,128)(2,1)}, u32[]{:S(2)}, u32[]{:S(2)}) collective-permute-start(bf16[240,2048]{1,0:T(8,128)(2,1)} %pad_maximum_fusion.1), channel_id=1, source_target_pairs={{0,3},{1,2},{2,1},{3,0},{4,7},{5,6},{6,5},{7,4},{8,11},{9,10},{10,... | collective-permute-start | bytes 2949128 | tf_op jit(solution)/shard_map/ppermute | solution.py:25
  53.2 10.6 %collective-permute-start = (bf16[384,512]{1,0:T(8,128)(2,1)S(1)}, bf16[384,512]{1,0:T(8,128)(2,1)S(1)}, u32[]{:S(2)}, u32[]{:S(2)}) collective-permute-start(bf16[384,512]{1,0:T(8,128)(2,1)S(1)} %get-tuple-element.20), channel_id=1, source_target_pairs={{0,4},{1,5},{2,6},{3,7},{4,0},{5,1},{6,2},{7,3},{8,12},{9,13},{10,... | collective-permute-start | bytes 1179656 | tf_op jit(solution)/shard_map/ppermute | solution.py:25
  56.4 11.8 %copy-start.4 = (bf16[1,176,2048]{2,1,0:T(8,128)(2,1)S(1)}, bf16[1,176,2048]{2,1,0:T(8,128)(2,1)}, u32[]{:S(2)}) copy-start(bf16[1,176,2048]{2,1,0:T(8,128)(2,1)} %param.17) | copy-start | bytes 2162692
  56.4 11.8 %collective-permute-start.1 = (bf16[384,512]{1,0:T(8,128)(2,1)S(1)}, bf16[384,512]{1,0:T(8,128)(2,1)S(1)}, u32[]{:S(2)}, u32[]{:S(2)}) collective-permute-start(bf16[384,512]{1,0:T(8,128)(2,1)S(1)} %get-tuple-element.19), channel_id=1, source_target_pairs={{0,28},{1,29},{2,30},{3,31},{4,8},{5,9},{6,10},{7,11},{8,4},{9,5},... | collective-permute-start | bytes 1179656 | tf_op jit(solution)/shard_map/ppermute | solution.py:25
  72.6 4.3 %copy-start.6 = (bf16[256,2048]{1,0:T(8,128)(2,1)S(1)}, bf16[256,2048]{1,0:T(8,128)(2,1)}, u32[]{:S(2)}) copy-start(bf16[256,2048]{1,0:T(8,128)(2,1)} %tokens.1) | copy-start | bytes 3145732
  72.7 4.4 %copy-start.11 = (f32[2048]{0:T(1024)S(1)}, f32[2048]{0:T(1024)}, u32[]{:S(2)}) copy-start(f32[2048]{0:T(1024)} %param.12) | copy-start | bytes 24580
  72.7 24.4 %all-to-all-start.1 = ((bf16[4,384,512]{2,1,0:T(8,128)(2,1)}), bf16[4,384,512]{2,1,0:T(8,128)(2,1)S(1)}, u32[]{:S(2)}, u32[]{:S(2)}) async-start(bf16[4,384,512]{2,1,0:T(8,128)(2,1)} %shard_map.111), calls=%async_computation.1 | async-start | bytes 3145728 | tf_op jit(solution)/shard_map/all_to_all | solution.py:16
  78.5 36.9 %copy-start.14 = (f32[256,2]{0,1:T(2,128)S(1)}, f32[256,2]{0,1:T(2,128)}, u32[]{:S(2)}) copy-start(f32[256,2]{0,1:T(2,128)} %param.14) | copy-start | bytes 6148
  78.5 36.9 %collective-permute-start.4 = (bf16[512,256]{1,0:T(8,128)(2,1)S(1)}, bf16[512,256]{1,0:T(8,128)(2,1)S(1)}, u32[]{:S(2)}, u32[]{:S(2)}) collective-permute-start(bf16[512,256]{1,0:T(8,128)(2,1)S(1)} %convolution_convert_fusion.2), channel_id=1, source_target_pairs={{0,4},{1,5},{2,6},{3,7},{4,8},{5,9},{6,10},{7,11},{8,12},{9,13},{1... | collective-permute-start | bytes 786440 | tf_op jit(solution)/shard_map/ppermute | solution.py:25
  98.0 32.5 %all-to-all-start.2 = ((bf16[24,16,512]{2,1,0:T(8,128)(2,1)}), bf16[24,16,512]{2,1,0:T(8,128)(2,1)S(1)}, u32[]{:S(2)}, u32[]{:S(2)}) async-start(bf16[24,16,512]{2,1,0:T(8,128)(2,1)} %bitcast.17), calls=%async_computation.2 | async-start | bytes 786432 | tf_op jit(solution)/shard_map/all_to_all | solution.py:16
  107.4 12.3 %collective-permute-start.5 = (bf16[512,256]{1,0:T(8,128)(2,1)S(1)}, bf16[512,256]{1,0:T(8,128)(2,1)S(1)}, u32[]{:S(2)}, u32[]{:S(2)}) collective-permute-start(bf16[512,256]{1,0:T(8,128)(2,1)S(1)} %convolution_convert_fusion.1), channel_id=1, source_target_pairs={{0,8},{1,9},{2,10},{3,11},{4,12},{5,13},{6,14},{7,15},{8,16},{9,17... | collective-permute-start | bytes 786440 | tf_op jit(solution)/shard_map/ppermute | solution.py:25
  111.9 9.3 %collective-permute-start.6 = (bf16[512,256]{1,0:T(8,128)(2,1)S(1)}, bf16[512,256]{1,0:T(8,128)(2,1)S(1)}, u32[]{:S(2)}, u32[]{:S(2)}) collective-permute-start(bf16[512,256]{1,0:T(8,128)(2,1)S(1)} %convolution_convert_fusion), channel_id=1, source_target_pairs={{0,28},{1,29},{2,30},{3,31},{4,0},{5,1},{6,2},{7,3},{8,4},{9,5},{1... | collective-permute-start | bytes 786440 | tf_op jit(solution)/shard_map/ppermute | solution.py:25
  121.5 20.3 %copy-start.16 = (f32[64]{0:T(128)S(1)}, f32[64]{0:T(128)}, u32[]{:S(2)}) copy-start(f32[64]{0:T(128)} %param.21) | copy-start | bytes 772
  121.5 20.3 %collective-permute-start.7 = (bf16[2,64,256]{2,1,0:T(8,128)(2,1)S(1)}, bf16[2,64,256]{2,1,0:T(8,128)(2,1)S(1)}, u32[]{:S(2)}, u32[]{:S(2)}) collective-permute-start(bf16[2,64,256]{2,1,0:T(8,128)(2,1)S(1)} %get-tuple-element.21), channel_id=1, source_target_pairs={{0,1},{1,2},{2,3},{3,0},{4,5},{5,6},{6,7},{7,4},{8,9},{9,10},{10,1... | collective-permute-start | bytes 196616 | tf_op jit(solution)/shard_map/ppermute | solution.py:25
  123.7 18.1 %collective-permute-start.8 = (bf16[2,64,256]{2,1,0:T(8,128)(2,1)S(1)}, bf16[2,64,256]{2,1,0:T(8,128)(2,1)S(1)}, u32[]{:S(2)}, u32[]{:S(2)}) collective-permute-start(bf16[2,64,256]{2,1,0:T(8,128)(2,1)S(1)} %get-tuple-element.23), channel_id=1, source_target_pairs={{0,2},{1,3},{2,0},{3,1},{4,6},{5,7},{6,4},{7,5},{8,10},{9,11},{10,... | collective-permute-start | bytes 196616 | tf_op jit(solution)/shard_map/ppermute | solution.py:25
  127.5 14.4 %collective-permute-start.9 = (bf16[2,64,256]{2,1,0:T(8,128)(2,1)S(1)}, bf16[2,64,256]{2,1,0:T(8,128)(2,1)S(1)}, u32[]{:S(2)}, u32[]{:S(2)}) collective-permute-start(bf16[2,64,256]{2,1,0:T(8,128)(2,1)S(1)} %get-tuple-element.22), channel_id=1, source_target_pairs={{0,3},{1,0},{2,1},{3,2},{4,7},{5,4},{6,5},{7,6},{8,11},{9,8},{10,9... | collective-permute-start | bytes 196616 | tf_op jit(solution)/shard_map/ppermute | solution.py:25
  132.0 18.0 %all-to-all-start.3 = ((bf16[8,64,256]{2,1,0:T(8,128)(2,1)}), bf16[8,64,256]{2,1,0:T(8,128)(2,1)S(1)}, u32[]{:S(2)}, u32[]{:S(2)}) async-start(bf16[8,64,256]{2,1,0:T(8,128)(2,1)} %bitcast.22), calls=%async_computation.3 | async-start | bytes 524288 | tf_op jit(solution)/shard_map/all_to_all | solution.py:16
  141.9 10.0 %collective-permute-start.10 = (bf16[64,256]{1,0:T(8,128)(2,1)S(1)}, bf16[64,256]{1,0:T(8,128)(2,1)S(1)}, u32[]{:S(2)}, u32[]{:S(2)}) collective-permute-start(bf16[64,256]{1,0:T(8,128)(2,1)S(1)} %dynamic-slice_bitcast_fusion.3), channel_id=1, source_target_pairs={{0,16},{1,17},{2,18},{3,19},{4,20},{5,21},{6,22},{7,23},{8,24},{9,... | collective-permute-start | bytes 98312 | tf_op jit(solution)/shard_map/ppermute | solution.py:25
  (8 other events, 13.6 us)

commit v8 on v7

--- a/solution.py
+++ b/solution.py
@@ -49,13 +49,14 @@
     )
 
 
-def front_kernel(where, ids, tokens, gain, rows, factors, places):
+def front_kernel(where, ids, tokens, gain, gate, up, rows, dense_hidden, places):
     experts = 32
     count, width = tokens.shape[0], rows.shape[1]
     few = rows.shape[0] // 24
     values = tokens[...].astype(jnp.float32)
     factor = lax.rsqrt(jnp.mean(values * values, axis=-1, keepdims=True) + EPSILON)
-    factors[...] = factor
+    whole = (values * factor * gain[...]).astype(jnp.bfloat16)
+    dense_hidden[...] = silu_times(dot(whole, gate[...], 1, 1), dot(whole, up[...], 1, 1))
     mine = pl.ds(pl.multiple_of(where[0] * width, 128), width)
     normed = (tokens[:, mine].astype(jnp.float32) * factor * gain[:, mine]).astype(jnp.bfloat16)
     expert_no = lax.broadcasted_iota(jnp.int32, (experts, count), 0)
@@ -127,15 +128,16 @@
     )(*operands)
 
 
-def front(where, ids, tokens, gain, rows, width):
+def front(where, ids, tokens, gain, gate, up, rows, width):
     count = tokens.shape[0]
     shapes = [
         jax.ShapeDtypeStruct((rows, width), jnp.bfloat16),
-        jax.ShapeDtypeStruct((count, 1), jnp.float32),
+        jax.ShapeDtypeStruct((count, gate.shape[0]), jnp.bfloat16),
         jax.ShapeDtypeStruct((2, count), jnp.int32),
     ]
     flops = 2 * rows * count * width
-    return on_core(front_kernel, flops, 2 * tokens.size, shapes, where, ids, tokens, gain)
+    operands = (where, ids, tokens, gain, gate, up)
+    return on_core(front_kernel, flops, 2 * tokens.size, shapes, *operands)
 
 
 def acts_of_landed(odd_y, rows, gate, up, first, second):
@@ -191,16 +193,21 @@
     second_w = send(packed(split, hidden_part), lambda y, x: (y, x + (1 if x % 2 else -1)))
 
     where = jnp.stack([odd_y, odd_x])
-    outgoing, factor, places = front(
-        where, expert_ids.T, tokens, norm_gain[None, :], rows_mine, 2 * wide
-    )
-    normed = (tokens.astype(jnp.float32) * factor * norm_gain[None, :]).astype(jnp.bfloat16)
+    outgoing, dense_hidden, places = front(
+        where,
+        expert_ids.T,
+        tokens,
+        norm_gain[None, :],
+        dense_gate_w.T,
+        dense_up_w.T,
+        rows_mine,
+        2 * wide,
+    )
     slot_no = lax.broadcasted_iota(jnp.int32, (rows_mine, group_tokens), 0)
     chosen = [(places[c][None, :] == slot_no).astype(jnp.bfloat16) for c in range(2)]
     landed = exchange(outgoing.reshape(experts, few, 2 * wide), "ep")
     landed = landed.reshape(rows_mine, 2 * wide)
 
-    dense_hidden = silu_times(dot(normed, dense_gate_w, 1, 0), dot(normed, dense_up_w, 1, 0))
 
     def dense_part(step):
         first = (mod_y + step) % 4 * row_width

time: 156 us -> 163 us (1.045)
  the two profiles are of different devices: /device:TPU:1 before, /device:TPU:6 now
where the time goes in v8:
time: 163 us; the launch traced here: 162 us
  starting transfers between devices  78.8 us (48%)
  waiting for transfers between devices  60.8 us (37%)
  Pallas kernels  8.55 us (5%)
  local copies, waits for them, and re-layouts  6.63 us (4%)
  other arithmetic  3.96 us (2%)
  matrix products  2.41 us (1%)
    ppermute x11, starting transfers between devices, send(): return lax.ppermute(value, TP, pairs)  44.4 us
    all_to_all x4, waiting for transfers between devices, exchange(): return lax.all_to_all(blocks, axes, split_axis=0, concat_axis=0, tiled=True)  39.9 us
    all_to_all x4, starting transfers between devices, exchange(): return lax.all_to_all(blocks, axes, split_axis=0, concat_axis=0, tiled=True)  34.4 us
    ppermute x11, waiting for transfers between devices, send(): return lax.ppermute(value, TP, pairs)  20.9 us
    pallas_call x3, Pallas kernels, on_core(): pl.pallas_call(kernel, out_shape=out_shape, in_specs=[pl.BlockSpec(memory...  8.55 us
    unnamed x26, local copies, waits for them, and re-layouts  5.39 us
  transfers between devices with their start and end apart: 15, of which 7 were waited for; matrix products, arithmetic and copies ran while one was open for 4% of the time, Pallas kernels for 1%

profile of v8, /device:TPU:6, one launch (start us, length us, event | category | flops | bytes accessed | tf_op | source)
XLA Modules:
  0.0 161.6 jit_solution(9885105015221918172)
XLA Ops:
  4.5 1.8 %shard_map.109 = (bf16[384,1024]{1,0:T(8,128)(2,1)S(1)}, bf16[256,32]{1,0:T(8,128)(2,1)S(1)}, s32[2,256]{1,0:T(2,128)S(1)}) custom-call(s32[2]{0:T(128)S(1)} %pad_add_fusion.where, s32[2,256]{1,0:T(2,128)S(1)} %bitcast.67, bf16[256,2048]{1,0:T(8,128)(2,1)S(1)} %copy-done.4, f32[1,2048]{1,0:T(1,128)S(1)} %bitcast.66, bf16[32,2048]{1,0:T(8,128)(2,1)S(1)} %bitcast.64, ...), custom_call_target="tpu_custom_call" | custom-call | flops 201326592 | bytes 1048576 | tf_op jit(solution)/shard_map/pallas_call | solution.py:121
  7.2 15.5 %all-to-all-start = ((bf16[24,16,1024]{2,1,0:T(8,128)(2,1)}), bf16[24,16,1024]{2,1,0:T(8,128)(2,1)S(1)}, u32[]{:S(2)}, u32[]{:S(2)}) async-start(bf16[24,16,1024]{2,1,0:T(8,128)(2,1)} %bitcast.63), calls=%async_computation | async-start | bytes 1572864 | tf_op jit(solution)/shard_map/all_to_all | solution.py:16
  24.0 2.7 %collective-permute-start.2 = (bf16[288,2048]{1,0:T(8,128)(2,1)}, bf16[288,2048]{1,0:T(8,128)(2,1)S(1)}, u32[]{:S(2)}, u32[]{:S(2)}) collective-permute-start(bf16[288,2048]{1,0:T(8,128)(2,1)} %pad_maximum_fusion), channel_id=1, source_target_pairs={{0,1},{1,0},{2,3},{3,2},{4,5},{5,4},{6,7},{7,6},{8,9},{9,8},{10,11... | collective-permute-start | bytes 3538952 | tf_op jit(solution)/shard_map/ppermute | solution.py:25
  28.8 3.0 %collective-permute-start.3 = (bf16[240,2048]{1,0:T(8,128)(2,1)}, bf16[240,2048]{1,0:T(8,128)(2,1)}, u32[]{:S(2)}, u32[]{:S(2)}) collective-permute-start(bf16[240,2048]{1,0:T(8,128)(2,1)} %pad_maximum_fusion.1), channel_id=1, source_target_pairs={{0,3},{1,2},{2,1},{3,0},{4,7},{5,6},{6,5},{7,4},{8,11},{9,10},{10,... | collective-permute-start | bytes 2949128 | tf_op jit(solution)/shard_map/ppermute | solution.py:25
  31.9 23.9 %all-to-all-done = bf16[24,16,1024]{2,1,0:T(8,128)(2,1)S(1)} async-done(((bf16[24,16,1024]{2,1,0:T(8,128)(2,1)}), bf16[24,16,1024]{2,1,0:T(8,128)(2,1)S(1)}, u32[]{:S(2)}, u32[]{:S(2)}) %all-to-all-start) | async-done | bytes 786464 | tf_op jit(solution)/shard_map/all_to_all | solution.py:16
  55.8 3.5 %collective-permute-start = (bf16[384,512]{1,0:T(8,128)(2,1)S(1)}, bf16[384,512]{1,0:T(8,128)(2,1)S(1)}, u32[]{:S(2)}, u32[]{:S(2)}) collective-permute-start(bf16[384,512]{1,0:T(8,128)(2,1)S(1)} %get-tuple-element.20), channel_id=1, source_target_pairs={{0,4},{1,5},{2,6},{3,7},{4,0},{5,1},{6,2},{7,3},{8,12},{9,13},{10,... | collective-permute-start | bytes 1179656 | tf_op jit(solution)/shard_map/ppermute | solution.py:25
  59.3 5.3 %collective-permute-start.1 = (bf16[384,512]{1,0:T(8,128)(2,1)S(1)}, bf16[384,512]{1,0:T(8,128)(2,1)S(1)}, u32[]{:S(2)}, u32[]{:S(2)}) collective-permute-start(bf16[384,512]{1,0:T(8,128)(2,1)S(1)} %get-tuple-element.19), channel_id=1, source_target_pairs={{0,28},{1,29},{2,30},{3,31},{4,8},{5,9},{6,10},{7,11},{8,4},{9,5},... | collective-permute-start | bytes 1179656 | tf_op jit(solution)/shard_map/ppermute | solution.py:25
  64.6 2.3 %shard_map.110 = (f32[176,384]{1,0:T(8,128)S(1)}, f32[176,384]{1,0:T(8,128)S(1)}, f32[192,384]{1,0:T(8,128)S(1)}, f32[160,384]{1,0:T(8,128)S(1)}) custom-call(s32[1]{0:T(128)} %bitcast.2.odd_y, bf16[384,1024]{1,0:T(8,128)(2,1)S(1)} %bitcast.53, bf16[176,2048]{1,0:T(8,128)(2,1)S(1)} %bitcast.56, bf16[176,2048]{1,0:T(8,128)(2,1)S(1)} %bitcast.60, ...), custom_call_target="tpu_custom_call" | custom-call | flops 553648128 | bytes 2359296 | tf_op jit(solution)/shard_map/pallas_call | solution.py:121
  67.0 4.7 %collective-permute-done.1.above = bf16[384,512]{1,0:T(8,128)(2,1)S(1)} collective-permute-done((bf16[384,512]{1,0:T(8,128)(2,1)S(1)}, bf16[384,512]{1,0:T(8,128)(2,1)S(1)}, u32[]{:S(2)}, u32[]{:S(2)}) %collective-permute-start.1) | collective-permute-done | bytes 393248 | tf_op jit(solution)/shard_map/ppermute | solution.py:25
  71.7 4.4 %shard_map.111 = bf16[4,384,512]{2,1,0:T(8,128)(2,1)} custom-call(s32[1]{0:T(128)} %bitcast.2.odd_y, bf16[384,512]{1,0:T(8,128)(2,1)S(1)} %collective-permute-done.below, bf16[384,512]{1,0:T(8,128)(2,1)S(1)} %collective-permute-done.1.above, bf16[176,2048]{1,0:T(8,128)(2,1)S(1)} %bitcast.57, bf16[176,2048]{1,0:T(8,128)(2,1)S(1)} %bitcast.61, ...), custom_call_target="tpu_custom_call" | custom-call | flops 1107296256 | bytes 4325376 | tf_op jit(solution)/shard_map/pallas_call | solution.py:121
  76.1 5.1 %all-to-all-start.1 = ((bf16[4,384,512]{2,1,0:T(8,128)(2,1)}), bf16[4,384,512]{2,1,0:T(8,128)(2,1)S(1)}, u32[]{:S(2)}, u32[]{:S(2)}) async-start(bf16[4,384,512]{2,1,0:T(8,128)(2,1)} %shard_map.111), calls=%async_computation.1 | async-start | bytes 3145728 | tf_op jit(solution)/shard_map/all_to_all | solution.py:16
  81.5 5.6 %collective-permute-start.6 = (bf16[512,256]{1,0:T(8,128)(2,1)S(1)}, bf16[512,256]{1,0:T(8,128)(2,1)S(1)}, u32[]{:S(2)}, u32[]{:S(2)}) collective-permute-start(bf16[512,256]{1,0:T(8,128)(2,1)S(1)} %convolution_convert_fusion), channel_id=1, source_target_pairs={{0,28},{1,29},{2,30},{3,31},{4,0},{5,1},{6,2},{7,3},{8,4},{9,5},{1... | collective-permute-start | bytes 786440 | tf_op jit(solution)/shard_map/ppermute | solution.py:25
  87.1 13.3 %all-to-all-done.1 = bf16[4,384,512]{2,1,0:T(8,128)(2,1)S(1)} async-done(((bf16[4,384,512]{2,1,0:T(8,128)(2,1)}), bf16[4,384,512]{2,1,0:T(8,128)(2,1)S(1)}, u32[]{:S(2)}, u32[]{:S(2)}) %all-to-all-start.1) | async-done | bytes 1572896 | tf_op jit(solution)/shard_map/all_to_all | solution.py:16
  101.3 6.3 %all-to-all-start.2 = ((bf16[24,16,512]{2,1,0:T(8,128)(2,1)}), bf16[24,16,512]{2,1,0:T(8,128)(2,1)S(1)}, u32[]{:S(2)}, u32[]{:S(2)}) async-start(bf16[24,16,512]{2,1,0:T(8,128)(2,1)} %bitcast.19), calls=%async_computation.2 | async-start | bytes 786432 | tf_op jit(solution)/shard_map/all_to_all | solution.py:16
  107.9 4.0 %collective-permute-start.5 = (bf16[512,256]{1,0:T(8,128)(2,1)S(1)}, bf16[512,256]{1,0:T(8,128)(2,1)S(1)}, u32[]{:S(2)}, u32[]{:S(2)}) collective-permute-start(bf16[512,256]{1,0:T(8,128)(2,1)S(1)} %convolution_convert_fusion.1), channel_id=1, source_target_pairs={{0,8},{1,9},{2,10},{3,11},{4,12},{5,13},{6,14},{7,15},{8,16},{9,17... | collective-permute-start | bytes 786440 | tf_op jit(solution)/shard_map/ppermute | solution.py:25
  112.1 1.9 %collective-permute-start.4 = (bf16[512,256]{1,0:T(8,128)(2,1)S(1)}, bf16[512,256]{1,0:T(8,128)(2,1)S(1)}, u32[]{:S(2)}, u32[]{:S(2)}) collective-permute-start(bf16[512,256]{1,0:T(8,128)(2,1)S(1)} %convolution_convert_fusion.2), channel_id=1, source_target_pairs={{0,4},{1,5},{2,6},{3,7},{4,8},{5,9},{6,10},{7,11},{8,12},{9,13},{1... | collective-permute-start | bytes 786440 | tf_op jit(solution)/shard_map/ppermute | solution.py:25
  114.1 12.1 %collective-permute-done.5 = bf16[512,256]{1,0:T(8,128)(2,1)S(1)} collective-permute-done((bf16[512,256]{1,0:T(8,128)(2,1)S(1)}, bf16[512,256]{1,0:T(8,128)(2,1)S(1)}, u32[]{:S(2)}, u32[]{:S(2)}) %collective-permute-start.5) | collective-permute-done | bytes 262176 | tf_op jit(solution)/shard_map/ppermute | solution.py:25
  126.2 3.6 %collective-permute-done.4 = bf16[512,256]{1,0:T(8,128)(2,1)S(1)} collective-permute-done((bf16[512,256]{1,0:T(8,128)(2,1)S(1)}, bf16[512,256]{1,0:T(8,128)(2,1)S(1)}, u32[]{:S(2)}, u32[]{:S(2)}) %collective-permute-start.4) | collective-permute-done | bytes 262176 | tf_op jit(solution)/shard_map/ppermute | solution.py:25
  130.2 2.6 %collective-permute-start.9 = (bf16[2,64,256]{2,1,0:T(8,128)(2,1)S(1)}, bf16[2,64,256]{2,1,0:T(8,128)(2,1)S(1)}, u32[]{:S(2)}, u32[]{:S(2)}) collective-permute-start(bf16[2,64,256]{2,1,0:T(8,128)(2,1)S(1)} %get-tuple-element.22), channel_id=1, source_target_pairs={{0,3},{1,0},{2,1},{3,2},{4,7},{5,4},{6,5},{7,6},{8,11},{9,8},{10,9... | collective-permute-start | bytes 196616 | tf_op jit(solution)/shard_map/ppermute | solution.py:25
  132.8 5.2 %collective-permute-start.8 = (bf16[2,64,256]{2,1,0:T(8,128)(2,1)S(1)}, bf16[2,64,256]{2,1,0:T(8,128)(2,1)S(1)}, u32[]{:S(2)}, u32[]{:S(2)}) collective-permute-start(bf16[2,64,256]{2,1,0:T(8,128)(2,1)S(1)} %get-tuple-element.23), channel_id=1, source_target_pairs={{0,2},{1,3},{2,0},{3,1},{4,6},{5,7},{6,4},{7,5},{8,10},{9,11},{10,... | collective-permute-start | bytes 196616 | tf_op jit(solution)/shard_map/ppermute | solution.py:25
  137.9 3.3 %collective-permute-start.7 = (bf16[2,64,256]{2,1,0:T(8,128)(2,1)S(1)}, bf16[2,64,256]{2,1,0:T(8,128)(2,1)S(1)}, u32[]{:S(2)}, u32[]{:S(2)}) collective-permute-start(bf16[2,64,256]{2,1,0:T(8,128)(2,1)S(1)} %get-tuple-element.21), channel_id=1, source_target_pairs={{0,1},{1,2},{2,3},{3,0},{4,5},{5,6},{6,7},{7,4},{8,9},{9,10},{10,1... | collective-permute-start | bytes 196616 | tf_op jit(solution)/shard_map/ppermute | solution.py:25
  142.6 7.5 %all-to-all-start.3 = ((bf16[8,64,256]{2,1,0:T(8,128)(2,1)}), bf16[8,64,256]{2,1,0:T(8,128)(2,1)S(1)}, u32[]{:S(2)}, u32[]{:S(2)}) async-start(bf16[8,64,256]{2,1,0:T(8,128)(2,1)} %bitcast.24), calls=%async_computation.3 | async-start | bytes 524288 | tf_op jit(solution)/shard_map/all_to_all | solution.py:16
  150.3 7.3 %collective-permute-start.10 = (bf16[64,256]{1,0:T(8,128)(2,1)S(1)}, bf16[64,256]{1,0:T(8,128)(2,1)S(1)}, u32[]{:S(2)}, u32[]{:S(2)}) collective-permute-start(bf16[64,256]{1,0:T(8,128)(2,1)S(1)} %dynamic-slice_bitcast_fusion.3), channel_id=1, source_target_pairs={{0,16},{1,17},{2,18},{3,19},{4,20},{5,21},{6,22},{7,23},{8,24},{9,... | collective-permute-start | bytes 98312 | tf_op jit(solution)/shard_map/ppermute | solution.py:25
  157.6 2.8 %all-to-all-done.3 = bf16[8,64,256]{2,1,0:T(8,128)(2,1)S(1)} async-done(((bf16[8,64,256]{2,1,0:T(8,128)(2,1)}), bf16[8,64,256]{2,1,0:T(8,128)(2,1)S(1)}, u32[]{:S(2)}, u32[]{:S(2)}) %all-to-all-start.3) | async-done | bytes 262176 | tf_op jit(solution)/shard_map/all_to_all | solution.py:16
  (61 shorter events, 13.6 us)
Async XLA Ops:
  0.0 22.7 %copy-start.1 = (bf16[1,2048,176]{1,2,0:T(8,128)(2,1)S(1)}, bf16[1,2048,176]{1,2,0:T(8,128)(2,1)}, u32[]{:S(2)}) copy-start(bf16[1,2048,176]{1,2,0:T(8,128)(2,1)} %param.16) | copy-start | bytes 2162692
  0.1 1.3 copy-start.4
  1.4 0.9 copy-start.6
  4.5 18.2 %copy-start = (bf16[1,2048,176]{1,2,0:T(8,128)(2,1)S(1)}, bf16[1,2048,176]{1,2,0:T(8,128)(2,1)}, u32[]{:S(2)}) copy-start(bf16[1,2048,176]{1,2,0:T(8,128)(2,1)} %param.15) | copy-start | bytes 2162692
  7.2 15.6 %copy-start.2 = (bf16[1,176,2048]{2,1,0:T(8,128)(2,1)S(1)}, bf16[1,176,2048]{2,1,0:T(8,128)(2,1)}, u32[]{:S(2)}) copy-start(bf16[1,176,2048]{2,1,0:T(8,128)(2,1)} %param.17) | copy-start | bytes 2162692
  7.2 48.5 %all-to-all-start = ((bf16[24,16,1024]{2,1,0:T(8,128)(2,1)}), bf16[24,16,1024]{2,1,0:T(8,128)(2,1)S(1)}, u32[]{:S(2)}, u32[]{:S(2)}) async-start(bf16[24,16,1024]{2,1,0:T(8,128)(2,1)} %bitcast.63), calls=%async_computation | async-start | bytes 1572864 | tf_op jit(solution)/shard_map/all_to_all | solution.py:16
  24.0 40.6 %collective-permute-start.2 = (bf16[288,2048]{1,0:T(8,128)(2,1)}, bf16[288,2048]{1,0:T(8,128)(2,1)S(1)}, u32[]{:S(2)}, u32[]{:S(2)}) collective-permute-start(bf16[288,2048]{1,0:T(8,128)(2,1)} %pad_maximum_fusion), channel_id=1, source_target_pairs={{0,1},{1,0},{2,3},{3,2},{4,5},{5,4},{6,7},{7,6},{8,9},{9,8},{10,11... | collective-permute-start | bytes 3538952 | tf_op jit(solution)/shard_map/ppermute | solution.py:25
  28.8 35.8 %collective-permute-start.3 = (bf16[240,2048]{1,0:T(8,128)(2,1)}, bf16[240,2048]{1,0:T(8,128)(2,1)}, u32[]{:S(2)}, u32[]{:S(2)}) collective-permute-start(bf16[240,2048]{1,0:T(8,128)(2,1)} %pad_maximum_fusion.1), channel_id=1, source_target_pairs={{0,3},{1,2},{2,1},{3,0},{4,7},{5,6},{6,5},{7,4},{8,11},{9,10},{10,... | collective-permute-start | bytes 2949128 | tf_op jit(solution)/shard_map/ppermute | solution.py:25
  55.8 11.2 %collective-permute-start = (bf16[384,512]{1,0:T(8,128)(2,1)S(1)}, bf16[384,512]{1,0:T(8,128)(2,1)S(1)}, u32[]{:S(2)}, u32[]{:S(2)}) collective-permute-start(bf16[384,512]{1,0:T(8,128)(2,1)S(1)} %get-tuple-element.20), channel_id=1, source_target_pairs={{0,4},{1,5},{2,6},{3,7},{4,0},{5,1},{6,2},{7,3},{8,12},{9,13},{10,... | collective-permute-start | bytes 1179656 | tf_op jit(solution)/shard_map/ppermute | solution.py:25
  59.3 12.4 %copy-start.3 = (bf16[1,176,2048]{2,1,0:T(8,128)(2,1)S(1)}, bf16[1,176,2048]{2,1,0:T(8,128)(2,1)}, u32[]{:S(2)}) copy-start(bf16[1,176,2048]{2,1,0:T(8,128)(2,1)} %param.17) | copy-start | bytes 2162692
  59.3 12.3 %collective-permute-start.1 = (bf16[384,512]{1,0:T(8,128)(2,1)S(1)}, bf16[384,512]{1,0:T(8,128)(2,1)S(1)}, u32[]{:S(2)}, u32[]{:S(2)}) collective-permute-start(bf16[384,512]{1,0:T(8,128)(2,1)S(1)} %get-tuple-element.19), channel_id=1, source_target_pairs={{0,28},{1,29},{2,30},{3,31},{4,8},{5,9},{6,10},{7,11},{8,4},{9,5},... | collective-permute-start | bytes 1179656 | tf_op jit(solution)/shard_map/ppermute | solution.py:25
  76.1 5.1 %copy-start.10 = (bf16[32,2048]{1,0:T(8,128)(2,1)S(1)}, bf16[32,2048]{1,0:T(8,128)(2,1)}, u32[]{:S(2)}) copy-start(bf16[32,2048]{1,0:T(8,128)(2,1)} %param.20) | copy-start | bytes 393220
  76.1 24.2 %all-to-all-start.1 = ((bf16[4,384,512]{2,1,0:T(8,128)(2,1)}), bf16[4,384,512]{2,1,0:T(8,128)(2,1)S(1)}, u32[]{:S(2)}, u32[]{:S(2)}) async-start(bf16[4,384,512]{2,1,0:T(8,128)(2,1)} %shard_map.111), calls=%async_computation.1 | async-start | bytes 3145728 | tf_op jit(solution)/shard_map/all_to_all | solution.py:16
  81.5 32.6 %copy-start.11 = (f32[256,2]{0,1:T(2,128)S(1)}, f32[256,2]{0,1:T(2,128)}, u32[]{:S(2)}) copy-start(f32[256,2]{0,1:T(2,128)} %param.14) | copy-start | bytes 6148
  81.5 32.7 %collective-permute-start.6 = (bf16[512,256]{1,0:T(8,128)(2,1)S(1)}, bf16[512,256]{1,0:T(8,128)(2,1)S(1)}, u32[]{:S(2)}, u32[]{:S(2)}) collective-permute-start(bf16[512,256]{1,0:T(8,128)(2,1)S(1)} %convolution_convert_fusion), channel_id=1, source_target_pairs={{0,28},{1,29},{2,30},{3,31},{4,0},{5,1},{6,2},{7,3},{8,4},{9,5},{1... | collective-permute-start | bytes 786440 | tf_op jit(solution)/shard_map/ppermute | solution.py:25
  101.3 39.9 %all-to-all-start.2 = ((bf16[24,16,512]{2,1,0:T(8,128)(2,1)}), bf16[24,16,512]{2,1,0:T(8,128)(2,1)S(1)}, u32[]{:S(2)}, u32[]{:S(2)}) async-start(bf16[24,16,512]{2,1,0:T(8,128)(2,1)} %bitcast.19), calls=%async_computation.2 | async-start | bytes 786432 | tf_op jit(solution)/shard_map/all_to_all | solution.py:16
  107.9 18.4 %collective-permute-start.5 = (bf16[512,256]{1,0:T(8,128)(2,1)S(1)}, bf16[512,256]{1,0:T(8,128)(2,1)S(1)}, u32[]{:S(2)}, u32[]{:S(2)}) collective-permute-start(bf16[512,256]{1,0:T(8,128)(2,1)S(1)} %convolution_convert_fusion.1), channel_id=1, source_target_pairs={{0,8},{1,9},{2,10},{3,11},{4,12},{5,13},{6,14},{7,15},{8,16},{9,17... | collective-permute-start | bytes 786440 | tf_op jit(solution)/shard_map/ppermute | solution.py:25
  112.1 17.7 %collective-permute-start.4 = (bf16[512,256]{1,0:T(8,128)(2,1)S(1)}, bf16[512,256]{1,0:T(8,128)(2,1)S(1)}, u32[]{:S(2)}, u32[]{:S(2)}) collective-permute-start(bf16[512,256]{1,0:T(8,128)(2,1)S(1)} %convolution_convert_fusion.2), channel_id=1, source_target_pairs={{0,4},{1,5},{2,6},{3,7},{4,8},{5,9},{6,10},{7,11},{8,12},{9,13},{1... | collective-permute-start | bytes 786440 | tf_op jit(solution)/shard_map/ppermute | solution.py:25
  130.1 20.1 %copy-start.12 = (f32[64]{0:T(128)S(1)}, f32[64]{0:T(128)}, u32[]{:S(2)}) copy-start(f32[64]{0:T(128)} %param.21) | copy-start | bytes 772
  130.2 20.0 %collective-permute-start.9 = (bf16[2,64,256]{2,1,0:T(8,128)(2,1)S(1)}, bf16[2,64,256]{2,1,0:T(8,128)(2,1)S(1)}, u32[]{:S(2)}, u32[]{:S(2)}) collective-permute-start(bf16[2,64,256]{2,1,0:T(8,128)(2,1)S(1)} %get-tuple-element.22), channel_id=1, source_target_pairs={{0,3},{1,0},{2,1},{3,2},{4,7},{5,4},{6,5},{7,6},{8,11},{9,8},{10,9... | collective-permute-start | bytes 196616 | tf_op jit(solution)/shard_map/ppermute | solution.py:25
  132.8 17.4 %collective-permute-start.8 = (bf16[2,64,256]{2,1,0:T(8,128)(2,1)S(1)}, bf16[2,64,256]{2,1,0:T(8,128)(2,1)S(1)}, u32[]{:S(2)}, u32[]{:S(2)}) collective-permute-start(bf16[2,64,256]{2,1,0:T(8,128)(2,1)S(1)} %get-tuple-element.23), channel_id=1, source_target_pairs={{0,2},{1,3},{2,0},{3,1},{4,6},{5,7},{6,4},{7,5},{8,10},{9,11},{10,... | collective-permute-start | bytes 196616 | tf_op jit(solution)/shard_map/ppermute | solution.py:25
  137.9 12.3 %collective-permute-start.7 = (bf16[2,64,256]{2,1,0:T(8,128)(2,1)S(1)}, bf16[2,64,256]{2,1,0:T(8,128)(2,1)S(1)}, u32[]{:S(2)}, u32[]{:S(2)}) collective-permute-start(bf16[2,64,256]{2,1,0:T(8,128)(2,1)S(1)} %get-tuple-element.21), channel_id=1, source_target_pairs={{0,1},{1,2},{2,3},{3,0},{4,5},{5,6},{6,7},{7,4},{8,9},{9,10},{10,1... | collective-permute-start | bytes 196616 | tf_op jit(solution)/shard_map/ppermute | solution.py:25
  142.6 17.7 %all-to-all-start.3 = ((bf16[8,64,256]{2,1,0:T(8,128)(2,1)}), bf16[8,64,256]{2,1,0:T(8,128)(2,1)S(1)}, u32[]{:S(2)}, u32[]{:S(2)}) async-start(bf16[8,64,256]{2,1,0:T(8,128)(2,1)} %bitcast.24), calls=%async_computation.3 | async-start | bytes 524288 | tf_op jit(solution)/shard_map/all_to_all | solution.py:16
  150.3 10.6 %collective-permute-start.10 = (bf16[64,256]{1,0:T(8,128)(2,1)S(1)}, bf16[64,256]{1,0:T(8,128)(2,1)S(1)}, u32[]{:S(2)}, u32[]{:S(2)}) collective-permute-start(bf16[64,256]{1,0:T(8,128)(2,1)S(1)} %dynamic-slice_bitcast_fusion.3), channel_id=1, source_target_pairs={{0,16},{1,17},{2,18},{3,19},{4,20},{5,21},{6,22},{7,23},{8,24},{9,... | collective-permute-start | bytes 98312 | tf_op jit(solution)/shard_map/ppermute | solution.py:25
  (4 other events, 3.2 us)
